TPU v7x, 256 devices: a whole 4x4x8 slice. The times are simulated.
256 devices in a mesh: fs: 32 (over z, y), tp: 8 (over x, core).
Axes of the slice: x: 4, y: 4, z: 8, core: 2. Of those that a mesh axis runs over, the one named last changes fastest.
Arguments:
- tokens: bfloat16 [8192, 2048], P('fs'), may hold values from -6 to 6
- routes: int32 [8192, 6], P('fs'), may hold values from 0 to 31, all different within a row; in each aligned block of 256 rows (0 to 255, 256 to 511, ...) at most 80 rows name the same one
- route_weights: float32 [8192, 6], P('fs'), may hold values from 0.1 to 1
- norm_gain: float32 [2048], P('fs'), may hold values from 0.1 to 1.9
- expert_gate: float32 [32, 2048, 1024], P(None, 'fs', 'tp'), may hold values from -0.125 to 0.125
- expert_up: float32 [32, 2048, 1024], P(None, 'fs', 'tp'), may hold values from -0.125 to 0.125
- expert_down: float32 [32, 2048, 1024], P(None, 'fs', 'tp'), may hold values from -0.1875 to 0.1875
- shared_gate: float32 [2048, 1024], P('fs', 'tp'), may hold values from -0.125 to 0.125
- shared_up: float32 [2048, 1024], P('fs', 'tp'), may hold values from -0.125 to 0.125
- shared_down: float32 [2048, 1024], P('fs', 'tp'), may hold values from -0.1875 to 0.1875
Outputs:
- layer_output: bfloat16 [8192, 2048], P('fs', 'tp')
- sample_gate: bfloat16 [32, 2048, 1024], P('fs', None, 'tp')
- sample_up: bfloat16 [32, 2048, 1024], P('fs', None, 'tp')
- sample_down: bfloat16 [32, 2048, 1024], P('fs', None, 'tp')
- common_gate: bfloat16 [2048, 1024], P(None, 'tp')
- common_up: bfloat16 [2048, 1024], P(None, 'tp')
- common_down: bfloat16 [2048, 1024], P(None, 'tp')
Inputs may be any that keep to these rules, and one draw needn't show every extreme that they name: `routes`: each row names 6 different experts. In each aligned block of 256 rows (the rows of one index of fs) no expert is named by more than 80 rows, a bound that some expert reaches in some blocks.
All inputs are finite; a program needn't handle non-finite values.
Results may differ from a plain program's by a relative error of at most 0.015.
Values may be sent and summed in bfloat16 or wider, within the bound.
No kernel may reach another device: no remote copies, remote signals or barrier semaphores. Data moves between devices by JAX's collectives and lax.ppermute only.
A program may use at most 128 MiB of HBM per device.

v0:
```python
import jax
import jax.numpy as jnp
from jax import lax
from jax.experimental import pallas as pl
from jax.experimental.pallas import tpu as pltpu
from jax.sharding import Mesh
from jax.sharding import PartitionSpec as P

EPSILON = 1e-06
FS = ("z", "y")
TP = ("x", "c")
NZ, NY, NX, NC = 8, 4, 4, 2
EXPERTS = 32
TOK = 256
D = 2048
FF = 1024
SHARE = 10
BF = jnp.bfloat16
F32 = jnp.float32


def iota(shape, dim):
    return lax.broadcasted_iota(jnp.int32, shape, dim)


def dot(a, b):
    return jnp.dot(a, b, preferred_element_type=F32)


def dot_t(a, b):
    return lax.dot_general(a, b, (((1,), (1,)), ((), ())), preferred_element_type=F32)


def flag(condition):
    return jnp.where(condition, 1.0, 0.0).astype(BF)


def shift(array, axis, size, by):
    return lax.ppermute(array, axis, [(i, (i + by) % size) for i in range(size)])


VMEM = pl.BlockSpec(memory_space=pltpu.VMEM)
SMEM = pl.BlockSpec(memory_space=pltpu.SMEM)
HBM = pl.BlockSpec(memory_space=pltpu.HBM)


def dispatch_kernel(at_ref, tokens_ref, routes_ref, packed_ref, normed_ref):
    base = (at_ref[0] * SHARE).astype(F32)
    values = tokens_ref[...].astype(F32)
    scale = lax.rsqrt(jnp.mean(values * values, axis=-1, keepdims=True) + EPSILON)
    normed = (values * scale).astype(BF)
    normed_ref[...] = normed
    expert = iota((EXPERTS, TOK), 0)
    member = jnp.zeros((EXPERTS, TOK), F32)
    for k in range(routes_ref.shape[0]):
        member = member + jnp.where(routes_ref[k : k + 1, :] == expert, 1.0, 0.0)
    earlier = flag(iota((TOK, TOK), 0) < iota((TOK, TOK), 1))
    position = dot(member.astype(BF), earlier)
    slot = jnp.where(member > 0.0, position, -1.0).astype(BF)
    row = iota((TOK, EXPERTS), 0)
    spread = flag(row // 8 == iota((TOK, EXPERTS), 1))
    slots = dot(spread, slot) - base
    inner = iota((TOK, TOK), 0) % 8
    first = flag(slots == inner.astype(F32))
    packed_ref[:, :D] = dot(first, normed).astype(BF)
    last = slots == (8 + inner % 2).astype(F32)
    tail = jnp.zeros((TOK, 512), F32)
    for j in range(4):
        pick = flag(jnp.logical_and(last, inner // 2 == j))
        tail = tail + dot(pick, normed[:, j * 512 : (j + 1) * 512])
    packed_ref[:, D:] = tail.astype(BF)


def dispatch(tokens, routes_t, at):
    return pl.pallas_call(
        dispatch_kernel,
        out_shape=(
            jax.ShapeDtypeStruct((TOK, D + 512), BF),
            jax.ShapeDtypeStruct((TOK, D), BF),
        ),
        in_specs=[SMEM, VMEM, VMEM],
        out_specs=(VMEM, VMEM),
        compiler_params=pltpu.CompilerParams(vmem_limit_bytes=24 << 20),
        cost_estimate=pl.CostEstimate(flops=10**9, bytes_accessed=4 << 20, transcendentals=0),
        name="dispatch",
    )(at, tokens, routes_t)


WAYS = 6
HALF = D // 2


def ffn_kernel(block_ref, *refs):
    source_refs = refs[: 3 * WAYS]
    out_ref, *sample_refs = refs[3 * WAYS : 3 * WAYS + 4]
    weight_ref, rows_ref, total_ref, hidden_ref, sems, sample_sems = refs[3 * WAYS + 4 :]
    copies = []
    for n in range(3):
        own, left, right, near, far, other = source_refs[n * WAYS : (n + 1) * WAYS]
        pieces = [
            (own, weight_ref.at[n, 0]),
            (left, weight_ref.at[n, 1]),
            (right, weight_ref.at[n, 2]),
            (near, weight_ref.at[n, 3, 0:HALF]),
            (far, weight_ref.at[n, 3, HALF:D]),
            (other, weight_ref.at[n, 4:8]),
        ]
        copies.append(
            [
                pltpu.make_async_copy(source, target, sems.at[n, i])
                for i, (source, target) in enumerate(pieces)
            ]
        )
    for group in zip(*copies):
        for copy in group:
            copy.start()

    rows_ref[0:TOK, :] = block_ref[:, :D]
    tail = block_ref[:, D:]
    out_row = iota((64, TOK), 0)
    in_row = iota((64, TOK), 1)
    for j in range(4):
        pick = flag(
            jnp.logical_and(out_row // 2 == in_row // 8, in_row % 8 == 2 * j + out_row % 2)
        )
        rows_ref[TOK : TOK + 64, j * 512 : (j + 1) * 512] = dot(pick, tail).astype(BF)

    def wide(n, first):
        return jnp.concatenate([weight_ref[n, first], weight_ref[n, first + 1]], axis=1)

    def step(first, fresh):
        gate = dot(rows_ref[...], wide(0, first))
        up = dot(rows_ref[...], wide(1, first))
        hidden_ref[...] = (gate / (1.0 + jnp.exp(-gate)) * up).astype(BF)
        for m in range(4):
            part = slice(m * 512, (m + 1) * 512)
            down = jnp.concatenate(
                [weight_ref[2, first, part, :], weight_ref[2, first + 1, part, :]], axis=1
            )
            term = dot_t(hidden_ref[...], down)
            if fresh:
                total_ref[:, part] = term
            else:
                total_ref[:, part] += term

    def wait(first, last):
        for i in range(first, last):
            for n in range(3):
                copies[n][i].wait()

    wait(0, 2)
    kept = [
        pltpu.make_async_copy(weight_ref.at[n, 0], sample_refs[n].at[0], sample_sems.at[n])
        for n in range(3)
    ]
    for copy in kept:
        copy.start()
    step(0, True)
    wait(2, WAYS)

    @pl.loop(1, 4)
    def _(pair):
        step(2 * pair, False)

    tail = total_ref[TOK : TOK + 64, :].astype(BF)
    out_row = iota((TOK, 64), 0)
    in_row = iota((TOK, 64), 1)
    packed = jnp.zeros((TOK, 512), F32)
    for j in range(4):
        pick = flag(
            jnp.logical_and(in_row // 2 == out_row // 8, out_row % 8 == 2 * j + in_row % 2)
        )
        piece = jnp.concatenate(
            [tail[:, x * 512 + j * 128 : x * 512 + (j + 1) * 128] for x in range(NX)], axis=1
        )
        packed = packed + dot(pick, piece)
    for x in range(NX):
        body = total_ref[0:TOK, x * 512 : (x + 1) * 512]
        out_ref[:, x, :, 0:512] = body.astype(BF).reshape(EXPERTS, 8, 512)
        out_ref[:, x, :, 512:640] = (
            packed[:, x * 128 : (x + 1) * 128].astype(BF).reshape(EXPERTS, 8, 128)
        )
    for copy in kept:
        copy.wait()


def ffn(block, gate, up, down):
    sample = jax.ShapeDtypeStruct((1, D, 128), BF)
    return pl.pallas_call(
        ffn_kernel,
        out_shape=(jax.ShapeDtypeStruct((EXPERTS, NX, 8, 640), BF), sample, sample, sample),
        in_specs=[VMEM] + [HBM] * (3 * WAYS),
        out_specs=(VMEM, HBM, HBM, HBM),
        scratch_shapes=[
            pltpu.VMEM((3, 8, D, 128), BF),
            pltpu.VMEM((TOK + 64, D), BF),
            pltpu.VMEM((TOK + 64, D), F32),
            pltpu.VMEM((TOK + 64, 256), BF),
            pltpu.SemaphoreType.DMA((3, WAYS)),
            pltpu.SemaphoreType.DMA((3,)),
        ],
        compiler_params=pltpu.CompilerParams(vmem_limit_bytes=52 << 20),
        cost_estimate=pl.CostEstimate(
            flops=6 * 320 * D * FF, bytes_accessed=16 << 20, transcendentals=320 * FF
        ),
        name="ffn",
    )(block, *gate, *up, *down)


def combine_kernel(core_ref, routes_ref, weights_ref, back_ref, own_ref, other_ref):
    core = core_ref[0]
    expert = iota((TOK, EXPERTS), 1)
    member = jnp.zeros((TOK, EXPERTS), F32)
    weight = jnp.zeros((TOK, EXPERTS), F32)
    for k in range(routes_ref.shape[1]):
        same = routes_ref[:, k : k + 1] == expert
        member = member + jnp.where(same, 1.0, 0.0)
        weight = weight + jnp.where(same, weights_ref[:, k : k + 1], 0.0)
    earlier = flag(iota((TOK, TOK), 1) < iota((TOK, TOK), 0))
    position = dot(earlier, member.astype(BF))
    slot = jnp.where(member > 0.0, position, -1.0).astype(BF)
    high = weight.astype(BF)
    low = (weight - high.astype(F32)).astype(BF)
    lanes = EXPERTS * NX * 8
    spread = flag(iota((EXPERTS, lanes), 1) // (NX * 8) == iota((EXPERTS, lanes), 0))
    slots = dot(slot, spread)
    lane = iota((TOK, lanes), 1)
    start = ((lane // 8) % NX * NC + core) * SHARE
    first = slots == (start + lane % 8).astype(F32)
    last = slots == (start + 8 + lane % 2).astype(F32)
    body = back_ref[:, 0:512]
    tail = back_ref[:, 512:640]
    total = jnp.zeros((TOK, 512), F32)
    pieces = [jnp.zeros((TOK, 128), F32)] * 4
    for part in (high, low):
        wide = dot(part, spread)
        total = total + dot(jnp.where(first, wide, 0.0).astype(BF), body)
        for j in range(4):
            mine = jnp.logical_and(last, lane % 8 // 2 == j)
            pieces[j] = pieces[j] + dot(jnp.where(mine, wide, 0.0).astype(BF), tail)
    total = total + jnp.concatenate(pieces, axis=1)
    left, right = total[:, :256], total[:, 256:]
    own_ref[...] = jnp.where(core == 0, left, right)
    other_ref[...] = jnp.where(core == 0, right, left).astype(BF)


def combine(back, routes, route_weights, core):
    return pl.pallas_call(
        combine_kernel,
        out_shape=(
            jax.ShapeDtypeStruct((TOK, 256), F32),
            jax.ShapeDtypeStruct((TOK, 256), BF),
        ),
        in_specs=[SMEM] + [VMEM] * 3,
        out_specs=(VMEM, VMEM),
        compiler_params=pltpu.CompilerParams(vmem_limit_bytes=24 << 20),
        cost_estimate=pl.CostEstimate(flops=10**9, bytes_accessed=4 << 20, transcendentals=0),
        name="combine",
    )(core, routes, route_weights, back)


def exchange(array, axes):
    return lax.all_to_all(array, axes, split_axis=0, concat_axis=0, tiled=True)


def after(*arrays):
    return lax.optimization_barrier(arrays)


def to_neighbours(rows):
    return shift(rows, "x", NX, 1), shift(rows, "x", NX, -1)


def to_opposite(near):
    return shift(near[0][:HALF], "x", NX, 1), shift(near[1][HALF:], "x", NX, -1)


def stacked(pieces):
    own, left, right, near, far = pieces
    return [own[None], left[None], right[None], jnp.concatenate([near, far])[None]]


def layer(
    tokens,
    routes,
    route_weights,
    norm_gain,
    expert_gate,
    expert_up,
    expert_down,
    shared_gate,
    shared_up,
    shared_down,
):
    x, c = (lax.axis_index(a).astype(jnp.int32) for a in TP)
    at = (x * NC + c).reshape(1)
    core = c.reshape(1)
    gain_rows = norm_gain[None, :, None]

    shared = jnp.concatenate(
        [
            (shared_gate * norm_gain[:, None]).astype(BF),
            (shared_up * norm_gain[:, None]).astype(BF),
            shared_down.astype(BF),
        ],
        axis=1,
    )
    common = lax.all_gather(shared, FS, axis=0, tiled=True)

    gate_in = (expert_gate * gain_rows).astype(BF)
    gate_in, expert_up, expert_down = after(gate_in, expert_up, expert_down)
    up_in = (expert_up * gain_rows).astype(BF)
    down_in = expert_down.astype(BF)
    packed, normed = dispatch(tokens, routes.T, at)

    gate_rows = exchange(gate_in, FS).reshape(D, 128)

    up_in, gate_rows = after(up_in, gate_rows)
    up_rows = exchange(up_in, FS).reshape(D, 128)
    gate_near = to_neighbours(gate_rows)

    down_in, up_rows, gate_near = after(down_in, up_rows, gate_near)
    down_rows = exchange(down_in, FS).reshape(D, 128)
    gate_far = to_opposite(gate_near)
    up_near = to_neighbours(up_rows)

    packed, down_rows, gate_far, up_near = after(packed, down_rows, gate_far, up_near)
    block = exchange(packed.reshape(EXPERTS, 8, D + 512), FS).reshape(TOK, D + 512)
    up_far = to_opposite(up_near)
    down_near = to_neighbours(down_rows)
    down_far = to_opposite(down_near)
    gate_all = [gate_rows, *gate_near, *gate_far]
    up_all = [up_rows, *up_near, *up_far]
    down_all = [down_rows, *down_near, *down_far]
    both = shift(jnp.concatenate(stacked(gate_all) + stacked(up_all)), "c", NC, 1)
    gate_all.append(both[:4])
    up_all.append(both[4:])
    down_all.append(shift(jnp.concatenate(stacked(down_all)), "c", NC, 1))

    common_gate, common_up, common_down = jnp.split(common, 3, axis=1)
    shared_hidden = (
        jax.nn.silu(dot(normed, common_gate)) * dot(normed, common_up)
    ).astype(BF)
    shared_terms = dot_t(shared_hidden, common_down).astype(BF)
    shared_terms = jnp.moveaxis(shared_terms.reshape(TOK, NX * NC, 256), 1, 0)
    shared_sum = lax.psum_scatter(shared_terms, TP, scatter_dimension=0, tiled=True)[0]

    results, sample_gate, sample_up, sample_down = ffn(block, gate_all, up_all, down_all)
    back = exchange(results.reshape(EXPERTS * NX, 8, 640), ("z", "y", "x"))
    own, other = combine(back.reshape(EXPERTS * NX * 8, 640), routes, route_weights, core)
    other = shift(other, "c", NC, 1)
    layer_output = (own + other.astype(F32) + shared_sum.astype(F32)).astype(BF)
    return (
        layer_output,
        sample_gate,
        sample_up,
        sample_down,
        common_gate,
        common_up,
        common_down,
    )


def solution(mesh):
    mesh = Mesh(mesh.devices.reshape(NZ, NY, NX, NC), FS + TP)
    return jax.shard_map(
        layer,
        mesh=mesh,
        in_specs=(
            P(FS, None),
            P(FS, None),
            P(FS, None),
            P(FS),
            P(None, FS, TP),
            P(None, FS, TP),
            P(None, FS, TP),
            P(FS, TP),
            P(FS, TP),
            P(FS, TP),
        ),
        out_specs=(
            P(FS, TP),
            P(FS, None, TP),
            P(FS, None, TP),
            P(FS, None, TP),
            P(None, TP),
            P(None, TP),
            P(None, TP),
        ),
        check_vma=False,
    )
```

profile of v0, /device:TPU:16, one launch (start us, length us, event | category | flops | bytes accessed | tf_op | source)
XLA Modules:
  0.0 251.3 jit_solution(107043689783148761)
XLA Ops:
  7.2 2.4 multiply_convert_fusion.1
  9.6 11.6 %all-to-all-start = ((bf16[32,64,128]{2,1,0:T(8,128)(2,1)}), bf16[32,64,128]{2,1,0:T(8,128)(2,1)S(1)}, u32[]{:S(2)}, u32[]{:S(2)}) async-start(bf16[32,64,128]{2,1,0:T(8,128)(2,1)} %multiply_convert_fusion.1), calls=%async_computation | async-start | bytes 1048576 | tf_op jit(solution)/shard_map/all_to_all | solution.py:263
  21.2 2.2 multiply_convert_fusion
  23.4 14.6 %all-to-all-done = bf16[32,64,128]{2,1,0:T(8,128)(2,1)S(1)} async-done(((bf16[32,64,128]{2,1,0:T(8,128)(2,1)}), bf16[32,64,128]{2,1,0:T(8,128)(2,1)S(1)}, u32[]{:S(2)}, u32[]{:S(2)}) %all-to-all-start) | async-done | bytes 524320 | tf_op jit(solution)/shard_map/all_to_all | solution.py:263
  38.0 5.6 %all-to-all-start.1 = ((bf16[32,64,128]{2,1,0:T(8,128)(2,1)}), bf16[32,64,128]{2,1,0:T(8,128)(2,1)S(1)}, u32[]{:S(2)}, u32[]{:S(2)}) async-start(bf16[32,64,128]{2,1,0:T(8,128)(2,1)} %multiply_convert_fusion), calls=%async_computation.1 | async-start | bytes 1048576 | tf_op jit(solution)/shard_map/all_to_all | solution.py:263
  45.1 1.7 collective-permute-start.1
  47.8 2.2 dispatch.1
  49.9 7.3 %collective-permute-done.refs_1_ = bf16[2048,128]{1,0:T(8,128)(2,1)} collective-permute-done((bf16[2048,128]{1,0:T(8,128)(2,1)S(1)}, bf16[2048,128]{1,0:T(8,128)(2,1)}, u32[]{:S(2)}, u32[]{:S(2)}) %collective-permute-start) | collective-permute-done | bytes 524320 | tf_op jit(solution)/shard_map/ppermute | solution.py:39
  57.2 2.3 all-to-all-done.1
  59.5 7.5 %all-to-all-start.2 = ((bf16[32,64,128]{2,1,0:T(8,128)(2,1)}), bf16[32,64,128]{2,1,0:T(8,128)(2,1)S(1)}, u32[]{:S(2)}, u32[]{:S(2)}) async-start(bf16[32,64,128]{2,1,0:T(8,128)(2,1)} %convert_element_type.37), calls=%async_computation.2 | async-start | bytes 1048576 | tf_op jit(solution)/shard_map/all_to_all | solution.py:263
  68.7 1.8 collective-permute-start.5
  72.7 3.0 %collective-permute-start.3 = (bf16[1024,128]{1,0:T(8,128)(2,1)S(1)}, bf16[1024,128]{1,0:T(8,128)(2,1)S(1)}, u32[]{:S(2)}, u32[]{:S(2)}) collective-permute-start(bf16[1024,128]{1,0:T(8,128)(2,1)S(1)} %slice.25), channel_id=1, source_target_pairs={{0,6},{2,0},{4,2},{6,4},{1,7},{3,1},{5,3},{7,5},{8,14},{10,8},{12,... | collective-permute-start | bytes 786440 | tf_op jit(solution)/shard_map/ppermute | solution.py:39
  78.1 6.8 %collective-permute-done.2.refs_3_ = bf16[1024,128]{1,0:T(8,128)(2,1)S(1)} collective-permute-done((bf16[1024,128]{1,0:T(8,128)(2,1)S(1)}, bf16[1024,128]{1,0:T(8,128)(2,1)S(1)}, u32[]{:S(2)}, u32[]{:S(2)}) %collective-permute-start.2) | collective-permute-done | bytes 262176 | tf_op jit(solution)/shard_map/ppermute | solution.py:39
  88.3 1.9 bitcast_dynamic-update-slice_fusion.1
  92.2 2.3 collective-permute-start.7
  94.5 1.9 bitcast_dynamic-update-slice_fusion
  101.1 1.9 collective-permute-start.10
  103.0 12.6 %collective-permute-done.9.refs_13_ = bf16[2048,128]{1,0:T(8,128)(2,1)S(1)} collective-permute-done((bf16[2048,128]{1,0:T(8,128)(2,1)S(1)}, bf16[2048,128]{1,0:T(8,128)(2,1)S(1)}, u32[]{:S(2)}, u32[]{:S(2)}) %collective-permute-start.9) | collective-permute-done | bytes 524320 | tf_op jit(solution)/shard_map/ppermute | solution.py:39
  118.2 3.2 %collective-permute-start.12 = (bf16[1024,128]{1,0:T(8,128)(2,1)}, bf16[1024,128]{1,0:T(8,128)(2,1)S(1)}, u32[]{:S(2)}, u32[]{:S(2)}) collective-permute-start(bf16[1024,128]{1,0:T(8,128)(2,1)} %slice.35), channel_id=1, source_target_pairs={{0,6},{2,0},{4,2},{6,4},{1,7},{3,1},{5,3},{7,5},{8,14},{10,8},{12,... | collective-permute-start | bytes 786440 | tf_op jit(solution)/shard_map/ppermute | solution.py:39
  122.2 9.8 %all-to-all-start.3 = ((bf16[32,8,2560]{2,1,0:T(8,128)(2,1)}), bf16[32,8,2560]{2,1,0:T(8,128)(2,1)}, u32[]{:S(2)}, u32[]{:S(2)}) async-start(bf16[32,8,2560]{2,1,0:T(8,128)(2,1)} %bitcast.6), calls=%async_computation.3 | async-start | bytes 2621440 | tf_op jit(solution)/shard_map/all_to_all | solution.py:263
  132.1 2.9 %pad_maximum_fusion = bf16[4,2048,128]{2,1,0:T(8,128)(2,1)} fusion(bf16[1,2048,128]{2,1,0:T(8,128)(2,1)S(1)} %maximum_bitcast_fusion.2, bf16[1,2048,128]{2,1,0:T(8,128)(2,1)} %bitcast.63, bf16[1,2048,128]{2,1,0:T(8,128)(2,1)} %bitcast.62, bf16[1,2048,128]{2,1,0:T(8,128)(2,1)S(1)} %bitcast.59), kind=kLoop, calls=%fused_computation.1 | loop fusion | flops 3145728 | bytes 4194304 | tf_op jit(solution)/shard_map/concatenate | solution.py:338
  135.0 4.6 %fusion.11 = (bf16[4,2048,128]{2,1,0:T(8,128)(2,1)}, bf16[4,2048,128]{2,1,0:T(8,128)(2,1)}) fusion(bf16[8,2048,128]{2,1,0:T(8,128)(2,1)} %collective-permute-done.8), kind=kLoop, calls=%fused_computation.29 | loop fusion | bytes 8388608 | tf_op jit(solution)/shard_map/slice | solution.py:337
  139.5 27.2 %all-to-all-done.3 = bf16[32,8,2560]{2,1,0:T(8,128)(2,1)} async-done(((bf16[32,8,2560]{2,1,0:T(8,128)(2,1)}), bf16[32,8,2560]{2,1,0:T(8,128)(2,1)}, u32[]{:S(2)}, u32[]{:S(2)}) %all-to-all-start.3) | async-done | bytes 1310752 | tf_op jit(solution)/shard_map/all_to_all | solution.py:263
  166.7 11.9 %ffn.1 = (bf16[32,4,8,640]{3,2,1,0:T(8,128)(2,1)}, bf16[1,2048,128]{2,1,0:T(8,128)(2,1)}, bf16[1,2048,128]{2,1,0:T(8,128)(2,1)}, bf16[1,2048,128]{2,1,0:T(8,128)(2,1)}) custom-call(bf16[256,2560]{1,0:T(8,128)(2,1)} %bitcast.7.block_ref, bf16[2048,128]{1,0:T(8,128)(2,1)} %bitcast.52, bf16[2048,128]{1,0:T(8,128)(2,1)} %collective-permute-done.refs_1_, ...), custom_call_target="tpu_custom_call" | custom-call | flops 4026531840 | bytes 16777216 | tf_op jit(solution)/shard_map/ffn/pallas_call | solution.py:189
  178.6 7.1 %all-to-all-start.4 = ((bf16[128,8,640]{2,1,0:T(8,128)(2,1)}), bf16[128,8,640]{2,1,0:T(8,128)(2,1)S(1)}, u32[]{:S(2)}, u32[]{:S(2)}) async-start(bf16[128,8,640]{2,1,0:T(8,128)(2,1)} %bitcast.61), calls=%async_computation.4 | async-start | bytes 2621440 | tf_op jit(solution)/shard_map/all_to_all | solution.py:263
  185.7 16.0 %all-gather.2.cloned.1.call-done = bf16[2048,384]{1,0:T(8,128)(2,1)} async-done(((bf16[64,384]{1,0:T(8,128)(2,1)}), bf16[2048,384]{1,0:T(8,128)(2,1)}) %all-gather.2.cloned.1.call-update) | async-done | bytes 1572880 | tf_op jit(solution)/shard_map/all_gather | solution.py:308
  201.7 2.4 fusion.12
  205.0 2.0 convolution_convert_fusion
  209.2 11.9 %all-to-all-done.4 = bf16[128,8,640]{2,1,0:T(8,128)(2,1)S(1)} async-done(((bf16[128,8,640]{2,1,0:T(8,128)(2,1)}), bf16[128,8,640]{2,1,0:T(8,128)(2,1)S(1)}, u32[]{:S(2)}, u32[]{:S(2)}) %all-to-all-start.4) | async-done | bytes 1310752 | tf_op jit(solution)/shard_map/all_to_all | solution.py:263
  221.0 3.1 %combine.1 = (f32[256,256]{1,0:T(8,128)S(1)}, bf16[256,256]{1,0:T(8,128)(2,1)S(1)}) custom-call(s32[1]{0:T(128)} %bitcast.core_ref, s32[256,6]{1,0:T(8,128)S(1)} %copy.19.routes_ref, f32[256,6]{1,0:T(8,128)S(1)} %copy.20.weights_ref, bf16[1024,640]{1,0:T(8,128)(2,1)S(1)} %bitcast.45), custom_call_target="tpu_custom_call" | custom-call | flops 1000000000 | bytes 4194304 | tf_op jit(solution)/shard_map/combine/pallas_call | solution.py:248
  224.3 18.5 %reduce-scatter.2.cloned.1.call-done = bf16[1,256,256]{2,1,0:T(8,128)(2,1)} async-done(((bf16[8,256,256]{2,1,0:T(8,128)(2,1)}), bf16[1,256,256]{2,1,0:T(8,128)(2,1)}) %reduce-scatter.2.cloned.1.call-update) | async-done | bytes 131088 | tf_op jit(solution)/shard_map/reduce_scatter | solution.py:346
  242.8 1.6 fusion.3
  (80 shorter events, 25.2 us)
Async XLA Ops:
  7.2 39.7 %copy-start.9 = (f32[32,64,128]{2,1,0:T(8,128)S(1)}, f32[32,64,128]{2,1,0:T(8,128)}, u32[]{:S(2)}) copy-start(f32[32,64,128]{2,1,0:T(8,128)} %param.16) | copy-start | bytes 3145732
  7.2 40.6 %copy-start = (s32[256,6]{0,1:T(8,128)S(1)}, s32[256,6]{0,1:T(8,128)}, u32[]{:S(2)}) copy-start(s32[256,6]{0,1:T(8,128)} %param.11) | copy-start | bytes 18436
  7.2 40.6 %copy-start.1 = (bf16[256,2048]{1,0:T(8,128)(2,1)S(1)}, bf16[256,2048]{1,0:T(8,128)(2,1)}, u32[]{:S(2)}) copy-start(bf16[256,2048]{1,0:T(8,128)(2,1)} %tokens_ref.1) | copy-start | bytes 3145732
  9.6 28.4 %all-to-all-start = ((bf16[32,64,128]{2,1,0:T(8,128)(2,1)}), bf16[32,64,128]{2,1,0:T(8,128)(2,1)S(1)}, u32[]{:S(2)}, u32[]{:S(2)}) async-start(bf16[32,64,128]{2,1,0:T(8,128)(2,1)} %multiply_convert_fusion.1), calls=%async_computation | async-start | bytes 1048576 | tf_op jit(solution)/shard_map/all_to_all | solution.py:263
  38.0 29.1 %copy-start.2 = (bf16[32,64,128]{2,1,0:T(8,128)(2,1)}, bf16[32,64,128]{2,1,0:T(8,128)(2,1)S(1)}, u32[]{:S(2)}) copy-start(bf16[32,64,128]{2,1,0:T(8,128)(2,1)S(1)} %all-to-all-done) | copy-start | bytes 1572868
  38.0 21.5 %all-to-all-start.1 = ((bf16[32,64,128]{2,1,0:T(8,128)(2,1)}), bf16[32,64,128]{2,1,0:T(8,128)(2,1)S(1)}, u32[]{:S(2)}, u32[]{:S(2)}) async-start(bf16[32,64,128]{2,1,0:T(8,128)(2,1)} %multiply_convert_fusion), calls=%async_computation.1 | async-start | bytes 1048576 | tf_op jit(solution)/shard_map/all_to_all | solution.py:263
  43.6 13.6 %collective-permute-start = (bf16[2048,128]{1,0:T(8,128)(2,1)S(1)}, bf16[2048,128]{1,0:T(8,128)(2,1)}, u32[]{:S(2)}, u32[]{:S(2)}) collective-permute-start(bf16[2048,128]{1,0:T(8,128)(2,1)S(1)} %bitcast.49), channel_id=1, source_target_pairs={{0,2},{2,4},{4,6},{6,0},{1,3},{3,5},{5,7},{7,1},{8,10},{10,12},{12... | collective-permute-start | bytes 1572872 | tf_op jit(solution)/shard_map/ppermute | solution.py:39
  45.1 12.1 %collective-permute-start.1 = (bf16[2048,128]{1,0:T(8,128)(2,1)S(1)}, bf16[2048,128]{1,0:T(8,128)(2,1)}, u32[]{:S(2)}, u32[]{:S(2)}) collective-permute-start(bf16[2048,128]{1,0:T(8,128)(2,1)S(1)} %bitcast.50), channel_id=1, source_target_pairs={{0,6},{2,0},{4,2},{6,4},{1,7},{3,1},{5,3},{7,5},{8,14},{10,8},{12,... | collective-permute-start | bytes 1572872 | tf_op jit(solution)/shard_map/ppermute | solution.py:39
  59.5 30.7 %copy-start.3 = (bf16[32,64,128]{2,1,0:T(8,128)(2,1)}, bf16[32,64,128]{2,1,0:T(8,128)(2,1)S(1)}, u32[]{:S(2)}) copy-start(bf16[32,64,128]{2,1,0:T(8,128)(2,1)S(1)} %all-to-all-done.1) | copy-start | bytes 1572868
  59.5 26.1 %all-to-all-start.2 = ((bf16[32,64,128]{2,1,0:T(8,128)(2,1)}), bf16[32,64,128]{2,1,0:T(8,128)(2,1)S(1)}, u32[]{:S(2)}, u32[]{:S(2)}) async-start(bf16[32,64,128]{2,1,0:T(8,128)(2,1)} %convert_element_type.37), calls=%async_computation.2 | async-start | bytes 1048576 | tf_op jit(solution)/shard_map/all_to_all | solution.py:263
  67.0 134.7 %all-gather.2.cloned.1.call-start = ((), (), s32[]{:S(2)}) async-start(), calls=%async_computation.6 | async-start | bytes 1622016 | tf_op jit(solution)/shard_map/all_gather | solution.py:308
  67.1 17.7 %collective-permute-start.4 = (bf16[2048,128]{1,0:T(8,128)(2,1)S(1)}, bf16[2048,128]{1,0:T(8,128)(2,1)S(1)}, u32[]{:S(2)}, u32[]{:S(2)}) collective-permute-start(bf16[2048,128]{1,0:T(8,128)(2,1)S(1)} %bitcast.53), channel_id=1, source_target_pairs={{0,2},{2,4},{4,6},{6,0},{1,3},{3,5},{5,7},{7,1},{8,10},{10,12},{12... | collective-permute-start | bytes 1572872 | tf_op jit(solution)/shard_map/ppermute | solution.py:39
  68.7 17.0 %collective-permute-start.5 = (bf16[2048,128]{1,0:T(8,128)(2,1)S(1)}, bf16[2048,128]{1,0:T(8,128)(2,1)}, u32[]{:S(2)}, u32[]{:S(2)}) collective-permute-start(bf16[2048,128]{1,0:T(8,128)(2,1)S(1)} %bitcast.54), channel_id=1, source_target_pairs={{0,6},{2,0},{4,2},{6,4},{1,7},{3,1},{5,3},{7,5},{8,14},{10,8},{12,... | collective-permute-start | bytes 1572872 | tf_op jit(solution)/shard_map/ppermute | solution.py:39
  71.4 13.4 %collective-permute-start.2 = (bf16[1024,128]{1,0:T(8,128)(2,1)S(1)}, bf16[1024,128]{1,0:T(8,128)(2,1)S(1)}, u32[]{:S(2)}, u32[]{:S(2)}) collective-permute-start(bf16[1024,128]{1,0:T(8,128)(2,1)S(1)} %slice.24), channel_id=1, source_target_pairs={{0,2},{2,4},{4,6},{6,0},{1,3},{3,5},{5,7},{7,1},{8,10},{10,12},{12... | collective-permute-start | bytes 786440 | tf_op jit(solution)/shard_map/ppermute | solution.py:39
  72.7 12.1 %collective-permute-start.3 = (bf16[1024,128]{1,0:T(8,128)(2,1)S(1)}, bf16[1024,128]{1,0:T(8,128)(2,1)S(1)}, u32[]{:S(2)}, u32[]{:S(2)}) collective-permute-start(bf16[1024,128]{1,0:T(8,128)(2,1)S(1)} %slice.25), channel_id=1, source_target_pairs={{0,6},{2,0},{4,2},{6,4},{1,7},{3,1},{5,3},{7,5},{8,14},{10,8},{12,... | collective-permute-start | bytes 786440 | tf_op jit(solution)/shard_map/ppermute | solution.py:39
  76.9 44.5 %copy-start.11 = (f32[64,128]{1,0:T(8,128)S(1)}, f32[64,128]{1,0:T(8,128)}, u32[]{:S(2)}) copy-start(f32[64,128]{1,0:T(8,128)} %param.17) | copy-start | bytes 98308
  76.9 44.5 %copy-start.12 = (f32[64,128]{1,0:T(8,128)S(1)}, f32[64,128]{1,0:T(8,128)}, u32[]{:S(2)}) copy-start(f32[64,128]{1,0:T(8,128)} %param.18) | copy-start | bytes 98308
  76.9 44.5 %copy-start.15 = (f32[64]{0:T(128)S(1)}, f32[64]{0:T(128)}, u32[]{:S(2)}) copy-start(f32[64]{0:T(128)} %param.13) | copy-start | bytes 772
  76.9 44.6 %copy-start.13 = (f32[64,128]{1,0:T(8,128)S(1)}, f32[64,128]{1,0:T(8,128)}, u32[]{:S(2)}) copy-start(f32[64,128]{1,0:T(8,128)} %param.19) | copy-start | bytes 98308
  85.7 46.4 %copy-start.5 = (bf16[32,64,128]{2,1,0:T(8,128)(2,1)}, bf16[32,64,128]{2,1,0:T(8,128)(2,1)S(1)}, u32[]{:S(2)}) copy-start(bf16[32,64,128]{2,1,0:T(8,128)(2,1)S(1)} %all-to-all-done.2) | copy-start | bytes 1572868
  90.2 7.6 %collective-permute-start.6 = (bf16[1024,128]{1,0:T(8,128)(2,1)S(1)}, bf16[1024,128]{1,0:T(8,128)(2,1)S(1)}, u32[]{:S(2)}, u32[]{:S(2)}) collective-permute-start(bf16[1024,128]{1,0:T(8,128)(2,1)S(1)} %slice.26), channel_id=1, source_target_pairs={{0,2},{2,4},{4,6},{6,0},{1,3},{3,5},{5,7},{7,1},{8,10},{10,12},{12... | collective-permute-start | bytes 786440 | tf_op jit(solution)/shard_map/ppermute | solution.py:39
  92.2 6.4 %collective-permute-start.7 = (bf16[1024,128]{1,0:T(8,128)(2,1)S(1)}, bf16[1024,128]{1,0:T(8,128)(2,1)S(1)}, u32[]{:S(2)}, u32[]{:S(2)}) collective-permute-start(bf16[1024,128]{1,0:T(8,128)(2,1)S(1)} %slice.27), channel_id=1, source_target_pairs={{0,6},{2,0},{4,2},{6,4},{1,7},{3,1},{5,3},{7,5},{8,14},{10,8},{12,... | collective-permute-start | bytes 786440 | tf_op jit(solution)/shard_map/ppermute | solution.py:39
  99.5 35.5 %collective-permute-start.8 = (bf16[8,2048,128]{2,1,0:T(8,128)(2,1)}, bf16[8,2048,128]{2,1,0:T(8,128)(2,1)}, u32[]{:S(2)}, u32[]{:S(2)}) collective-permute-start(bf16[8,2048,128]{2,1,0:T(8,128)(2,1)} %fusion.2), channel_id=1, source_target_pairs={{0,1},{1,0},{2,3},{3,2},{4,5},{5,4},{6,7},{7,6},{8,9},{9,8},{10,11... | collective-permute-start | bytes 12582920 | tf_op jit(solution)/shard_map/ppermute | solution.py:39
  99.5 16.0 %collective-permute-start.9 = (bf16[2048,128]{1,0:T(8,128)(2,1)S(1)}, bf16[2048,128]{1,0:T(8,128)(2,1)S(1)}, u32[]{:S(2)}, u32[]{:S(2)}) collective-permute-start(bf16[2048,128]{1,0:T(8,128)(2,1)S(1)} %bitcast.57), channel_id=1, source_target_pairs={{0,2},{2,4},{4,6},{6,0},{1,3},{3,5},{5,7},{7,1},{8,10},{10,12},{12... | collective-permute-start | bytes 1572872 | tf_op jit(solution)/shard_map/ppermute | solution.py:39
  101.1 15.5 %collective-permute-start.10 = (bf16[2048,128]{1,0:T(8,128)(2,1)S(1)}, bf16[2048,128]{1,0:T(8,128)(2,1)S(1)}, u32[]{:S(2)}, u32[]{:S(2)}) collective-permute-start(bf16[2048,128]{1,0:T(8,128)(2,1)S(1)} %bitcast.58), channel_id=1, source_target_pairs={{0,6},{2,0},{4,2},{6,4},{1,7},{3,1},{5,3},{7,5},{8,14},{10,8},{12,... | collective-permute-start | bytes 1572872 | tf_op jit(solution)/shard_map/ppermute | solution.py:39
  116.4 15.6 %collective-permute-start.11 = (bf16[1024,128]{1,0:T(8,128)(2,1)S(1)}, bf16[1024,128]{1,0:T(8,128)(2,1)S(1)}, u32[]{:S(2)}, u32[]{:S(2)}) collective-permute-start(bf16[1024,128]{1,0:T(8,128)(2,1)S(1)} %slice.34), channel_id=1, source_target_pairs={{0,2},{2,4},{4,6},{6,0},{1,3},{3,5},{5,7},{7,1},{8,10},{10,12},{12... | collective-permute-start | bytes 786440 | tf_op jit(solution)/shard_map/ppermute | solution.py:39
  118.2 13.8 %collective-permute-start.12 = (bf16[1024,128]{1,0:T(8,128)(2,1)}, bf16[1024,128]{1,0:T(8,128)(2,1)S(1)}, u32[]{:S(2)}, u32[]{:S(2)}) collective-permute-start(bf16[1024,128]{1,0:T(8,128)(2,1)} %slice.35), channel_id=1, source_target_pairs={{0,6},{2,0},{4,2},{6,4},{1,7},{3,1},{5,3},{7,5},{8,14},{10,8},{12,... | collective-permute-start | bytes 786440 | tf_op jit(solution)/shard_map/ppermute | solution.py:39
  122.2 44.5 %all-to-all-start.3 = ((bf16[32,8,2560]{2,1,0:T(8,128)(2,1)}), bf16[32,8,2560]{2,1,0:T(8,128)(2,1)}, u32[]{:S(2)}, u32[]{:S(2)}) async-start(bf16[32,8,2560]{2,1,0:T(8,128)(2,1)} %bitcast.6), calls=%async_computation.3 | async-start | bytes 2621440 | tf_op jit(solution)/shard_map/all_to_all | solution.py:263
  135.0 31.7 %collective-permute-start.13 = (bf16[4,2048,128]{2,1,0:T(8,128)(2,1)}, bf16[4,2048,128]{2,1,0:T(8,128)(2,1)}, u32[]{:S(2)}, u32[]{:S(2)}) collective-permute-start(bf16[4,2048,128]{2,1,0:T(8,128)(2,1)} %pad_maximum_fusion), channel_id=1, source_target_pairs={{0,1},{1,0},{2,3},{3,2},{4,5},{5,4},{6,7},{7,6},{8,9},{9,8},{10,11... | collective-permute-start | bytes 6291464 | tf_op jit(solution)/shard_map/ppermute | solution.py:39
  178.6 42.5 %all-to-all-start.4 = ((bf16[128,8,640]{2,1,0:T(8,128)(2,1)}), bf16[128,8,640]{2,1,0:T(8,128)(2,1)S(1)}, u32[]{:S(2)}, u32[]{:S(2)}) async-start(bf16[128,8,640]{2,1,0:T(8,128)(2,1)} %bitcast.61), calls=%async_computation.4 | async-start | bytes 2621440 | tf_op jit(solution)/shard_map/all_to_all | solution.py:263
  185.7 57.1 %reduce-scatter.2.cloned.1.call-start = ((), (), s32[]{:S(2)}) async-start(), calls=%async_computation.7 | async-start | bytes 1179648 | tf_op jit(solution)/shard_map/reduce_scatter | solution.py:346
  224.2 18.6 %collective-permute-start.14 = (bf16[256,256]{1,0:T(8,128)(2,1)S(1)}, bf16[256,256]{1,0:T(8,128)(2,1)S(1)}, u32[]{:S(2)}, u32[]{:S(2)}) collective-permute-start(bf16[256,256]{1,0:T(8,128)(2,1)S(1)} %get-tuple-element.48), channel_id=1, source_target_pairs={{0,1},{1,0},{2,3},{3,2},{4,5},{5,4},{6,7},{7,6},{8,9},{9,8},{10,11... | collective-permute-start | bytes 393224 | tf_op jit(solution)/shard_map/ppermute | solution.py:39
  (6 other events, 14.0 us)
Sparse Core Ops, SparseCore 0:
  122.3 79.4 all-gather.1
  209.0 33.7 reduce-scatter.1
where the time goes:
time: 252 us; the launch traced here: 251 us
  waiting for transfers between devices  119 us (47%)
  starting transfers between devices  62 us (25%)
  local copies, waits for them, and re-layouts  23.4 us (9%)
  Pallas kernels  17.2 us (7%)
  between operations  14.4 us (6%)
  other arithmetic  12.5 us (5%)
    all_to_all x5, waiting for transfers between devices, exchange(): return lax.all_to_all(array, axes, split_axis=0, concat_axis=0, tiled=True)  56 us
    all_to_all x5, starting transfers between devices, exchange(): return lax.all_to_all(array, axes, split_axis=0, concat_axis=0, tiled=True)  41.5 us
    ppermute x15, waiting for transfers between devices, shift(): lax.ppermute(array, axis, [(i, (i + by) % size) for i in range(size)])  28.9 us
    ppermute x15, starting transfers between devices, shift(): lax.ppermute(array, axis, [(i, (i + by) % size) for i in range(size)])  20.4 us
    reduce_scatter x1, waiting for transfers between devices, layer(): lax.psum_scatter(shared_terms, TP, scatter_dimension=0, tiled=True)[0]  18.5 us
    all_gather x1, waiting for transfers between devices, layer(): common = lax.all_gather(shared, FS, axis=0, tiled=True)  16 us
    pallas_call x1, Pallas kernels, ffn(): pl.pallas_call(ffn_kernel, out_shape=(jax.ShapeDtypeStruct((EXPERTS, NX,...  11.9 us
    unnamed x40, local copies, waits for them, and re-layouts  9.95 us
  transfers between devices with their start and end apart: 22, of which 11 were waited for; matrix products, arithmetic and copies ran while one was open for 10% of the time, Pallas kernels for 7%

commit v1 on v0

--- a/solution.py
+++ b/solution.py
@@ -86,34 +86,46 @@
     )(at, tokens, routes_t)
 
 
-WAYS = 6
-HALF = D // 2
+def round_kernel(gain_ref, gate_ref, up_ref, out_ref):
+    gain = gain_ref[...]
+    out_ref[:, 0] = (gate_ref[...] * gain[None]).astype(BF)
+    out_ref[:, 1] = (up_ref[...] * gain[None]).astype(BF)
+
+
+def round_both(gain, gate, up):
+    block = pl.BlockSpec((8, 64, 128), lambda i: (i, 0, 0))
+    return pl.pallas_call(
+        round_kernel,
+        out_shape=jax.ShapeDtypeStruct((EXPERTS, 2, 64, 128), BF),
+        grid=(EXPERTS // 8,),
+        in_specs=[pl.BlockSpec((64, 1), lambda i: (0, 0)), block, block],
+        out_specs=pl.BlockSpec((8, 2, 64, 128), lambda i: (i, 0, 0, 0)),
+        compiler_params=pltpu.CompilerParams(vmem_limit_bytes=16 << 20),
+        cost_estimate=pl.CostEstimate(flops=10**7, bytes_accessed=3 << 20, transcendentals=0),
+        name="round_both",
+    )(gain.reshape(64, 1), gate, up)
+
+
+WAYS = 10
+HALF = 16
 
 
 def ffn_kernel(block_ref, *refs):
-    source_refs = refs[: 3 * WAYS]
-    out_ref, *sample_refs = refs[3 * WAYS : 3 * WAYS + 4]
-    weight_ref, rows_ref, total_ref, hidden_ref, sems, sample_sems = refs[3 * WAYS + 4 :]
-    copies = []
-    for n in range(3):
-        own, left, right, near, far, other = source_refs[n * WAYS : (n + 1) * WAYS]
-        pieces = [
-            (own, weight_ref.at[n, 0]),
-            (left, weight_ref.at[n, 1]),
-            (right, weight_ref.at[n, 2]),
-            (near, weight_ref.at[n, 3, 0:HALF]),
-            (far, weight_ref.at[n, 3, HALF:D]),
-            (other, weight_ref.at[n, 4:8]),
-        ]
-        copies.append(
-            [
-                pltpu.make_async_copy(source, target, sems.at[n, i])
-                for i, (source, target) in enumerate(pieces)
-            ]
-        )
-    for group in zip(*copies):
-        for copy in group:
-            copy.start()
+    both_refs, single_refs = refs[:WAYS], refs[WAYS : 2 * WAYS]
+    out_ref, *sample_refs = refs[2 * WAYS : 2 * WAYS + 4]
+    weight_ref, rows_ref, total_ref, hidden_ref, sems, sample_sems = refs[2 * WAYS + 4 :]
+    places = []
+    for side in range(2):
+        at = 4 * side
+        places += [(at, slice(None)), (at + 1, slice(None)), (at + 2, slice(None))]
+        places += [(at + 3, slice(0, HALF)), (at + 3, slice(HALF, None))]
+    copies = {}
+    for i, (at, part) in enumerate(places):
+        for n in range(3):
+            source = both_refs[i].at[:, n] if n < 2 else single_refs[i]
+            target = weight_ref.at[n, at, part]
+            copies[n, i] = pltpu.make_async_copy(source, target, sems.at[n, i])
+            copies[n, i].start()
 
     rows_ref[0:TOK, :] = block_ref[:, :D]
     tail = block_ref[:, D:]
@@ -125,42 +137,36 @@
         )
         rows_ref[TOK : TOK + 64, j * 512 : (j + 1) * 512] = dot(pick, tail).astype(BF)
 
-    def wide(n, first):
-        return jnp.concatenate([weight_ref[n, first], weight_ref[n, first + 1]], axis=1)
-
-    def step(first, fresh):
-        gate = dot(rows_ref[...], wide(0, first))
-        up = dot(rows_ref[...], wide(1, first))
+    def wide(n, pair, part=slice(None)):
+        return jnp.concatenate(
+            [weight_ref[n, 2 * pair + i, part].reshape(-1, 128) for i in range(2)], axis=1
+        )
+
+    kept = []
+    for pair in range(4):
+        needed = [i for i, (at, _) in enumerate(places) if at // 2 == pair]
+        for n in range(2):
+            for i in needed:
+                copies[n, i].wait()
+        gate = dot(rows_ref[...], wide(0, pair))
+        up = dot(rows_ref[...], wide(1, pair))
         hidden_ref[...] = (gate / (1.0 + jnp.exp(-gate)) * up).astype(BF)
+        for i in needed:
+            copies[2, i].wait()
         for m in range(4):
-            part = slice(m * 512, (m + 1) * 512)
-            down = jnp.concatenate(
-                [weight_ref[2, first, part, :], weight_ref[2, first + 1, part, :]], axis=1
-            )
-            term = dot_t(hidden_ref[...], down)
-            if fresh:
-                total_ref[:, part] = term
+            term = dot_t(hidden_ref[...], wide(2, pair, slice(m * 8, (m + 1) * 8)))
+            if pair == 0:
+                total_ref[:, m * 512 : (m + 1) * 512] = term
             else:
-                total_ref[:, part] += term
-
-    def wait(first, last):
-        for i in range(first, last):
+                total_ref[:, m * 512 : (m + 1) * 512] += term
+        if pair == 0:
             for n in range(3):
-                copies[n][i].wait()
-
-    wait(0, 2)
-    kept = [
-        pltpu.make_async_copy(weight_ref.at[n, 0], sample_refs[n].at[0], sample_sems.at[n])
-        for n in range(3)
-    ]
-    for copy in kept:
-        copy.start()
-    step(0, True)
-    wait(2, WAYS)
-
-    @pl.loop(1, 4)
-    def _(pair):
-        step(2 * pair, False)
+                kept.append(
+                    pltpu.make_async_copy(
+                        weight_ref.at[n, 0], sample_refs[n], sample_sems.at[n]
+                    )
+                )
+                kept[n].start()
 
     tail = total_ref[TOK : TOK + 64, :].astype(BF)
     out_row = iota((TOK, 64), 0)
@@ -184,15 +190,15 @@
         copy.wait()
 
 
-def ffn(block, gate, up, down):
-    sample = jax.ShapeDtypeStruct((1, D, 128), BF)
+def ffn(block, both, single):
+    sample = jax.ShapeDtypeStruct((EXPERTS, 64, 128), BF)
     return pl.pallas_call(
         ffn_kernel,
         out_shape=(jax.ShapeDtypeStruct((EXPERTS, NX, 8, 640), BF), sample, sample, sample),
-        in_specs=[VMEM] + [HBM] * (3 * WAYS),
+        in_specs=[VMEM] + [HBM] * (2 * WAYS),
         out_specs=(VMEM, HBM, HBM, HBM),
         scratch_shapes=[
-            pltpu.VMEM((3, 8, D, 128), BF),
+            pltpu.VMEM((3, 8, EXPERTS, 64, 128), BF),
             pltpu.VMEM((TOK + 64, D), BF),
             pltpu.VMEM((TOK + 64, D), F32),
             pltpu.VMEM((TOK + 64, 256), BF),
@@ -204,7 +210,7 @@
             flops=6 * 320 * D * FF, bytes_accessed=16 << 20, transcendentals=320 * FF
         ),
         name="ffn",
-    )(block, *gate, *up, *down)
+    )(block, *both, *single)
 
 
 def combine_kernel(core_ref, routes_ref, weights_ref, back_ref, own_ref, other_ref):
@@ -259,6 +265,31 @@
     )(core, routes, route_weights, back)
 
 
+def shared_kernel(normed_ref, common_ref, terms_ref, *common_refs):
+    for n in range(3):
+        common_refs[n][...] = common_ref[:, n * 128 : (n + 1) * 128]
+    act = dot(normed_ref[...], common_ref[:, 0:256])
+    gate, up = act[:, 0:128], act[:, 128:256]
+    hidden = (gate / (1.0 + jnp.exp(-gate)) * up).astype(BF)
+    for n in range(NX * NC):
+        terms_ref[n] = dot_t(hidden, common_ref[n * 256 : (n + 1) * 256, 256:384]).astype(BF)
+
+
+def shared_expert(normed, common):
+    shape = jax.ShapeDtypeStruct((D, 128), BF)
+    return pl.pallas_call(
+        shared_kernel,
+        out_shape=(jax.ShapeDtypeStruct((NX * NC, TOK, 256), BF), shape, shape, shape),
+        in_specs=[VMEM] * 2,
+        out_specs=(VMEM,) * 4,
+        compiler_params=pltpu.CompilerParams(vmem_limit_bytes=24 << 20),
+        cost_estimate=pl.CostEstimate(
+            flops=6 * TOK * D * 128, bytes_accessed=6 << 20, transcendentals=TOK * 128
+        ),
+        name="shared_expert",
+    )(normed, common)
+
+
 def exchange(array, axes):
     return lax.all_to_all(array, axes, split_axis=0, concat_axis=0, tiled=True)
 
@@ -273,11 +304,6 @@
 
 def to_opposite(near):
     return shift(near[0][:HALF], "x", NX, 1), shift(near[1][HALF:], "x", NX, -1)
-
-
-def stacked(pieces):
-    own, left, right, near, far = pieces
-    return [own[None], left[None], right[None], jnp.concatenate([near, far])[None]]
 
 
 def layer(
@@ -295,7 +321,6 @@
     x, c = (lax.axis_index(a).astype(jnp.int32) for a in TP)
     at = (x * NC + c).reshape(1)
     core = c.reshape(1)
-    gain_rows = norm_gain[None, :, None]
 
     shared = jnp.concatenate(
         [
@@ -307,54 +332,40 @@
     )
     common = lax.all_gather(shared, FS, axis=0, tiled=True)
 
-    gate_in = (expert_gate * gain_rows).astype(BF)
-    gate_in, expert_up, expert_down = after(gate_in, expert_up, expert_down)
-    up_in = (expert_up * gain_rows).astype(BF)
+    both_in = round_both(norm_gain, expert_gate, expert_up)
+    both_in, expert_down = after(both_in, expert_down)
     down_in = expert_down.astype(BF)
     packed, normed = dispatch(tokens, routes.T, at)
 
-    gate_rows = exchange(gate_in, FS).reshape(D, 128)
-
-    up_in, gate_rows = after(up_in, gate_rows)
-    up_rows = exchange(up_in, FS).reshape(D, 128)
-    gate_near = to_neighbours(gate_rows)
-
-    down_in, up_rows, gate_near = after(down_in, up_rows, gate_near)
-    down_rows = exchange(down_in, FS).reshape(D, 128)
-    gate_far = to_opposite(gate_near)
-    up_near = to_neighbours(up_rows)
-
-    packed, down_rows, gate_far, up_near = after(packed, down_rows, gate_far, up_near)
+    both_rows = exchange(both_in, FS)
+
+    down_in, both_rows = after(down_in, both_rows)
+    down_rows = exchange(down_in, FS)
+    both_near = to_neighbours(both_rows)
+
+    packed, down_rows = after(packed, down_rows)
     block = exchange(packed.reshape(EXPERTS, 8, D + 512), FS).reshape(TOK, D + 512)
-    up_far = to_opposite(up_near)
+    both_far = to_opposite(both_near)
     down_near = to_neighbours(down_rows)
     down_far = to_opposite(down_near)
-    gate_all = [gate_rows, *gate_near, *gate_far]
-    up_all = [up_rows, *up_near, *up_far]
+    both_all = [both_rows, *both_near, *both_far]
     down_all = [down_rows, *down_near, *down_far]
-    both = shift(jnp.concatenate(stacked(gate_all) + stacked(up_all)), "c", NC, 1)
-    gate_all.append(both[:4])
-    up_all.append(both[4:])
-    down_all.append(shift(jnp.concatenate(stacked(down_all)), "c", NC, 1))
-
-    common_gate, common_up, common_down = jnp.split(common, 3, axis=1)
-    shared_hidden = (
-        jax.nn.silu(dot(normed, common_gate)) * dot(normed, common_up)
-    ).astype(BF)
-    shared_terms = dot_t(shared_hidden, common_down).astype(BF)
-    shared_terms = jnp.moveaxis(shared_terms.reshape(TOK, NX * NC, 256), 1, 0)
+    both_all += [shift(piece, "c", NC, 1) for piece in both_all]
+    down_all += [shift(piece, "c", NC, 1) for piece in down_all]
+
+    shared_terms, common_gate, common_up, common_down = shared_expert(normed, common)
     shared_sum = lax.psum_scatter(shared_terms, TP, scatter_dimension=0, tiled=True)[0]
 
-    results, sample_gate, sample_up, sample_down = ffn(block, gate_all, up_all, down_all)
+    results, sample_gate, sample_up, sample_down = ffn(block, both_all, down_all)
     back = exchange(results.reshape(EXPERTS * NX, 8, 640), ("z", "y", "x"))
     own, other = combine(back.reshape(EXPERTS * NX * 8, 640), routes, route_weights, core)
     other = shift(other, "c", NC, 1)
     layer_output = (own + other.astype(F32) + shared_sum.astype(F32)).astype(BF)
     return (
         layer_output,
-        sample_gate,
-        sample_up,
-        sample_down,
+        sample_gate.reshape(1, D, 128),
+        sample_up.reshape(1, D, 128),
+        sample_down.reshape(1, D, 128),
         common_gate,
         common_up,
         common_down,

time: 252 us -> 211 us (0.84)
  local copies, waits for them, and re-layouts: 23.4 us -> 8.01 us
  starting transfers between devices: 62 us -> 48.7 us
  other arithmetic: 12.5 us -> 3.19 us
  waiting for transfers between devices: 119 us -> 115 us
  Pallas kernels: 17.2 us -> 20.2 us
    ppermute x15 -> x19, starting transfers between devices: 20.4 us -> 12.2 us  [shift(): lax.ppermute(array, axis, [(i, (i + by) % size) for i in range(size)])]
    reduce_scatter x1, waiting for transfers between devices: 18.5 us -> 12.7 us  [layer(): lax.psum_scatter(shared_terms, TP, scatter_dimension=0, tiled=True)[0]]
    all_to_all x5 -> x4, starting transfers between devices: 41.5 us -> 36.3 us  [exchange(): return lax.all_to_all(array, axes, split_axis=0, concat_axis=0, tiled=True)]
    unnamed x40 -> x42, local copies, waits for them, and re-layouts: 9.95 us -> 5.08 us
    convert_element_type x2 -> x0, other arithmetic: 4.59 us -> none  [the longest x1 2.37 us: layer(): gate_in = (expert_gate * gain_rows).astype(BF)]
    slice x1 -> x0, local copies, waits for them, and re-layouts: 4.55 us -> none  [layer(): up_all.append(both[4:])]
    pallas_call x0 -> x2, Pallas kernels: none -> 4.51 us  [the longest x1 2.79 us: shared_expert(): pl.pallas_call(shared_kernel, out_shape=(jax.ShapeDtypeStruct((NX * NC, T...]
    concatenate x2 -> x0, other arithmetic: 3.76 us -> none  [the longest x1 2.89 us: layer(): down_all.append(shift(jnp.concatenate(stacked(down_all)), 'c', NC, 1))]
  transfers between devices with their start and end apart: 22 -> 25, of which waited for: 11 -> 12; matrix products, arithmetic and copies ran while one was open for 10% -> 2% of each run, Pallas kernels for 7% -> 9%
where the time goes in v1:
time: 211 us; the launch traced here: 209 us
  waiting for transfers between devices  115 us (55%)
  starting transfers between devices  48.7 us (23%)
  Pallas kernels  20.2 us (10%)
  between operations  14.3 us (7%)
  local copies, waits for them, and re-layouts  8.01 us (4%)
  other arithmetic  3.19 us (2%)
    all_to_all x4, waiting for transfers between devices, exchange(): return lax.all_to_all(array, axes, split_axis=0, concat_axis=0, tiled=True)  54.7 us
    all_to_all x4, starting transfers between devices, exchange(): return lax.all_to_all(array, axes, split_axis=0, concat_axis=0, tiled=True)  36.3 us
    ppermute x19, waiting for transfers between devices, shift(): lax.ppermute(array, axis, [(i, (i + by) % size) for i in range(size)])  32.2 us
    all_gather x1, waiting for transfers between devices, layer(): common = lax.all_gather(shared, FS, axis=0, tiled=True)  15.2 us
    reduce_scatter x1, waiting for transfers between devices, layer(): lax.psum_scatter(shared_terms, TP, scatter_dimension=0, tiled=True)[0]  12.7 us
    ppermute x19, starting transfers between devices, shift(): lax.ppermute(array, axis, [(i, (i + by) % size) for i in range(size)])  12.2 us
    pallas_call x1, Pallas kernels, ffn(): pl.pallas_call(ffn_kernel, out_shape=(jax.ShapeDtypeStruct((EXPERTS, NX,...  10.3 us
    unnamed x42, local copies, waits for them, and re-layouts  5.08 us
  transfers between devices with their start and end apart: 25, of which 12 were waited for; matrix products, arithmetic and copies ran while one was open for 2% of the time, Pallas kernels for 9%

profile of v1, /device:TPU:16, one launch (start us, length us, event | category | flops | bytes accessed | tf_op | source)
XLA Modules:
  0.0 209.3 jit_solution(16128119160664602569)
XLA Ops:
  7.9 1.2 copy-done.1
  9.1 1.2 copy-done.2
  10.4 1.7 round_both.1
  12.1 11.7 %all-to-all-start = ((bf16[32,2,64,128]{3,2,1,0:T(8,128)(2,1)}), bf16[32,2,64,128]{3,2,1,0:T(8,128)(2,1)S(1)}, u32[]{:S(2)}, u32[]{:S(2)}) async-start(bf16[32,2,64,128]{3,2,1,0:T(8,128)(2,1)} %round_both.1), calls=%async_computation | async-start | bytes 2097152 | tf_op jit(solution)/shard_map/all_to_all | solution.py:294
  24.7 27.2 %all-to-all-done.refs_0_ = bf16[32,2,64,128]{3,2,1,0:T(8,128)(2,1)S(1)} async-done(((bf16[32,2,64,128]{3,2,1,0:T(8,128)(2,1)}), bf16[32,2,64,128]{3,2,1,0:T(8,128)(2,1)S(1)}, u32[]{:S(2)}, u32[]{:S(2)}) %all-to-all-start) | async-done | bytes 1048608 | tf_op jit(solution)/shard_map/all_to_all | solution.py:294
  51.9 5.6 %all-to-all-start.1 = ((bf16[32,64,128]{2,1,0:T(8,128)(2,1)}), bf16[32,64,128]{2,1,0:T(8,128)(2,1)}, u32[]{:S(2)}, u32[]{:S(2)}) async-start(bf16[32,64,128]{2,1,0:T(8,128)(2,1)} %convert_element_type.24), calls=%async_computation.1 | async-start | bytes 1048576 | tf_op jit(solution)/shard_map/all_to_all | solution.py:294
  57.5 1.6 collective-permute-start
  59.1 1.7 collective-permute-start.1
  60.8 2.2 %dispatch.1 = (bf16[256,2560]{1,0:T(8,128)(2,1)}, bf16[256,2048]{1,0:T(8,128)(2,1)S(1)}) custom-call(s32[1]{0:T(128)} %bitcast.1.at_ref, bf16[256,2048]{1,0:T(8,128)(2,1)S(1)} %copy-done.4, s32[6,256]{1,0:T(8,128)S(1)} %bitcast.15), custom_call_target="tpu_custom_call" | custom-call | flops 1000000000 | bytes 4194304 | tf_op jit(solution)/shard_map/dispatch/pallas_call | solution.py:75
  63.0 10.3 %all-to-all-done.1.refs_10_ = bf16[32,64,128]{2,1,0:T(8,128)(2,1)} async-done(((bf16[32,64,128]{2,1,0:T(8,128)(2,1)}), bf16[32,64,128]{2,1,0:T(8,128)(2,1)}, u32[]{:S(2)}, u32[]{:S(2)}) %all-to-all-start.1) | async-done | bytes 524320 | tf_op jit(solution)/shard_map/all_to_all | solution.py:294
  73.3 5.8 %all-to-all-start.2 = ((bf16[32,8,2560]{2,1,0:T(8,128)(2,1)}), bf16[32,8,2560]{2,1,0:T(8,128)(2,1)}, u32[]{:S(2)}, u32[]{:S(2)}) async-start(bf16[32,8,2560]{2,1,0:T(8,128)(2,1)} %bitcast.4), calls=%async_computation.2 | async-start | bytes 2621440 | tf_op jit(solution)/shard_map/all_to_all | solution.py:294
  79.3 1.6 collective-permute-start.9
  81.6 1.8 collective-permute-start.10
  83.4 1.1 slice.16
  84.9 1.1 slice.17
  86.0 9.6 %collective-permute-done.9.refs_11_ = bf16[32,64,128]{2,1,0:T(8,128)(2,1)S(1)} collective-permute-done((bf16[32,64,128]{2,1,0:T(8,128)(2,1)}, bf16[32,64,128]{2,1,0:T(8,128)(2,1)S(1)}, u32[]{:S(2)}, u32[]{:S(2)}) %collective-permute-start.9) | collective-permute-done | bytes 524320 | tf_op jit(solution)/shard_map/ppermute | solution.py:39
  95.6 1.5 collective-permute-start.3
  98.2 8.6 %collective-permute-done.2.refs_3_ = bf16[16,2,64,128]{3,2,1,0:T(8,128)(2,1)S(1)} collective-permute-done((bf16[16,2,64,128]{3,2,1,0:T(8,128)(2,1)S(1)}, bf16[16,2,64,128]{3,2,1,0:T(8,128)(2,1)S(1)}, u32[]{:S(2)}, u32[]{:S(2)}) %collective-permute-start.2) | collective-permute-done | bytes 524320 | tf_op jit(solution)/shard_map/ppermute | solution.py:39
  106.8 1.7 collective-permute-done.3.refs_4_
  108.5 3.3 %collective-permute-done.11.refs_13_ = bf16[16,64,128]{2,1,0:T(8,128)(2,1)S(1)} collective-permute-done((bf16[16,64,128]{2,1,0:T(8,128)(2,1)S(1)}, bf16[16,64,128]{2,1,0:T(8,128)(2,1)S(1)}, u32[]{:S(2)}, u32[]{:S(2)}) %collective-permute-start.11) | collective-permute-done | bytes 262176 | tf_op jit(solution)/shard_map/ppermute | solution.py:39
  111.9 1.5 collective-permute-start.12
  113.4 6.3 %collective-permute-done.12.refs_14_ = bf16[16,64,128]{2,1,0:T(8,128)(2,1)S(1)} collective-permute-done((bf16[16,64,128]{2,1,0:T(8,128)(2,1)S(1)}, bf16[16,64,128]{2,1,0:T(8,128)(2,1)S(1)}, u32[]{:S(2)}, u32[]{:S(2)}) %collective-permute-start.12) | collective-permute-done | bytes 262176 | tf_op jit(solution)/shard_map/ppermute | solution.py:39
  121.4 1.7 collective-permute-done.17.refs_19_
  124.1 10.3 %ffn.1 = (bf16[32,4,8,640]{3,2,1,0:T(8,128)(2,1)}, bf16[32,64,128]{2,1,0:T(8,128)(2,1)}, bf16[32,64,128]{2,1,0:T(8,128)(2,1)}, bf16[32,64,128]{2,1,0:T(8,128)(2,1)}) custom-call(bf16[256,2560]{1,0:T(8,128)(2,1)} %bitcast.5.block_ref, bf16[32,2,64,128]{3,2,1,0:T(8,128)(2,1)} %copy-done.6, bf16[32,2,64,128]{3,2,1,0:T(8,128)(2,1)} %collective-permute-done.refs_1_, ...), custom_call_target="tpu_custom_call" | custom-call | flops 4026531840 | bytes 16777216 | tf_op jit(solution)/shard_map/ffn/pallas_call | solution.py:195
  134.5 13.2 %all-to-all-start.3 = ((bf16[128,8,640]{2,1,0:T(8,128)(2,1)}), bf16[128,8,640]{2,1,0:T(8,128)(2,1)S(1)}, u32[]{:S(2)}, u32[]{:S(2)}) async-start(bf16[128,8,640]{2,1,0:T(8,128)(2,1)} %bitcast.16), calls=%async_computation.3 | async-start | bytes 2621440 | tf_op jit(solution)/shard_map/all_to_all | solution.py:294
  148.0 15.2 %all-gather.2.cloned.1.call-done.common_ref = bf16[2048,384]{1,0:T(8,128)(2,1)} async-done(((bf16[64,384]{1,0:T(8,128)(2,1)}), bf16[2048,384]{1,0:T(8,128)(2,1)}) %all-gather.2.cloned.1.call-update) | async-done | bytes 1572880 | tf_op jit(solution)/shard_map/all_gather | solution.py:333
  163.2 1.4 copy-done
  164.6 2.8 %shared_expert.1 = (bf16[8,256,256]{2,1,0:T(8,128)(2,1)}, bf16[2048,128]{1,0:T(8,128)(2,1)}, bf16[2048,128]{1,0:T(8,128)(2,1)}, bf16[2048,128]{1,0:T(8,128)(2,1)}) custom-call(bf16[256,2048]{1,0:T(8,128)(2,1)S(1)} %get-tuple-element.35.normed_ref, bf16[2048,384]{1,0:T(8,128)(2,1)S(1)} %copy-done), custom_call_target="tpu_custom_call" | custom-call | flops 402653184 | bytes 6291456 | tf_op jit(solution)/shard_map/shared_expert/pallas_call | solution.py:280
  167.7 17.3 %all-to-all-done.3 = bf16[128,8,640]{2,1,0:T(8,128)(2,1)S(1)} async-done(((bf16[128,8,640]{2,1,0:T(8,128)(2,1)}), bf16[128,8,640]{2,1,0:T(8,128)(2,1)S(1)}, u32[]{:S(2)}, u32[]{:S(2)}) %all-to-all-start.3) | async-done | bytes 1310752 | tf_op jit(solution)/shard_map/all_to_all | solution.py:294
  185.0 3.1 %combine.1 = (f32[256,256]{1,0:T(8,128)S(1)}, bf16[256,256]{1,0:T(8,128)(2,1)S(1)}) custom-call(s32[1]{0:T(128)} %bitcast.core_ref, s32[256,6]{1,0:T(8,128)S(1)} %copy.18.routes_ref, f32[256,6]{1,0:T(8,128)S(1)} %copy.19.weights_ref, bf16[1024,640]{1,0:T(8,128)(2,1)S(1)} %bitcast.14), custom_call_target="tpu_custom_call" | custom-call | flops 1000000000 | bytes 4194304 | tf_op jit(solution)/shard_map/combine/pallas_call | solution.py:254
  188.2 12.7 %reduce-scatter.2.cloned.1.call-done = bf16[1,256,256]{2,1,0:T(8,128)(2,1)} async-done(((bf16[8,256,256]{2,1,0:T(8,128)(2,1)}), bf16[1,256,256]{2,1,0:T(8,128)(2,1)}) %reduce-scatter.2.cloned.1.call-update) | async-done | bytes 131088 | tf_op jit(solution)/shard_map/reduce_scatter | solution.py:357
  200.9 1.6 fusion
  (77 shorter events, 7.2 us)
Async XLA Ops:
  12.1 39.8 %all-to-all-start = ((bf16[32,2,64,128]{3,2,1,0:T(8,128)(2,1)}), bf16[32,2,64,128]{3,2,1,0:T(8,128)(2,1)S(1)}, u32[]{:S(2)}, u32[]{:S(2)}) async-start(bf16[32,2,64,128]{3,2,1,0:T(8,128)(2,1)} %round_both.1), calls=%async_computation | async-start | bytes 2097152 | tf_op jit(solution)/shard_map/all_to_all | solution.py:294
  23.8 37.0 %copy-start.3 = (s32[256,6]{0,1:T(8,128)S(1)}, s32[256,6]{0,1:T(8,128)}, u32[]{:S(2)}) copy-start(s32[256,6]{0,1:T(8,128)} %param.11) | copy-start | bytes 18436
  23.8 37.0 %copy-start.4 = (bf16[256,2048]{1,0:T(8,128)(2,1)S(1)}, bf16[256,2048]{1,0:T(8,128)(2,1)}, u32[]{:S(2)}) copy-start(bf16[256,2048]{1,0:T(8,128)(2,1)} %tokens_ref.1) | copy-start | bytes 3145732
  51.9 27.3 %copy-start.6 = (bf16[32,2,64,128]{3,2,1,0:T(8,128)(2,1)}, bf16[32,2,64,128]{3,2,1,0:T(8,128)(2,1)S(1)}, u32[]{:S(2)}) copy-start(bf16[32,2,64,128]{3,2,1,0:T(8,128)(2,1)S(1)} %all-to-all-done.refs_0_) | copy-start | bytes 3145732
  51.9 21.5 %all-to-all-start.1 = ((bf16[32,64,128]{2,1,0:T(8,128)(2,1)}), bf16[32,64,128]{2,1,0:T(8,128)(2,1)}, u32[]{:S(2)}, u32[]{:S(2)}) async-start(bf16[32,64,128]{2,1,0:T(8,128)(2,1)} %convert_element_type.24), calls=%async_computation.1 | async-start | bytes 1048576 | tf_op jit(solution)/shard_map/all_to_all | solution.py:294
  57.5 25.9 %collective-permute-start = (bf16[32,2,64,128]{3,2,1,0:T(8,128)(2,1)S(1)}, bf16[32,2,64,128]{3,2,1,0:T(8,128)(2,1)}, u32[]{:S(2)}, u32[]{:S(2)}) collective-permute-start(bf16[32,2,64,128]{3,2,1,0:T(8,128)(2,1)S(1)} %all-to-all-done.refs_0_), channel_id=1, source_target_pairs={{0,2},{2,4},{4,6},{6,0},{1,3},{3,5},{5,7},{7,1},{8,10},{10,12},{12... | collective-permute-start | bytes 3145736 | tf_op jit(solution)/shard_map/ppermute | solution.py:39
  59.1 25.4 %collective-permute-start.1 = (bf16[32,2,64,128]{3,2,1,0:T(8,128)(2,1)S(1)}, bf16[32,2,64,128]{3,2,1,0:T(8,128)(2,1)}, u32[]{:S(2)}, u32[]{:S(2)}) collective-permute-start(bf16[32,2,64,128]{3,2,1,0:T(8,128)(2,1)S(1)} %all-to-all-done.refs_0_), channel_id=1, source_target_pairs={{0,6},{2,0},{4,2},{6,4},{1,7},{3,1},{5,3},{7,5},{8,14},{10,8},{12,... | collective-permute-start | bytes 3145736 | tf_op jit(solution)/shard_map/ppermute | solution.py:39
  73.3 50.8 %all-to-all-start.2 = ((bf16[32,8,2560]{2,1,0:T(8,128)(2,1)}), bf16[32,8,2560]{2,1,0:T(8,128)(2,1)}, u32[]{:S(2)}, u32[]{:S(2)}) async-start(bf16[32,8,2560]{2,1,0:T(8,128)(2,1)} %bitcast.4), calls=%async_computation.2 | async-start | bytes 2621440 | tf_op jit(solution)/shard_map/all_to_all | solution.py:294
  79.1 84.1 %all-gather.2.cloned.1.call-start = ((), (), s32[]{:S(2)}) async-start(), calls=%async_computation.5 | async-start | bytes 1622016 | tf_op jit(solution)/shard_map/all_gather | solution.py:333
  79.2 18.0 %collective-permute-start.4 = (bf16[32,2,64,128]{3,2,1,0:T(8,128)(2,1)S(1)}, bf16[32,2,64,128]{3,2,1,0:T(8,128)(2,1)}, u32[]{:S(2)}, u32[]{:S(2)}) collective-permute-start(bf16[32,2,64,128]{3,2,1,0:T(8,128)(2,1)S(1)} %all-to-all-done.refs_0_), channel_id=1, source_target_pairs={{0,1},{1,0},{2,3},{3,2},{4,5},{5,4},{6,7},{7,6},{8,9},{9,8},{10,11... | collective-permute-start | bytes 3145736 | tf_op jit(solution)/shard_map/ppermute | solution.py:39
  79.3 16.3 %collective-permute-start.9 = (bf16[32,64,128]{2,1,0:T(8,128)(2,1)}, bf16[32,64,128]{2,1,0:T(8,128)(2,1)S(1)}, u32[]{:S(2)}, u32[]{:S(2)}) collective-permute-start(bf16[32,64,128]{2,1,0:T(8,128)(2,1)} %all-to-all-done.1.refs_10_), channel_id=1, source_target_pairs={{0,2},{2,4},{4,6},{6,0},{1,3},{3,5},{5,7},{7,1},{8,10},{10,12},{12... | collective-permute-start | bytes 1572872 | tf_op jit(solution)/shard_map/ppermute | solution.py:39
  81.6 16.1 %collective-permute-start.10 = (bf16[32,64,128]{2,1,0:T(8,128)(2,1)}, bf16[32,64,128]{2,1,0:T(8,128)(2,1)S(1)}, u32[]{:S(2)}, u32[]{:S(2)}) collective-permute-start(bf16[32,64,128]{2,1,0:T(8,128)(2,1)} %all-to-all-done.1.refs_10_), channel_id=1, source_target_pairs={{0,6},{2,0},{4,2},{6,4},{1,7},{3,1},{5,3},{7,5},{8,14},{10,8},{12,... | collective-permute-start | bytes 1572872 | tf_op jit(solution)/shard_map/ppermute | solution.py:39
  83.4 14.3 %collective-permute-start.13 = (bf16[32,64,128]{2,1,0:T(8,128)(2,1)}, bf16[32,64,128]{2,1,0:T(8,128)(2,1)S(1)}, u32[]{:S(2)}, u32[]{:S(2)}) collective-permute-start(bf16[32,64,128]{2,1,0:T(8,128)(2,1)} %all-to-all-done.1.refs_10_), channel_id=1, source_target_pairs={{0,1},{1,0},{2,3},{3,2},{4,5},{5,4},{6,7},{7,6},{8,9},{9,8},{10,11... | collective-permute-start | bytes 1572872 | tf_op jit(solution)/shard_map/ppermute | solution.py:39
  84.5 22.3 %collective-permute-start.2 = (bf16[16,2,64,128]{3,2,1,0:T(8,128)(2,1)S(1)}, bf16[16,2,64,128]{3,2,1,0:T(8,128)(2,1)S(1)}, u32[]{:S(2)}, u32[]{:S(2)}) collective-permute-start(bf16[16,2,64,128]{3,2,1,0:T(8,128)(2,1)S(1)} %slice.16), channel_id=1, source_target_pairs={{0,2},{2,4},{4,6},{6,0},{1,3},{3,5},{5,7},{7,1},{8,10},{10,12},{12... | collective-permute-start | bytes 1572872 | tf_op jit(solution)/shard_map/ppermute | solution.py:39
  95.6 28.6 %copy-start.7 = (bf16[32,64,128]{2,1,0:T(8,128)(2,1)}, bf16[32,64,128]{2,1,0:T(8,128)(2,1)S(1)}, u32[]{:S(2)}) copy-start(bf16[32,64,128]{2,1,0:T(8,128)(2,1)S(1)} %collective-permute-done.9.refs_11_) | copy-start | bytes 1572868
  95.6 12.9 %collective-permute-start.3 = (bf16[16,2,64,128]{3,2,1,0:T(8,128)(2,1)S(1)}, bf16[16,2,64,128]{3,2,1,0:T(8,128)(2,1)S(1)}, u32[]{:S(2)}, u32[]{:S(2)}) collective-permute-start(bf16[16,2,64,128]{3,2,1,0:T(8,128)(2,1)S(1)} %slice.17), channel_id=1, source_target_pairs={{0,6},{2,0},{4,2},{6,4},{1,7},{3,1},{5,3},{7,5},{8,14},{10,8},{12,... | collective-permute-start | bytes 1572872 | tf_op jit(solution)/shard_map/ppermute | solution.py:39
  97.1 14.7 %collective-permute-start.11 = (bf16[16,64,128]{2,1,0:T(8,128)(2,1)S(1)}, bf16[16,64,128]{2,1,0:T(8,128)(2,1)S(1)}, u32[]{:S(2)}, u32[]{:S(2)}) collective-permute-start(bf16[16,64,128]{2,1,0:T(8,128)(2,1)S(1)} %slice.18), channel_id=1, source_target_pairs={{0,2},{2,4},{4,6},{6,0},{1,3},{3,5},{5,7},{7,1},{8,10},{10,12},{12... | collective-permute-start | bytes 786440 | tf_op jit(solution)/shard_map/ppermute | solution.py:39
  97.7 25.5 %copy-start.8 = (bf16[32,64,128]{2,1,0:T(8,128)(2,1)}, bf16[32,64,128]{2,1,0:T(8,128)(2,1)S(1)}, u32[]{:S(2)}) copy-start(bf16[32,64,128]{2,1,0:T(8,128)(2,1)S(1)} %collective-permute-done.10.refs_12_) | copy-start | bytes 1572868
  97.7 22.0 %collective-permute-start.14 = (bf16[32,64,128]{2,1,0:T(8,128)(2,1)S(1)}, bf16[32,64,128]{2,1,0:T(8,128)(2,1)S(1)}, u32[]{:S(2)}, u32[]{:S(2)}) collective-permute-start(bf16[32,64,128]{2,1,0:T(8,128)(2,1)S(1)} %collective-permute-done.9.refs_11_), channel_id=1, source_target_pairs={{0,1},{1,0},{2,3},{3,2},{4,5},{5,4},{6,7},{7,6},{8,9},{9,8},{10,11... | collective-permute-start | bytes 1572872 | tf_op jit(solution)/shard_map/ppermute | solution.py:39
  97.7 25.5 %copy-start.14 = (bf16[32,64,128]{2,1,0:T(8,128)(2,1)}, bf16[32,64,128]{2,1,0:T(8,128)(2,1)S(1)}, u32[]{:S(2)}) copy-start(bf16[32,64,128]{2,1,0:T(8,128)(2,1)S(1)} %collective-permute-done.13.refs_15_) | copy-start | bytes 1572868
  97.7 22.5 %collective-permute-start.15 = (bf16[32,64,128]{2,1,0:T(8,128)(2,1)S(1)}, bf16[32,64,128]{2,1,0:T(8,128)(2,1)S(1)}, u32[]{:S(2)}, u32[]{:S(2)}) collective-permute-start(bf16[32,64,128]{2,1,0:T(8,128)(2,1)S(1)} %collective-permute-done.10.refs_12_), channel_id=1, source_target_pairs={{0,1},{1,0},{2,3},{3,2},{4,5},{5,4},{6,7},{7,6},{8,9},{9,8},{10,11... | collective-permute-start | bytes 1572872 | tf_op jit(solution)/shard_map/ppermute | solution.py:39
  106.8 16.4 %collective-permute-start.5 = (bf16[32,2,64,128]{3,2,1,0:T(8,128)(2,1)}, bf16[32,2,64,128]{3,2,1,0:T(8,128)(2,1)}, u32[]{:S(2)}, u32[]{:S(2)}) collective-permute-start(bf16[32,2,64,128]{3,2,1,0:T(8,128)(2,1)} %collective-permute-done.refs_1_), channel_id=1, source_target_pairs={{0,1},{1,0},{2,3},{3,2},{4,5},{5,4},{6,7},{7,6},{8,9},{9,8},{10,11... | collective-permute-start | bytes 3145736 | tf_op jit(solution)/shard_map/ppermute | solution.py:39
  108.5 14.7 %copy-start.15 = (bf16[16,2,64,128]{3,2,1,0:T(8,128)(2,1)}, bf16[16,2,64,128]{3,2,1,0:T(8,128)(2,1)S(1)}, u32[]{:S(2)}) copy-start(bf16[16,2,64,128]{3,2,1,0:T(8,128)(2,1)S(1)} %collective-permute-done.3.refs_4_) | copy-start | bytes 1572868
  108.5 15.6 %collective-permute-start.6 = (bf16[32,2,64,128]{3,2,1,0:T(8,128)(2,1)}, bf16[32,2,64,128]{3,2,1,0:T(8,128)(2,1)}, u32[]{:S(2)}, u32[]{:S(2)}) collective-permute-start(bf16[32,2,64,128]{3,2,1,0:T(8,128)(2,1)} %collective-permute-done.1.refs_2_), channel_id=1, source_target_pairs={{0,1},{1,0},{2,3},{3,2},{4,5},{5,4},{6,7},{7,6},{8,9},{9,8},{10,11... | collective-permute-start | bytes 3145736 | tf_op jit(solution)/shard_map/ppermute | solution.py:39
  111.9 7.9 %collective-permute-start.12 = (bf16[16,64,128]{2,1,0:T(8,128)(2,1)S(1)}, bf16[16,64,128]{2,1,0:T(8,128)(2,1)S(1)}, u32[]{:S(2)}, u32[]{:S(2)}) collective-permute-start(bf16[16,64,128]{2,1,0:T(8,128)(2,1)S(1)} %slice.19), channel_id=1, source_target_pairs={{0,6},{2,0},{4,2},{6,4},{1,7},{3,1},{5,3},{7,5},{8,14},{10,8},{12,... | collective-permute-start | bytes 786440 | tf_op jit(solution)/shard_map/ppermute | solution.py:39
  119.7 1.5 collective-permute-start.16
  119.8 3.4 %collective-permute-start.7 = (bf16[16,2,64,128]{3,2,1,0:T(8,128)(2,1)S(1)}, bf16[16,2,64,128]{3,2,1,0:T(8,128)(2,1)S(1)}, u32[]{:S(2)}, u32[]{:S(2)}) collective-permute-start(bf16[16,2,64,128]{3,2,1,0:T(8,128)(2,1)S(1)} %collective-permute-done.2.refs_3_), channel_id=1, source_target_pairs={{0,1},{1,0},{2,3},{3,2},{4,5},{5,4},{6,7},{7,6},{8,9},{9,8},{10,11... | collective-permute-start | bytes 1572872 | tf_op jit(solution)/shard_map/ppermute | solution.py:39
  120.3 2.9 %collective-permute-start.8 = (bf16[16,2,64,128]{3,2,1,0:T(8,128)(2,1)S(1)}, bf16[16,2,64,128]{3,2,1,0:T(8,128)(2,1)S(1)}, u32[]{:S(2)}, u32[]{:S(2)}) collective-permute-start(bf16[16,2,64,128]{3,2,1,0:T(8,128)(2,1)S(1)} %collective-permute-done.3.refs_4_), channel_id=1, source_target_pairs={{0,1},{1,0},{2,3},{3,2},{4,5},{5,4},{6,7},{7,6},{8,9},{9,8},{10,11... | collective-permute-start | bytes 1572872 | tf_op jit(solution)/shard_map/ppermute | solution.py:39
  121.3 1.9 collective-permute-start.17
  134.5 50.5 %all-to-all-start.3 = ((bf16[128,8,640]{2,1,0:T(8,128)(2,1)}), bf16[128,8,640]{2,1,0:T(8,128)(2,1)S(1)}, u32[]{:S(2)}, u32[]{:S(2)}) async-start(bf16[128,8,640]{2,1,0:T(8,128)(2,1)} %bitcast.16), calls=%async_computation.3 | async-start | bytes 2621440 | tf_op jit(solution)/shard_map/all_to_all | solution.py:294
  147.7 53.2 %reduce-scatter.2.cloned.1.call-start = ((), (), s32[]{:S(2)}) async-start(), calls=%async_computation.6 | async-start | bytes 1179648 | tf_op jit(solution)/shard_map/reduce_scatter | solution.py:357
  188.1 12.8 %collective-permute-start.18 = (bf16[256,256]{1,0:T(8,128)(2,1)S(1)}, bf16[256,256]{1,0:T(8,128)(2,1)S(1)}, u32[]{:S(2)}, u32[]{:S(2)}) collective-permute-start(bf16[256,256]{1,0:T(8,128)(2,1)S(1)} %get-tuple-element.34), channel_id=1, source_target_pairs={{0,1},{1,0},{2,3},{3,2},{4,5},{5,4},{6,7},{7,6},{8,9},{9,8},{10,11... | collective-permute-start | bytes 393224 | tf_op jit(solution)/shard_map/ppermute | solution.py:39
  (13 other events, 56.8 us)
Sparse Core Ops, SparseCore 0:
  83.1 80.0 all-gather.1
  167.5 33.3 reduce-scatter.1

commit v2 on v1

--- a/solution.py
+++ b/solution.py
@@ -87,7 +87,8 @@
 
 
 def round_kernel(gain_ref, gate_ref, up_ref, out_ref):
-    gain = gain_ref[...]
+    diagonal = iota((64, 64), 0) == iota((64, 64), 1)
+    gain = jnp.sum(jnp.where(diagonal, gain_ref[...], 0.0), axis=1, keepdims=True)
     out_ref[:, 0] = (gate_ref[...] * gain[None]).astype(BF)
     out_ref[:, 1] = (up_ref[...] * gain[None]).astype(BF)
 
@@ -98,12 +99,12 @@
         round_kernel,
         out_shape=jax.ShapeDtypeStruct((EXPERTS, 2, 64, 128), BF),
         grid=(EXPERTS // 8,),
-        in_specs=[pl.BlockSpec((64, 1), lambda i: (0, 0)), block, block],
+        in_specs=[pl.BlockSpec((1, 64), lambda i: (0, 0)), block, block],
         out_specs=pl.BlockSpec((8, 2, 64, 128), lambda i: (i, 0, 0, 0)),
-        compiler_params=pltpu.CompilerParams(vmem_limit_bytes=16 << 20),
+        compiler_params=pltpu.CompilerParams(vmem_limit_bytes=60 << 20),
         cost_estimate=pl.CostEstimate(flops=10**7, bytes_accessed=3 << 20, transcendentals=0),
         name="round_both",
-    )(gain.reshape(64, 1), gate, up)
+    )(gain.reshape(1, 64), gate, up)
 
 
 WAYS = 10
@@ -113,7 +114,7 @@
 def ffn_kernel(block_ref, *refs):
     both_refs, single_refs = refs[:WAYS], refs[WAYS : 2 * WAYS]
     out_ref, *sample_refs = refs[2 * WAYS : 2 * WAYS + 4]
-    weight_ref, rows_ref, total_ref, hidden_ref, sems, sample_sems = refs[2 * WAYS + 4 :]
+    weight_ref, rows_ref, hidden_ref, sems, sample_sems = refs[2 * WAYS + 4 :]
     places = []
     for side in range(2):
         at = 4 * side
@@ -137,55 +138,50 @@
         )
         rows_ref[TOK : TOK + 64, j * 512 : (j + 1) * 512] = dot(pick, tail).astype(BF)
 
-    def wide(n, pair, part=slice(None)):
+    def wide(n, blocks, part=slice(None)):
         return jnp.concatenate(
-            [weight_ref[n, 2 * pair + i, part].reshape(-1, 128) for i in range(2)], axis=1
+            [weight_ref[n, i, part].reshape(-1, 128) for i in blocks], axis=1
         )
 
     kept = []
+
+    def keep(n):
+        kept.append(
+            pltpu.make_async_copy(weight_ref.at[n, 0], sample_refs[n], sample_sems.at[n])
+        )
+        kept[n].start()
+
     for pair in range(4):
-        needed = [i for i, (at, _) in enumerate(places) if at // 2 == pair]
-        for n in range(2):
-            for i in needed:
-                copies[n, i].wait()
-        gate = dot(rows_ref[...], wide(0, pair))
-        up = dot(rows_ref[...], wide(1, pair))
-        hidden_ref[...] = (gate / (1.0 + jnp.exp(-gate)) * up).astype(BF)
-        for i in needed:
-            copies[2, i].wait()
-        for m in range(4):
-            term = dot_t(hidden_ref[...], wide(2, pair, slice(m * 8, (m + 1) * 8)))
-            if pair == 0:
-                total_ref[:, m * 512 : (m + 1) * 512] = term
-            else:
-                total_ref[:, m * 512 : (m + 1) * 512] += term
+        for i, (at, _) in enumerate(places):
+            if at // 2 == pair:
+                copies[0, i].wait()
+                copies[1, i].wait()
+        blocks = (2 * pair, 2 * pair + 1)
+        gate = dot(rows_ref[...], wide(0, blocks))
+        up = dot(rows_ref[...], wide(1, blocks))
+        hidden = gate / (1.0 + jnp.exp(-gate)) * up
+        hidden_ref[:, pair * 256 : (pair + 1) * 256] = hidden.astype(BF)
         if pair == 0:
-            for n in range(3):
-                kept.append(
-                    pltpu.make_async_copy(
-                        weight_ref.at[n, 0], sample_refs[n], sample_sems.at[n]
-                    )
-                )
-                kept[n].start()
-
-    tail = total_ref[TOK : TOK + 64, :].astype(BF)
+            keep(0)
+            keep(1)
+
+    for i in range(WAYS):
+        copies[2, i].wait()
+    keep(2)
     out_row = iota((TOK, 64), 0)
     in_row = iota((TOK, 64), 1)
-    packed = jnp.zeros((TOK, 512), F32)
-    for j in range(4):
-        pick = flag(
-            jnp.logical_and(in_row // 2 == out_row // 8, out_row % 8 == 2 * j + in_row % 2)
-        )
-        piece = jnp.concatenate(
-            [tail[:, x * 512 + j * 128 : x * 512 + (j + 1) * 128] for x in range(NX)], axis=1
-        )
-        packed = packed + dot(pick, piece)
+    picks = [
+        flag(jnp.logical_and(in_row // 2 == out_row // 8, out_row % 8 == 2 * j + in_row % 2))
+        for j in range(4)
+    ]
     for x in range(NX):
-        body = total_ref[0:TOK, x * 512 : (x + 1) * 512]
-        out_ref[:, x, :, 0:512] = body.astype(BF).reshape(EXPERTS, 8, 512)
-        out_ref[:, x, :, 512:640] = (
-            packed[:, x * 128 : (x + 1) * 128].astype(BF).reshape(EXPERTS, 8, 128)
-        )
+        result = dot_t(hidden_ref[...], wide(2, range(8), slice(x * 8, (x + 1) * 8)))
+        result = result.astype(BF)
+        packed = jnp.zeros((TOK, 128), F32)
+        for j in range(4):
+            packed = packed + dot(picks[j], result[TOK:, j * 128 : (j + 1) * 128])
+        out_ref[:, x, :, 0:512] = result[:TOK].reshape(EXPERTS, 8, 512)
+        out_ref[:, x, :, 512:640] = packed.astype(BF).reshape(EXPERTS, 8, 128)
     for copy in kept:
         copy.wait()
 
@@ -200,8 +196,7 @@
         scratch_shapes=[
             pltpu.VMEM((3, 8, EXPERTS, 64, 128), BF),
             pltpu.VMEM((TOK + 64, D), BF),
-            pltpu.VMEM((TOK + 64, D), F32),
-            pltpu.VMEM((TOK + 64, 256), BF),
+            pltpu.VMEM((TOK + 64, FF), BF),
             pltpu.SemaphoreType.DMA((3, WAYS)),
             pltpu.SemaphoreType.DMA((3,)),
         ],
@@ -213,7 +208,7 @@
     )(block, *both, *single)
 
 
-def combine_kernel(core_ref, routes_ref, weights_ref, back_ref, own_ref, other_ref):
+def mixing_kernel(core_ref, routes_ref, weights_ref, first_ref, last_ref):
     core = core_ref[0]
     expert = iota((TOK, EXPERTS), 1)
     member = jnp.zeros((TOK, EXPERTS), F32)
@@ -225,69 +220,115 @@
     earlier = flag(iota((TOK, TOK), 1) < iota((TOK, TOK), 0))
     position = dot(earlier, member.astype(BF))
     slot = jnp.where(member > 0.0, position, -1.0).astype(BF)
-    high = weight.astype(BF)
-    low = (weight - high.astype(F32)).astype(BF)
-    lanes = EXPERTS * NX * 8
-    spread = flag(iota((EXPERTS, lanes), 1) // (NX * 8) == iota((EXPERTS, lanes), 0))
+    spread = flag(iota((EXPERTS, LANES), 1) // (NX * 8) == iota((EXPERTS, LANES), 0))
     slots = dot(slot, spread)
-    lane = iota((TOK, lanes), 1)
+    wide = dot(weight.astype(BF), spread)
+    lane = iota((TOK, LANES), 1)
     start = ((lane // 8) % NX * NC + core) * SHARE
     first = slots == (start + lane % 8).astype(F32)
     last = slots == (start + 8 + lane % 2).astype(F32)
-    body = back_ref[:, 0:512]
+    first_ref[...] = jnp.where(first, wide, 0.0).astype(BF)
+    last_ref[...] = jnp.where(last, wide, 0.0).astype(BF)
+
+
+LANES = EXPERTS * NX * 8
+
+
+def mixing(routes, route_weights, core):
+    shape = jax.ShapeDtypeStruct((TOK, LANES), BF)
+    return pl.pallas_call(
+        mixing_kernel,
+        out_shape=(shape, shape),
+        in_specs=[SMEM, VMEM, VMEM],
+        out_specs=(VMEM, VMEM),
+        compiler_params=pltpu.CompilerParams(vmem_limit_bytes=24 << 20),
+        cost_estimate=pl.CostEstimate(flops=10**9, bytes_accessed=4 << 20, transcendentals=0),
+        name="mixing",
+    )(core, routes, route_weights)
+
+
+def combine_kernel(
+    core_ref, back_ref, first_hbm, last_hbm, own_ref, other_ref, first_ref, last_ref, sems
+):
+    core = core_ref[0]
+    copies = [
+        pltpu.make_async_copy(source, target, sems.at[i])
+        for i, (source, target) in enumerate(
+            ((first_hbm, first_ref), (last_hbm, last_ref))
+        )
+    ]
+    for copy in copies:
+        copy.start()
+    copies[0].wait()
+    total = dot(first_ref[...], back_ref[:, 0:512])
     tail = back_ref[:, 512:640]
-    total = jnp.zeros((TOK, 512), F32)
-    pieces = [jnp.zeros((TOK, 128), F32)] * 4
-    for part in (high, low):
-        wide = dot(part, spread)
-        total = total + dot(jnp.where(first, wide, 0.0).astype(BF), body)
-        for j in range(4):
-            mine = jnp.logical_and(last, lane % 8 // 2 == j)
-            pieces[j] = pieces[j] + dot(jnp.where(mine, wide, 0.0).astype(BF), tail)
+    lane = iota((TOK, LANES), 1)
+    copies[1].wait()
+    last = last_ref[...]
+    pieces = []
+    for j in range(4):
+        mine = lane % 8 // 2 == j
+        pieces.append(dot(jnp.where(mine, last, jnp.zeros_like(last)), tail))
     total = total + jnp.concatenate(pieces, axis=1)
     left, right = total[:, :256], total[:, 256:]
     own_ref[...] = jnp.where(core == 0, left, right)
     other_ref[...] = jnp.where(core == 0, right, left).astype(BF)
 
 
-def combine(back, routes, route_weights, core):
+def combine(back, mix, core):
     return pl.pallas_call(
         combine_kernel,
         out_shape=(
             jax.ShapeDtypeStruct((TOK, 256), F32),
             jax.ShapeDtypeStruct((TOK, 256), BF),
         ),
-        in_specs=[SMEM] + [VMEM] * 3,
+        in_specs=[SMEM, VMEM, HBM, HBM],
         out_specs=(VMEM, VMEM),
+        scratch_shapes=[
+            pltpu.VMEM((TOK, LANES), BF),
+            pltpu.VMEM((TOK, LANES), BF),
+            pltpu.SemaphoreType.DMA((2,)),
+        ],
         compiler_params=pltpu.CompilerParams(vmem_limit_bytes=24 << 20),
         cost_estimate=pl.CostEstimate(flops=10**9, bytes_accessed=4 << 20, transcendentals=0),
         name="combine",
-    )(core, routes, route_weights, back)
-
-
-def shared_kernel(normed_ref, common_ref, terms_ref, *common_refs):
-    for n in range(3):
-        common_refs[n][...] = common_ref[:, n * 128 : (n + 1) * 128]
-    act = dot(normed_ref[...], common_ref[:, 0:256])
+    )(core, back, *mix)
+
+
+Z_ORDER = (0, 4, 2, 6, 1, 5, 3, 7)
+
+
+def shared_kernel(at_ref, normed_ref, *refs):
+    block_refs, terms_ref, common_refs = refs[:NY], refs[NY], refs[NY + 1 :]
+    z, y = at_ref[0], at_ref[1]
+    for dy in range(NY):
+        for dz in range(NZ):
+            row = ((z + Z_ORDER[dz]) % NZ * NY + (y + dy) % NY) * 64
+            part = pl.ds(pl.multiple_of(row, 64), 64)
+            for n in range(3):
+                common_refs[n][part, :] = block_refs[dy][dz, :, n * 128 : (n + 1) * 128]
+    normed = normed_ref[...]
+    both = jnp.concatenate([common_refs[0][...], common_refs[1][...]], axis=1)
+    act = dot(normed, both)
     gate, up = act[:, 0:128], act[:, 128:256]
     hidden = (gate / (1.0 + jnp.exp(-gate)) * up).astype(BF)
     for n in range(NX * NC):
-        terms_ref[n] = dot_t(hidden, common_ref[n * 256 : (n + 1) * 256, 256:384]).astype(BF)
-
-
-def shared_expert(normed, common):
+        terms_ref[n] = dot_t(hidden, common_refs[2][n * 256 : (n + 1) * 256, :]).astype(BF)
+
+
+def shared_expert(normed, blocks, at):
     shape = jax.ShapeDtypeStruct((D, 128), BF)
     return pl.pallas_call(
         shared_kernel,
         out_shape=(jax.ShapeDtypeStruct((NX * NC, TOK, 256), BF), shape, shape, shape),
-        in_specs=[VMEM] * 2,
+        in_specs=[SMEM] + [VMEM] * (1 + NY),
         out_specs=(VMEM,) * 4,
         compiler_params=pltpu.CompilerParams(vmem_limit_bytes=24 << 20),
         cost_estimate=pl.CostEstimate(
             flops=6 * TOK * D * 128, bytes_accessed=6 << 20, transcendentals=TOK * 128
         ),
         name="shared_expert",
-    )(normed, common)
+    )(at, normed, *blocks)
 
 
 def exchange(array, axes):
@@ -318,7 +359,7 @@
     shared_up,
     shared_down,
 ):
-    x, c = (lax.axis_index(a).astype(jnp.int32) for a in TP)
+    z, y, x, c = (lax.axis_index(a).astype(jnp.int32) for a in FS + TP)
     at = (x * NC + c).reshape(1)
     core = c.reshape(1)
 
@@ -330,7 +371,10 @@
         ],
         axis=1,
     )
-    common = lax.all_gather(shared, FS, axis=0, tiled=True)
+    column = shared[None]
+    for k in (4, 2, 1):
+        column = jnp.concatenate([column, shift(column, "z", NZ, -k)])
+    blocks = [column] + [shift(column, "y", NY, -k) for k in range(1, NY)]
 
     both_in = round_both(norm_gain, expert_gate, expert_up)
     both_in, expert_down = after(both_in, expert_down)
@@ -353,12 +397,15 @@
     both_all += [shift(piece, "c", NC, 1) for piece in both_all]
     down_all += [shift(piece, "c", NC, 1) for piece in down_all]
 
-    shared_terms, common_gate, common_up, common_down = shared_expert(normed, common)
+    shared_terms, common_gate, common_up, common_down = shared_expert(
+        normed, blocks, jnp.stack([z, y])
+    )
     shared_sum = lax.psum_scatter(shared_terms, TP, scatter_dimension=0, tiled=True)[0]
 
     results, sample_gate, sample_up, sample_down = ffn(block, both_all, down_all)
+    mix = mixing(routes, route_weights, core)
     back = exchange(results.reshape(EXPERTS * NX, 8, 640), ("z", "y", "x"))
-    own, other = combine(back.reshape(EXPERTS * NX * 8, 640), routes, route_weights, core)
+    own, other = combine(back.reshape(EXPERTS * NX * 8, 640), mix, core)
     other = shift(other, "c", NC, 1)
     layer_output = (own + other.astype(F32) + shared_sum.astype(F32)).astype(BF)
     return (

time: 211 us -> 257 us (1.22)
  waiting for transfers between devices: 115 us -> 152 us
  starting transfers between devices: 48.7 us -> 59.9 us
    ppermute x19 -> x25, waiting for transfers between devices: 32.2 us -> 82.3 us  [shift(): lax.ppermute(array, axis, [(i, (i + by) % size) for i in range(size)])]
    reduce_scatter x1, waiting for transfers between devices: 12.7 us -> 32.5 us  [layer(): lax.psum_scatter(shared_terms, TP, scatter_dimension=0, tiled=True)[0]]
    all_to_all x4, waiting for transfers between devices: 54.7 us -> 37.5 us  [exchange(): return lax.all_to_all(array, axes, split_axis=0, concat_axis=0, tiled=True)]
    all_gather x1 -> x0, waiting for transfers between devices: 15.2 us -> none  [layer(): common = lax.all_gather(shared, FS, axis=0, tiled=True)]
    ppermute x19 -> x25, starting transfers between devices: 12.2 us -> 24.6 us  [shift(): lax.ppermute(array, axis, [(i, (i + by) % size) for i in range(size)])]
  transfers between devices with their start and end apart: 25 -> 30, of which waited for: 12 -> 15; matrix products, arithmetic and copies ran while one was open for 2% -> 1% of each run, Pallas kernels for 9% -> 7%
where the time goes in v2:
time: 257 us
  waiting for transfers between devices  152 us (59%)
  starting transfers between devices  59.9 us (23%)
  Pallas kernels  21.6 us (8%)
  between operations  14.4 us (6%)
  local copies, waits for them, and re-layouts  5.64 us (2%)
  other arithmetic  2.74 us (1%)
    ppermute x25, waiting for transfers between devices, shift(): lax.ppermute(array, axis, [(i, (i + by) % size) for i in range(size)])  82.3 us
    all_to_all x4, waiting for transfers between devices, exchange(): return lax.all_to_all(array, axes, split_axis=0, concat_axis=0, tiled=True)  37.5 us
    all_to_all x4, starting transfers between devices, exchange(): return lax.all_to_all(array, axes, split_axis=0, concat_axis=0, tiled=True)  35.2 us
    reduce_scatter x1, waiting for transfers between devices, layer(): lax.psum_scatter(shared_terms, TP, scatter_dimension=0, tiled=True)[0]  32.5 us
    ppermute x25, starting transfers between devices, shift(): lax.ppermute(array, axis, [(i, (i + by) % size) for i in range(size)])  24.6 us
    pallas_call x1, Pallas kernels, ffn(): pl.pallas_call(ffn_kernel, out_shape=(jax.ShapeDtypeStruct((EXPERTS, NX,...  10.5 us
  transfers between devices with their start and end apart: 30, of which 15 were waited for; matrix products, arithmetic and copies ran while one was open for 1% of the time, Pallas kernels for 7%

profile of v2, /device:TPU:16, one launch (start us, length us, event | category | flops | bytes accessed | tf_op | source)
XLA Modules:
  0.0 256.5 jit_solution(12112885797908494864)
XLA Ops:
  7.2 3.8 %round_both.1 = bf16[32,2,64,128]{3,2,1,0:T(8,128)(2,1)} custom-call(f32[1,64]{1,0:T(1,128)} %bitcast.21, f32[32,64,128]{2,1,0:T(8,128)} %gate_ref.1, f32[32,64,128]{2,1,0:T(8,128)} %up_ref.1), custom_call_target="tpu_custom_call" | custom-call | flops 10000000 | bytes 3145728 | tf_op jit(solution)/shard_map/round_both/pallas_call | solution.py:98
  10.9 11.7 %all-to-all-start = ((bf16[32,2,64,128]{3,2,1,0:T(8,128)(2,1)}), bf16[32,2,64,128]{3,2,1,0:T(8,128)(2,1)S(1)}, u32[]{:S(2)}, u32[]{:S(2)}) async-start(bf16[32,2,64,128]{3,2,1,0:T(8,128)(2,1)} %round_both.1), calls=%async_computation | async-start | bytes 2097152 | tf_op jit(solution)/shard_map/all_to_all | solution.py:335
  23.6 27.2 %all-to-all-done.refs_0_ = bf16[32,2,64,128]{3,2,1,0:T(8,128)(2,1)S(1)} async-done(((bf16[32,2,64,128]{3,2,1,0:T(8,128)(2,1)}), bf16[32,2,64,128]{3,2,1,0:T(8,128)(2,1)S(1)}, u32[]{:S(2)}, u32[]{:S(2)}) %all-to-all-start) | async-done | bytes 1048608 | tf_op jit(solution)/shard_map/all_to_all | solution.py:335
  50.7 5.6 %all-to-all-start.1 = ((bf16[32,64,128]{2,1,0:T(8,128)(2,1)}), bf16[32,64,128]{2,1,0:T(8,128)(2,1)}, u32[]{:S(2)}, u32[]{:S(2)}) async-start(bf16[32,64,128]{2,1,0:T(8,128)(2,1)} %convert_element_type.24), calls=%async_computation.1 | async-start | bytes 1048576 | tf_op jit(solution)/shard_map/all_to_all | solution.py:335
  56.4 1.6 collective-permute-start
  57.9 1.7 collective-permute-start.1
  59.7 2.2 dispatch.1
  61.9 10.3 %all-to-all-done.1.refs_10_ = bf16[32,64,128]{2,1,0:T(8,128)(2,1)} async-done(((bf16[32,64,128]{2,1,0:T(8,128)(2,1)}), bf16[32,64,128]{2,1,0:T(8,128)(2,1)}, u32[]{:S(2)}, u32[]{:S(2)}) %all-to-all-start.1) | async-done | bytes 524320 | tf_op jit(solution)/shard_map/all_to_all | solution.py:335
  72.2 5.8 %all-to-all-start.2 = ((bf16[32,8,2560]{2,1,0:T(8,128)(2,1)}), bf16[32,8,2560]{2,1,0:T(8,128)(2,1)}, u32[]{:S(2)}, u32[]{:S(2)}) async-start(bf16[32,8,2560]{2,1,0:T(8,128)(2,1)} %bitcast.4), calls=%async_computation.2 | async-start | bytes 2621440 | tf_op jit(solution)/shard_map/all_to_all | solution.py:335
  78.1 1.6 collective-permute-start.9
  79.8 5.5 %collective-permute-start.19 = (bf16[1,64,384]{2,1,0:T(8,128)(2,1)S(1)}, bf16[1,64,384]{2,1,0:T(8,128)(2,1)S(1)}, u32[]{:S(2)}, u32[]{:S(2)}) collective-permute-start(bf16[1,64,384]{2,1,0:T(8,128)(2,1)S(1)} %maximum_bitcast_fusion), channel_id=1, source_target_pairs={{0,128},{32,160},{64,192},{96,224},{128,0},{160,32},{192,64},{224,... | collective-permute-start | bytes 147464 | tf_op jit(solution)/shard_map/ppermute | solution.py:39
  85.2 27.4 %collective-permute-done.19 = bf16[1,64,384]{2,1,0:T(8,128)(2,1)S(1)} collective-permute-done((bf16[1,64,384]{2,1,0:T(8,128)(2,1)S(1)}, bf16[1,64,384]{2,1,0:T(8,128)(2,1)S(1)}, u32[]{:S(2)}, u32[]{:S(2)}) %collective-permute-start.19) | collective-permute-done | bytes 49184 | tf_op jit(solution)/shard_map/ppermute | solution.py:39
  113.3 2.8 %collective-permute-start.10 = (bf16[32,64,128]{2,1,0:T(8,128)(2,1)}, bf16[32,64,128]{2,1,0:T(8,128)(2,1)S(1)}, u32[]{:S(2)}, u32[]{:S(2)}) collective-permute-start(bf16[32,64,128]{2,1,0:T(8,128)(2,1)} %all-to-all-done.1.refs_10_), channel_id=1, source_target_pairs={{0,6},{2,0},{4,2},{6,4},{1,7},{3,1},{5,3},{7,5},{8,14},{10,8},{12,... | collective-permute-start | bytes 1572872 | tf_op jit(solution)/shard_map/ppermute | solution.py:39
  119.3 1.5 collective-permute-start.2
  120.8 1.7 collective-permute-start.3
  122.9 5.7 %collective-permute-done.10.refs_12_ = bf16[32,64,128]{2,1,0:T(8,128)(2,1)S(1)} collective-permute-done((bf16[32,64,128]{2,1,0:T(8,128)(2,1)}, bf16[32,64,128]{2,1,0:T(8,128)(2,1)S(1)}, u32[]{:S(2)}, u32[]{:S(2)}) %collective-permute-start.10) | collective-permute-done | bytes 524320 | tf_op jit(solution)/shard_map/ppermute | solution.py:39
  129.2 6.1 %collective-permute-done.2.refs_3_ = bf16[16,2,64,128]{3,2,1,0:T(8,128)(2,1)S(1)} collective-permute-done((bf16[16,2,64,128]{3,2,1,0:T(8,128)(2,1)S(1)}, bf16[16,2,64,128]{3,2,1,0:T(8,128)(2,1)S(1)}, u32[]{:S(2)}, u32[]{:S(2)}) %collective-permute-start.2) | collective-permute-done | bytes 524320 | tf_op jit(solution)/shard_map/ppermute | solution.py:39
  135.3 2.0 collective-permute-done.3.refs_4_
  137.4 2.2 collective-permute-done.11.refs_13_
  139.6 1.6 collective-permute-start.12
  141.1 6.2 %collective-permute-done.12.refs_14_ = bf16[16,64,128]{2,1,0:T(8,128)(2,1)S(1)} collective-permute-done((bf16[16,64,128]{2,1,0:T(8,128)(2,1)S(1)}, bf16[16,64,128]{2,1,0:T(8,128)(2,1)S(1)}, u32[]{:S(2)}, u32[]{:S(2)}) %collective-permute-start.12) | collective-permute-done | bytes 262176 | tf_op jit(solution)/shard_map/ppermute | solution.py:39
  149.1 1.7 collective-permute-done.17.refs_19_
  153.4 10.5 %ffn.1 = (bf16[32,4,8,640]{3,2,1,0:T(8,128)(2,1)}, bf16[32,64,128]{2,1,0:T(8,128)(2,1)}, bf16[32,64,128]{2,1,0:T(8,128)(2,1)}, bf16[32,64,128]{2,1,0:T(8,128)(2,1)}) custom-call(bf16[256,2560]{1,0:T(8,128)(2,1)} %bitcast.5.block_ref, bf16[32,2,64,128]{3,2,1,0:T(8,128)(2,1)} %copy-done.4, bf16[32,2,64,128]{3,2,1,0:T(8,128)(2,1)} %collective-permute-done.refs_1_, ...), custom_call_target="tpu_custom_call" | custom-call | flops 4026531840 | bytes 16777216 | tf_op jit(solution)/shard_map/ffn/pallas_call | solution.py:191
  164.0 12.1 %all-to-all-start.3 = ((bf16[128,8,640]{2,1,0:T(8,128)(2,1)}), bf16[128,8,640]{2,1,0:T(8,128)(2,1)S(1)}, u32[]{:S(2)}, u32[]{:S(2)}) async-start(bf16[128,8,640]{2,1,0:T(8,128)(2,1)} %bitcast.20), calls=%async_computation.3 | async-start | bytes 2621440 | tf_op jit(solution)/shard_map/all_to_all | solution.py:335
  176.9 2.7 %collective-permute-start.23 = (bf16[8,64,384]{2,1,0:T(8,128)(2,1)S(1)}, bf16[8,64,384]{2,1,0:T(8,128)(2,1)S(1)}, u32[]{:S(2)}, u32[]{:S(2)}) collective-permute-start(bf16[8,64,384]{2,1,0:T(8,128)(2,1)S(1)} %pad_maximum_fusion.refs_0_), channel_id=1, source_target_pairs={{0,16},{8,24},{16,0},{24,8},{1,17},{9,25},{17,1},{25,9},{2,18},{10... | collective-permute-start | bytes 1179656 | tf_op jit(solution)/shard_map/ppermute | solution.py:39
  179.9 15.4 %collective-permute-done.22.refs_1_ = bf16[8,64,384]{2,1,0:T(8,128)(2,1)S(1)} collective-permute-done((bf16[8,64,384]{2,1,0:T(8,128)(2,1)S(1)}, bf16[8,64,384]{2,1,0:T(8,128)(2,1)S(1)}, u32[]{:S(2)}, u32[]{:S(2)}) %collective-permute-start.22) | collective-permute-done | bytes 393248 | tf_op jit(solution)/shard_map/ppermute | solution.py:39
  195.3 3.1 %collective-permute-done.23.refs_2_ = bf16[8,64,384]{2,1,0:T(8,128)(2,1)S(1)} collective-permute-done((bf16[8,64,384]{2,1,0:T(8,128)(2,1)S(1)}, bf16[8,64,384]{2,1,0:T(8,128)(2,1)S(1)}, u32[]{:S(2)}, u32[]{:S(2)}) %collective-permute-start.23) | collective-permute-done | bytes 393248 | tf_op jit(solution)/shard_map/ppermute | solution.py:39
  198.4 10.7 %collective-permute-done.24.refs_3_ = bf16[8,64,384]{2,1,0:T(8,128)(2,1)} collective-permute-done((bf16[8,64,384]{2,1,0:T(8,128)(2,1)S(1)}, bf16[8,64,384]{2,1,0:T(8,128)(2,1)}, u32[]{:S(2)}, u32[]{:S(2)}) %collective-permute-start.24) | collective-permute-done | bytes 393248 | tf_op jit(solution)/shard_map/ppermute | solution.py:39
  209.1 2.9 %shared_expert.1 = (bf16[8,256,256]{2,1,0:T(8,128)(2,1)S(1)}, bf16[2048,128]{1,0:T(8,128)(2,1)}, bf16[2048,128]{1,0:T(8,128)(2,1)}, bf16[2048,128]{1,0:T(8,128)(2,1)}) custom-call(s32[2]{0:T(128)S(1)} %pad_add_fusion.at_ref, bf16[256,2048]{1,0:T(8,128)(2,1)S(1)} %get-tuple-element.39.normed_ref, bf16[8,64,384]{2,1,0:T(8,128)(2,1)S(1)} %pad_maximum_fusion.refs_0_, ...), custom_call_target="tpu_custom_call" | custom-call | flops 402653184 | bytes 6291456 | tf_op jit(solution)/shard_map/shared_expert/pallas_call | solution.py:321
  214.3 1.2 combine.1
  215.6 32.5 %reduce-scatter.2.cloned.1.call-done = bf16[1,256,256]{2,1,0:T(8,128)(2,1)} async-done(((bf16[8,256,256]{2,1,0:T(8,128)(2,1)}), bf16[1,256,256]{2,1,0:T(8,128)(2,1)}) %reduce-scatter.2.cloned.1.call-update) | async-done | bytes 131088 | tf_op jit(solution)/shard_map/reduce_scatter | solution.py:403
  248.1 1.6 fusion
  (90 shorter events, 13.6 us)
Async XLA Ops:
  10.9 39.8 %all-to-all-start = ((bf16[32,2,64,128]{3,2,1,0:T(8,128)(2,1)}), bf16[32,2,64,128]{3,2,1,0:T(8,128)(2,1)S(1)}, u32[]{:S(2)}, u32[]{:S(2)}) async-start(bf16[32,2,64,128]{3,2,1,0:T(8,128)(2,1)} %round_both.1), calls=%async_computation | async-start | bytes 2097152 | tf_op jit(solution)/shard_map/all_to_all | solution.py:335
  22.7 37.0 %copy-start.1 = (s32[256,6]{0,1:T(8,128)S(1)}, s32[256,6]{0,1:T(8,128)}, u32[]{:S(2)}) copy-start(s32[256,6]{0,1:T(8,128)} %param.11) | copy-start | bytes 18436
  22.7 37.0 %copy-start.2 = (bf16[256,2048]{1,0:T(8,128)(2,1)S(1)}, bf16[256,2048]{1,0:T(8,128)(2,1)}, u32[]{:S(2)}) copy-start(bf16[256,2048]{1,0:T(8,128)(2,1)} %tokens_ref.1) | copy-start | bytes 3145732
  50.7 21.5 %all-to-all-start.1 = ((bf16[32,64,128]{2,1,0:T(8,128)(2,1)}), bf16[32,64,128]{2,1,0:T(8,128)(2,1)}, u32[]{:S(2)}, u32[]{:S(2)}) async-start(bf16[32,64,128]{2,1,0:T(8,128)(2,1)} %convert_element_type.24), calls=%async_computation.1 | async-start | bytes 1048576 | tf_op jit(solution)/shard_map/all_to_all | solution.py:335
  56.4 56.9 %collective-permute-start = (bf16[32,2,64,128]{3,2,1,0:T(8,128)(2,1)S(1)}, bf16[32,2,64,128]{3,2,1,0:T(8,128)(2,1)}, u32[]{:S(2)}, u32[]{:S(2)}) collective-permute-start(bf16[32,2,64,128]{3,2,1,0:T(8,128)(2,1)S(1)} %all-to-all-done.refs_0_), channel_id=1, source_target_pairs={{0,2},{2,4},{4,6},{6,0},{1,3},{3,5},{5,7},{7,1},{8,10},{10,12},{12... | collective-permute-start | bytes 3145736 | tf_op jit(solution)/shard_map/ppermute | solution.py:39
  57.9 59.2 %collective-permute-start.1 = (bf16[32,2,64,128]{3,2,1,0:T(8,128)(2,1)S(1)}, bf16[32,2,64,128]{3,2,1,0:T(8,128)(2,1)}, u32[]{:S(2)}, u32[]{:S(2)}) collective-permute-start(bf16[32,2,64,128]{3,2,1,0:T(8,128)(2,1)S(1)} %all-to-all-done.refs_0_), channel_id=1, source_target_pairs={{0,6},{2,0},{4,2},{6,4},{1,7},{3,1},{5,3},{7,5},{8,14},{10,8},{12,... | collective-permute-start | bytes 3145736 | tf_op jit(solution)/shard_map/ppermute | solution.py:39
  72.2 81.2 %all-to-all-start.2 = ((bf16[32,8,2560]{2,1,0:T(8,128)(2,1)}), bf16[32,8,2560]{2,1,0:T(8,128)(2,1)}, u32[]{:S(2)}, u32[]{:S(2)}) async-start(bf16[32,8,2560]{2,1,0:T(8,128)(2,1)} %bitcast.4), calls=%async_computation.2 | async-start | bytes 2621440 | tf_op jit(solution)/shard_map/all_to_all | solution.py:335
  78.0 44.6 %collective-permute-start.4 = (bf16[32,2,64,128]{3,2,1,0:T(8,128)(2,1)S(1)}, bf16[32,2,64,128]{3,2,1,0:T(8,128)(2,1)S(1)}, u32[]{:S(2)}, u32[]{:S(2)}) collective-permute-start(bf16[32,2,64,128]{3,2,1,0:T(8,128)(2,1)S(1)} %all-to-all-done.refs_0_), channel_id=1, source_target_pairs={{0,1},{1,0},{2,3},{3,2},{4,5},{5,4},{6,7},{7,6},{8,9},{9,8},{10,11... | collective-permute-start | bytes 3145736 | tf_op jit(solution)/shard_map/ppermute | solution.py:39
  78.1 42.7 %collective-permute-start.9 = (bf16[32,64,128]{2,1,0:T(8,128)(2,1)}, bf16[32,64,128]{2,1,0:T(8,128)(2,1)S(1)}, u32[]{:S(2)}, u32[]{:S(2)}) collective-permute-start(bf16[32,64,128]{2,1,0:T(8,128)(2,1)} %all-to-all-done.1.refs_10_), channel_id=1, source_target_pairs={{0,2},{2,4},{4,6},{6,0},{1,3},{3,5},{5,7},{7,1},{8,10},{10,12},{12... | collective-permute-start | bytes 1572872 | tf_op jit(solution)/shard_map/ppermute | solution.py:39
  79.8 32.9 %collective-permute-start.19 = (bf16[1,64,384]{2,1,0:T(8,128)(2,1)S(1)}, bf16[1,64,384]{2,1,0:T(8,128)(2,1)S(1)}, u32[]{:S(2)}, u32[]{:S(2)}) collective-permute-start(bf16[1,64,384]{2,1,0:T(8,128)(2,1)S(1)} %maximum_bitcast_fusion), channel_id=1, source_target_pairs={{0,128},{32,160},{64,192},{96,224},{128,0},{160,32},{192,64},{224,... | collective-permute-start | bytes 147464 | tf_op jit(solution)/shard_map/ppermute | solution.py:39
  112.7 6.6 %collective-permute-start.20 = (bf16[2,64,384]{2,1,0:T(8,128)(2,1)S(1)}, bf16[2,64,384]{2,1,0:T(8,128)(2,1)S(1)}, u32[]{:S(2)}, u32[]{:S(2)}) collective-permute-start(bf16[2,64,384]{2,1,0:T(8,128)(2,1)S(1)} %pad_maximum_fusion.2), channel_id=1, source_target_pairs={{0,192},{32,224},{64,0},{96,32},{128,64},{160,96},{192,128},{224,1... | collective-permute-start | bytes 294920 | tf_op jit(solution)/shard_map/ppermute | solution.py:39
  113.3 15.4 %collective-permute-start.10 = (bf16[32,64,128]{2,1,0:T(8,128)(2,1)}, bf16[32,64,128]{2,1,0:T(8,128)(2,1)S(1)}, u32[]{:S(2)}, u32[]{:S(2)}) collective-permute-start(bf16[32,64,128]{2,1,0:T(8,128)(2,1)} %all-to-all-done.1.refs_10_), channel_id=1, source_target_pairs={{0,6},{2,0},{4,2},{6,4},{1,7},{3,1},{5,3},{7,5},{8,14},{10,8},{12,... | collective-permute-start | bytes 1572872 | tf_op jit(solution)/shard_map/ppermute | solution.py:39
  117.1 11.5 %collective-permute-start.13 = (bf16[32,64,128]{2,1,0:T(8,128)(2,1)}, bf16[32,64,128]{2,1,0:T(8,128)(2,1)S(1)}, u32[]{:S(2)}, u32[]{:S(2)}) collective-permute-start(bf16[32,64,128]{2,1,0:T(8,128)(2,1)} %all-to-all-done.1.refs_10_), channel_id=1, source_target_pairs={{0,1},{1,0},{2,3},{3,2},{4,5},{5,4},{6,7},{7,6},{8,9},{9,8},{10,11... | collective-permute-start | bytes 1572872 | tf_op jit(solution)/shard_map/ppermute | solution.py:39
  119.3 16.0 %collective-permute-start.2 = (bf16[16,2,64,128]{3,2,1,0:T(8,128)(2,1)S(1)}, bf16[16,2,64,128]{3,2,1,0:T(8,128)(2,1)S(1)}, u32[]{:S(2)}, u32[]{:S(2)}) collective-permute-start(bf16[16,2,64,128]{3,2,1,0:T(8,128)(2,1)S(1)} %slice.16), channel_id=1, source_target_pairs={{0,2},{2,4},{4,6},{6,0},{1,3},{3,5},{5,7},{7,1},{8,10},{10,12},{12... | collective-permute-start | bytes 1572872 | tf_op jit(solution)/shard_map/ppermute | solution.py:39
  120.8 16.5 %collective-permute-start.3 = (bf16[16,2,64,128]{3,2,1,0:T(8,128)(2,1)S(1)}, bf16[16,2,64,128]{3,2,1,0:T(8,128)(2,1)S(1)}, u32[]{:S(2)}, u32[]{:S(2)}) collective-permute-start(bf16[16,2,64,128]{3,2,1,0:T(8,128)(2,1)S(1)} %slice.17), channel_id=1, source_target_pairs={{0,6},{2,0},{4,2},{6,4},{1,7},{3,1},{5,3},{7,5},{8,14},{10,8},{12,... | collective-permute-start | bytes 1572872 | tf_op jit(solution)/shard_map/ppermute | solution.py:39
  122.6 17.0 %collective-permute-start.11 = (bf16[16,64,128]{2,1,0:T(8,128)(2,1)S(1)}, bf16[16,64,128]{2,1,0:T(8,128)(2,1)S(1)}, u32[]{:S(2)}, u32[]{:S(2)}) collective-permute-start(bf16[16,64,128]{2,1,0:T(8,128)(2,1)S(1)} %slice.18), channel_id=1, source_target_pairs={{0,2},{2,4},{4,6},{6,0},{1,3},{3,5},{5,7},{7,1},{8,10},{10,12},{12... | collective-permute-start | bytes 786440 | tf_op jit(solution)/shard_map/ppermute | solution.py:39
  128.7 18.7 %collective-permute-start.14 = (bf16[32,64,128]{2,1,0:T(8,128)(2,1)S(1)}, bf16[32,64,128]{2,1,0:T(8,128)(2,1)S(1)}, u32[]{:S(2)}, u32[]{:S(2)}) collective-permute-start(bf16[32,64,128]{2,1,0:T(8,128)(2,1)S(1)} %collective-permute-done.9.refs_11_), channel_id=1, source_target_pairs={{0,1},{1,0},{2,3},{3,2},{4,5},{5,4},{6,7},{7,6},{8,9},{9,8},{10,11... | collective-permute-start | bytes 1572872 | tf_op jit(solution)/shard_map/ppermute | solution.py:39
  128.7 19.2 %collective-permute-start.15 = (bf16[32,64,128]{2,1,0:T(8,128)(2,1)S(1)}, bf16[32,64,128]{2,1,0:T(8,128)(2,1)S(1)}, u32[]{:S(2)}, u32[]{:S(2)}) collective-permute-start(bf16[32,64,128]{2,1,0:T(8,128)(2,1)S(1)} %collective-permute-done.10.refs_12_), channel_id=1, source_target_pairs={{0,1},{1,0},{2,3},{3,2},{4,5},{5,4},{6,7},{7,6},{8,9},{9,8},{10,11... | collective-permute-start | bytes 1572872 | tf_op jit(solution)/shard_map/ppermute | solution.py:39
  135.3 16.1 %collective-permute-start.5 = (bf16[32,2,64,128]{3,2,1,0:T(8,128)(2,1)}, bf16[32,2,64,128]{3,2,1,0:T(8,128)(2,1)S(1)}, u32[]{:S(2)}, u32[]{:S(2)}) collective-permute-start(bf16[32,2,64,128]{3,2,1,0:T(8,128)(2,1)} %collective-permute-done.refs_1_), channel_id=1, source_target_pairs={{0,1},{1,0},{2,3},{3,2},{4,5},{5,4},{6,7},{7,6},{8,9},{9,8},{10,11... | collective-permute-start | bytes 3145736 | tf_op jit(solution)/shard_map/ppermute | solution.py:39
  137.3 16.1 %collective-permute-start.6 = (bf16[32,2,64,128]{3,2,1,0:T(8,128)(2,1)}, bf16[32,2,64,128]{3,2,1,0:T(8,128)(2,1)}, u32[]{:S(2)}, u32[]{:S(2)}) collective-permute-start(bf16[32,2,64,128]{3,2,1,0:T(8,128)(2,1)} %collective-permute-done.1.refs_2_), channel_id=1, source_target_pairs={{0,1},{1,0},{2,3},{3,2},{4,5},{5,4},{6,7},{7,6},{8,9},{9,8},{10,11... | collective-permute-start | bytes 3145736 | tf_op jit(solution)/shard_map/ppermute | solution.py:39
  139.6 7.8 %collective-permute-start.12 = (bf16[16,64,128]{2,1,0:T(8,128)(2,1)S(1)}, bf16[16,64,128]{2,1,0:T(8,128)(2,1)S(1)}, u32[]{:S(2)}, u32[]{:S(2)}) collective-permute-start(bf16[16,64,128]{2,1,0:T(8,128)(2,1)S(1)} %slice.19), channel_id=1, source_target_pairs={{0,6},{2,0},{4,2},{6,4},{1,7},{3,1},{5,3},{7,5},{8,14},{10,8},{12,... | collective-permute-start | bytes 786440 | tf_op jit(solution)/shard_map/ppermute | solution.py:39
  147.4 1.5 collective-permute-start.16
  147.4 4.0 %collective-permute-start.7 = (bf16[16,2,64,128]{3,2,1,0:T(8,128)(2,1)S(1)}, bf16[16,2,64,128]{3,2,1,0:T(8,128)(2,1)S(1)}, u32[]{:S(2)}, u32[]{:S(2)}) collective-permute-start(bf16[16,2,64,128]{3,2,1,0:T(8,128)(2,1)S(1)} %collective-permute-done.2.refs_3_), channel_id=1, source_target_pairs={{0,1},{1,0},{2,3},{3,2},{4,5},{5,4},{6,7},{7,6},{8,9},{9,8},{10,11... | collective-permute-start | bytes 1572872 | tf_op jit(solution)/shard_map/ppermute | solution.py:39
  147.9 3.5 %collective-permute-start.8 = (bf16[16,2,64,128]{3,2,1,0:T(8,128)(2,1)S(1)}, bf16[16,2,64,128]{3,2,1,0:T(8,128)(2,1)S(1)}, u32[]{:S(2)}, u32[]{:S(2)}) collective-permute-start(bf16[16,2,64,128]{3,2,1,0:T(8,128)(2,1)S(1)} %collective-permute-done.3.refs_4_), channel_id=1, source_target_pairs={{0,1},{1,0},{2,3},{3,2},{4,5},{5,4},{6,7},{7,6},{8,9},{9,8},{10,11... | collective-permute-start | bytes 1572872 | tf_op jit(solution)/shard_map/ppermute | solution.py:39
  148.9 1.9 collective-permute-start.17
  150.8 25.4 %collective-permute-start.21 = (bf16[4,64,384]{2,1,0:T(8,128)(2,1)S(1)}, bf16[4,64,384]{2,1,0:T(8,128)(2,1)S(1)}, u32[]{:S(2)}, u32[]{:S(2)}) collective-permute-start(bf16[4,64,384]{2,1,0:T(8,128)(2,1)S(1)} %pad_maximum_fusion.1), channel_id=1, source_target_pairs={{0,224},{32,0},{64,32},{96,64},{128,96},{160,128},{192,160},{224,1... | collective-permute-start | bytes 589832 | tf_op jit(solution)/shard_map/ppermute | solution.py:39
  164.0 50.4 %all-to-all-start.3 = ((bf16[128,8,640]{2,1,0:T(8,128)(2,1)}), bf16[128,8,640]{2,1,0:T(8,128)(2,1)S(1)}, u32[]{:S(2)}, u32[]{:S(2)}) async-start(bf16[128,8,640]{2,1,0:T(8,128)(2,1)} %bitcast.20), calls=%async_computation.3 | async-start | bytes 2621440 | tf_op jit(solution)/shard_map/all_to_all | solution.py:335
  176.1 72.0 %reduce-scatter.2.cloned.1.call-start = ((), (), s32[]{:S(2)}) async-start(), calls=%async_computation.5 | async-start | bytes 1179648 | tf_op jit(solution)/shard_map/reduce_scatter | solution.py:403
  176.2 19.1 %collective-permute-start.22 = (bf16[8,64,384]{2,1,0:T(8,128)(2,1)S(1)}, bf16[8,64,384]{2,1,0:T(8,128)(2,1)S(1)}, u32[]{:S(2)}, u32[]{:S(2)}) collective-permute-start(bf16[8,64,384]{2,1,0:T(8,128)(2,1)S(1)} %pad_maximum_fusion.refs_0_), channel_id=1, source_target_pairs={{0,24},{8,0},{16,8},{24,16},{1,25},{9,1},{17,9},{25,17},{2,26},{10... | collective-permute-start | bytes 1179656 | tf_op jit(solution)/shard_map/ppermute | solution.py:39
  176.9 21.5 %collective-permute-start.23 = (bf16[8,64,384]{2,1,0:T(8,128)(2,1)S(1)}, bf16[8,64,384]{2,1,0:T(8,128)(2,1)S(1)}, u32[]{:S(2)}, u32[]{:S(2)}) collective-permute-start(bf16[8,64,384]{2,1,0:T(8,128)(2,1)S(1)} %pad_maximum_fusion.refs_0_), channel_id=1, source_target_pairs={{0,16},{8,24},{16,0},{24,8},{1,17},{9,25},{17,1},{25,9},{2,18},{10... | collective-permute-start | bytes 1179656 | tf_op jit(solution)/shard_map/ppermute | solution.py:39
  179.5 29.5 %collective-permute-start.24 = (bf16[8,64,384]{2,1,0:T(8,128)(2,1)S(1)}, bf16[8,64,384]{2,1,0:T(8,128)(2,1)}, u32[]{:S(2)}, u32[]{:S(2)}) collective-permute-start(bf16[8,64,384]{2,1,0:T(8,128)(2,1)S(1)} %pad_maximum_fusion.refs_0_), channel_id=1, source_target_pairs={{0,8},{8,16},{16,24},{24,0},{1,9},{9,17},{17,25},{25,1},{2,10},{10... | collective-permute-start | bytes 1179656 | tf_op jit(solution)/shard_map/ppermute | solution.py:39
  215.5 32.6 %collective-permute-start.18 = (bf16[256,256]{1,0:T(8,128)(2,1)S(1)}, bf16[256,256]{1,0:T(8,128)(2,1)S(1)}, u32[]{:S(2)}, u32[]{:S(2)}) collective-permute-start(bf16[256,256]{1,0:T(8,128)(2,1)S(1)} %get-tuple-element.38), channel_id=1, source_target_pairs={{0,1},{1,0},{2,3},{3,2},{4,5},{5,4},{6,7},{7,6},{8,9},{9,8},{10,11... | collective-permute-start | bytes 393224 | tf_op jit(solution)/shard_map/ppermute | solution.py:39
  (18 other events, 198.3 us)
Sparse Core Ops, SparseCore 0:
  213.2 34.8 reduce-scatter.1

commit v3 on v2

--- a/solution.py
+++ b/solution.py
@@ -295,40 +295,29 @@
     )(core, back, *mix)
 
 
-Z_ORDER = (0, 4, 2, 6, 1, 5, 3, 7)
-
-
-def shared_kernel(at_ref, normed_ref, *refs):
-    block_refs, terms_ref, common_refs = refs[:NY], refs[NY], refs[NY + 1 :]
-    z, y = at_ref[0], at_ref[1]
-    for dy in range(NY):
-        for dz in range(NZ):
-            row = ((z + Z_ORDER[dz]) % NZ * NY + (y + dy) % NY) * 64
-            part = pl.ds(pl.multiple_of(row, 64), 64)
-            for n in range(3):
-                common_refs[n][part, :] = block_refs[dy][dz, :, n * 128 : (n + 1) * 128]
-    normed = normed_ref[...]
-    both = jnp.concatenate([common_refs[0][...], common_refs[1][...]], axis=1)
-    act = dot(normed, both)
+def shared_kernel(normed_ref, common_ref, terms_ref, *common_refs):
+    for n in range(3):
+        common_refs[n][...] = common_ref[:, n * 128 : (n + 1) * 128]
+    act = dot(normed_ref[...], common_ref[:, 0:256])
     gate, up = act[:, 0:128], act[:, 128:256]
     hidden = (gate / (1.0 + jnp.exp(-gate)) * up).astype(BF)
     for n in range(NX * NC):
-        terms_ref[n] = dot_t(hidden, common_refs[2][n * 256 : (n + 1) * 256, :]).astype(BF)
-
-
-def shared_expert(normed, blocks, at):
+        terms_ref[n] = dot_t(hidden, common_ref[n * 256 : (n + 1) * 256, 256:384]).astype(BF)
+
+
+def shared_expert(normed, common):
     shape = jax.ShapeDtypeStruct((D, 128), BF)
     return pl.pallas_call(
         shared_kernel,
         out_shape=(jax.ShapeDtypeStruct((NX * NC, TOK, 256), BF), shape, shape, shape),
-        in_specs=[SMEM] + [VMEM] * (1 + NY),
+        in_specs=[VMEM] * 2,
         out_specs=(VMEM,) * 4,
         compiler_params=pltpu.CompilerParams(vmem_limit_bytes=24 << 20),
         cost_estimate=pl.CostEstimate(
             flops=6 * TOK * D * 128, bytes_accessed=6 << 20, transcendentals=TOK * 128
         ),
         name="shared_expert",
-    )(at, normed, *blocks)
+    )(normed, common)
 
 
 def exchange(array, axes):
@@ -359,7 +348,7 @@
     shared_up,
     shared_down,
 ):
-    z, y, x, c = (lax.axis_index(a).astype(jnp.int32) for a in FS + TP)
+    x, c = (lax.axis_index(a).astype(jnp.int32) for a in TP)
     at = (x * NC + c).reshape(1)
     core = c.reshape(1)
 
@@ -371,10 +360,7 @@
         ],
         axis=1,
     )
-    column = shared[None]
-    for k in (4, 2, 1):
-        column = jnp.concatenate([column, shift(column, "z", NZ, -k)])
-    blocks = [column] + [shift(column, "y", NY, -k) for k in range(1, NY)]
+    common = lax.all_gather(shared, FS, axis=0, tiled=True)
 
     both_in = round_both(norm_gain, expert_gate, expert_up)
     both_in, expert_down = after(both_in, expert_down)
@@ -397,9 +383,7 @@
     both_all += [shift(piece, "c", NC, 1) for piece in both_all]
     down_all += [shift(piece, "c", NC, 1) for piece in down_all]
 
-    shared_terms, common_gate, common_up, common_down = shared_expert(
-        normed, blocks, jnp.stack([z, y])
-    )
+    shared_terms, common_gate, common_up, common_down = shared_expert(normed, common)
     shared_sum = lax.psum_scatter(shared_terms, TP, scatter_dimension=0, tiled=True)[0]
 
     results, sample_gate, sample_up, sample_down = ffn(block, both_all, down_all)

time: 257 us -> 210 us (0.82)
  waiting for transfers between devices: 152 us -> 116 us
  starting transfers between devices: 59.9 us -> 48.5 us
    ppermute x25 -> x19, waiting for transfers between devices: 82.3 us -> 32.2 us  [shift(): lax.ppermute(array, axis, [(i, (i + by) % size) for i in range(size)])]
    reduce_scatter x1, waiting for transfers between devices: 32.5 us -> 14.8 us  [layer(): lax.psum_scatter(shared_terms, TP, scatter_dimension=0, tiled=True)[0]]
    all_to_all x4, waiting for transfers between devices: 37.5 us -> 53.5 us  [exchange(): return lax.all_to_all(array, axes, split_axis=0, concat_axis=0, tiled=True)]
    all_gather x0 -> x1, waiting for transfers between devices: none -> 15.5 us  [layer(): common = lax.all_gather(shared, FS, axis=0, tiled=True)]
    ppermute x25 -> x19, starting transfers between devices: 24.6 us -> 12.2 us  [shift(): lax.ppermute(array, axis, [(i, (i + by) % size) for i in range(size)])]
  transfers between devices with their start and end apart: 30 -> 25, of which waited for: 15 -> 12; matrix products, arithmetic and copies ran while one was open for 1% -> 2% of each run, Pallas kernels for 7% -> 8%
where the time goes in v3:
time: 210 us; the launch traced here: 208 us
  waiting for transfers between devices  116 us (55%)
  starting transfers between devices  48.5 us (23%)
  Pallas kernels  21.4 us (10%)
  between operations  14.3 us (7%)
  local copies, waits for them, and re-layouts  4.82 us (2%)
  other arithmetic  3.19 us (2%)
    all_to_all x4, waiting for transfers between devices, exchange(): return lax.all_to_all(array, axes, split_axis=0, concat_axis=0, tiled=True)  53.5 us
    all_to_all x4, starting transfers between devices, exchange(): return lax.all_to_all(array, axes, split_axis=0, concat_axis=0, tiled=True)  36.3 us
    ppermute x19, waiting for transfers between devices, shift(): lax.ppermute(array, axis, [(i, (i + by) % size) for i in range(size)])  32.2 us
    all_gather x1, waiting for transfers between devices, layer(): common = lax.all_gather(shared, FS, axis=0, tiled=True)  15.5 us
    reduce_scatter x1, waiting for transfers between devices, layer(): lax.psum_scatter(shared_terms, TP, scatter_dimension=0, tiled=True)[0]  14.8 us
    ppermute x19, starting transfers between devices, shift(): lax.ppermute(array, axis, [(i, (i + by) % size) for i in range(size)])  12.2 us
    pallas_call x1, Pallas kernels, ffn(): pl.pallas_call(ffn_kernel, out_shape=(jax.ShapeDtypeStruct((EXPERTS, NX,...  10.5 us
  transfers between devices with their start and end apart: 25, of which 12 were waited for; matrix products, arithmetic and copies ran while one was open for 2% of the time, Pallas kernels for 8%

profile of v3, /device:TPU:16, one launch (start us, length us, event | category | flops | bytes accessed | tf_op | source)
XLA Modules:
  0.0 208.4 jit_solution(27316219336312828)
XLA Ops:
  7.2 3.7 %round_both.1 = bf16[32,2,64,128]{3,2,1,0:T(8,128)(2,1)} custom-call(f32[1,64]{1,0:T(1,128)} %bitcast.17, f32[32,64,128]{2,1,0:T(8,128)} %gate_ref.1, f32[32,64,128]{2,1,0:T(8,128)} %up_ref.1), custom_call_target="tpu_custom_call" | custom-call | flops 10000000 | bytes 3145728 | tf_op jit(solution)/shard_map/round_both/pallas_call | solution.py:98
  10.9 11.7 %all-to-all-start = ((bf16[32,2,64,128]{3,2,1,0:T(8,128)(2,1)}), bf16[32,2,64,128]{3,2,1,0:T(8,128)(2,1)S(1)}, u32[]{:S(2)}, u32[]{:S(2)}) async-start(bf16[32,2,64,128]{3,2,1,0:T(8,128)(2,1)} %round_both.1), calls=%async_computation | async-start | bytes 2097152 | tf_op jit(solution)/shard_map/all_to_all | solution.py:324
  23.5 27.2 %all-to-all-done.refs_0_ = bf16[32,2,64,128]{3,2,1,0:T(8,128)(2,1)S(1)} async-done(((bf16[32,2,64,128]{3,2,1,0:T(8,128)(2,1)}), bf16[32,2,64,128]{3,2,1,0:T(8,128)(2,1)S(1)}, u32[]{:S(2)}, u32[]{:S(2)}) %all-to-all-start) | async-done | bytes 1048608 | tf_op jit(solution)/shard_map/all_to_all | solution.py:324
  50.7 5.6 %all-to-all-start.1 = ((bf16[32,64,128]{2,1,0:T(8,128)(2,1)}), bf16[32,64,128]{2,1,0:T(8,128)(2,1)}, u32[]{:S(2)}, u32[]{:S(2)}) async-start(bf16[32,64,128]{2,1,0:T(8,128)(2,1)} %convert_element_type.24), calls=%async_computation.1 | async-start | bytes 1048576 | tf_op jit(solution)/shard_map/all_to_all | solution.py:324
  56.3 1.6 collective-permute-start
  57.9 1.7 collective-permute-start.1
  59.7 2.2 %dispatch.1 = (bf16[256,2560]{1,0:T(8,128)(2,1)}, bf16[256,2048]{1,0:T(8,128)(2,1)S(1)}) custom-call(s32[1]{0:T(128)} %bitcast.1.at_ref, bf16[256,2048]{1,0:T(8,128)(2,1)S(1)} %copy-done.2, s32[6,256]{1,0:T(8,128)S(1)} %bitcast.15), custom_call_target="tpu_custom_call" | custom-call | flops 1000000000 | bytes 4194304 | tf_op jit(solution)/shard_map/dispatch/pallas_call | solution.py:75
  61.8 10.3 %all-to-all-done.1.refs_10_ = bf16[32,64,128]{2,1,0:T(8,128)(2,1)} async-done(((bf16[32,64,128]{2,1,0:T(8,128)(2,1)}), bf16[32,64,128]{2,1,0:T(8,128)(2,1)}, u32[]{:S(2)}, u32[]{:S(2)}) %all-to-all-start.1) | async-done | bytes 524320 | tf_op jit(solution)/shard_map/all_to_all | solution.py:324
  72.2 5.8 %all-to-all-start.2 = ((bf16[32,8,2560]{2,1,0:T(8,128)(2,1)}), bf16[32,8,2560]{2,1,0:T(8,128)(2,1)}, u32[]{:S(2)}, u32[]{:S(2)}) async-start(bf16[32,8,2560]{2,1,0:T(8,128)(2,1)} %bitcast.4), calls=%async_computation.2 | async-start | bytes 2621440 | tf_op jit(solution)/shard_map/all_to_all | solution.py:324
  78.1 1.6 collective-permute-start.9
  80.4 1.8 collective-permute-start.10
  82.3 1.1 slice.16
  83.7 1.1 slice.17
  84.8 9.6 %collective-permute-done.9.refs_11_ = bf16[32,64,128]{2,1,0:T(8,128)(2,1)S(1)} collective-permute-done((bf16[32,64,128]{2,1,0:T(8,128)(2,1)}, bf16[32,64,128]{2,1,0:T(8,128)(2,1)S(1)}, u32[]{:S(2)}, u32[]{:S(2)}) %collective-permute-start.9) | collective-permute-done | bytes 524320 | tf_op jit(solution)/shard_map/ppermute | solution.py:39
  94.4 1.5 collective-permute-start.3
  97.1 8.6 %collective-permute-done.2.refs_3_ = bf16[16,2,64,128]{3,2,1,0:T(8,128)(2,1)S(1)} collective-permute-done((bf16[16,2,64,128]{3,2,1,0:T(8,128)(2,1)S(1)}, bf16[16,2,64,128]{3,2,1,0:T(8,128)(2,1)S(1)}, u32[]{:S(2)}, u32[]{:S(2)}) %collective-permute-start.2) | collective-permute-done | bytes 524320 | tf_op jit(solution)/shard_map/ppermute | solution.py:39
  105.6 1.7 collective-permute-done.3.refs_4_
  107.4 3.3 %collective-permute-done.11.refs_13_ = bf16[16,64,128]{2,1,0:T(8,128)(2,1)S(1)} collective-permute-done((bf16[16,64,128]{2,1,0:T(8,128)(2,1)S(1)}, bf16[16,64,128]{2,1,0:T(8,128)(2,1)S(1)}, u32[]{:S(2)}, u32[]{:S(2)}) %collective-permute-start.11) | collective-permute-done | bytes 262176 | tf_op jit(solution)/shard_map/ppermute | solution.py:39
  110.7 1.5 collective-permute-start.12
  112.2 6.3 %collective-permute-done.12.refs_14_ = bf16[16,64,128]{2,1,0:T(8,128)(2,1)S(1)} collective-permute-done((bf16[16,64,128]{2,1,0:T(8,128)(2,1)S(1)}, bf16[16,64,128]{2,1,0:T(8,128)(2,1)S(1)}, u32[]{:S(2)}, u32[]{:S(2)}) %collective-permute-start.12) | collective-permute-done | bytes 262176 | tf_op jit(solution)/shard_map/ppermute | solution.py:39
  119.2 0.9 collective-permute-done.16.refs_18_
  120.2 1.7 collective-permute-done.17.refs_19_
  123.0 10.5 %ffn.1 = (bf16[32,4,8,640]{3,2,1,0:T(8,128)(2,1)}, bf16[32,64,128]{2,1,0:T(8,128)(2,1)}, bf16[32,64,128]{2,1,0:T(8,128)(2,1)}, bf16[32,64,128]{2,1,0:T(8,128)(2,1)}) custom-call(bf16[256,2560]{1,0:T(8,128)(2,1)} %bitcast.5.block_ref, bf16[32,2,64,128]{3,2,1,0:T(8,128)(2,1)} %copy-done.4, bf16[32,2,64,128]{3,2,1,0:T(8,128)(2,1)} %collective-permute-done.refs_1_, ...), custom_call_target="tpu_custom_call" | custom-call | flops 4026531840 | bytes 16777216 | tf_op jit(solution)/shard_map/ffn/pallas_call | solution.py:191
  133.5 13.2 %all-to-all-start.3 = ((bf16[128,8,640]{2,1,0:T(8,128)(2,1)}), bf16[128,8,640]{2,1,0:T(8,128)(2,1)S(1)}, u32[]{:S(2)}, u32[]{:S(2)}) async-start(bf16[128,8,640]{2,1,0:T(8,128)(2,1)} %bitcast.16), calls=%async_computation.3 | async-start | bytes 2621440 | tf_op jit(solution)/shard_map/all_to_all | solution.py:324
  146.8 15.5 %all-gather.2.cloned.1.call-done.common_ref = bf16[2048,384]{1,0:T(8,128)(2,1)} async-done(((bf16[64,384]{1,0:T(8,128)(2,1)}), bf16[2048,384]{1,0:T(8,128)(2,1)}) %all-gather.2.cloned.1.call-update) | async-done | bytes 1572880 | tf_op jit(solution)/shard_map/all_gather | solution.py:363
  162.3 1.4 copy-done
  163.7 2.8 %shared_expert.1 = (bf16[8,256,256]{2,1,0:T(8,128)(2,1)}, bf16[2048,128]{1,0:T(8,128)(2,1)}, bf16[2048,128]{1,0:T(8,128)(2,1)}, bf16[2048,128]{1,0:T(8,128)(2,1)}) custom-call(bf16[256,2048]{1,0:T(8,128)(2,1)S(1)} %get-tuple-element.39.normed_ref, bf16[2048,384]{1,0:T(8,128)(2,1)S(1)} %copy-done), custom_call_target="tpu_custom_call" | custom-call | flops 402653184 | bytes 6291456 | tf_op jit(solution)/shard_map/shared_expert/pallas_call | solution.py:310
  166.8 1.0 mixing.1
  167.8 16.0 %all-to-all-done.3 = bf16[128,8,640]{2,1,0:T(8,128)(2,1)S(1)} async-done(((bf16[128,8,640]{2,1,0:T(8,128)(2,1)}), bf16[128,8,640]{2,1,0:T(8,128)(2,1)S(1)}, u32[]{:S(2)}, u32[]{:S(2)}) %all-to-all-start.3) | async-done | bytes 1310752 | tf_op jit(solution)/shard_map/all_to_all | solution.py:324
  183.8 1.2 combine.1
  185.1 14.8 %reduce-scatter.2.cloned.1.call-done = bf16[1,256,256]{2,1,0:T(8,128)(2,1)} async-done(((bf16[8,256,256]{2,1,0:T(8,128)(2,1)}), bf16[1,256,256]{2,1,0:T(8,128)(2,1)}) %reduce-scatter.2.cloned.1.call-update) | async-done | bytes 131088 | tf_op jit(solution)/shard_map/reduce_scatter | solution.py:387
  200.0 1.6 fusion
  (73 shorter events, 5.3 us)
Async XLA Ops:
  10.9 39.8 %all-to-all-start = ((bf16[32,2,64,128]{3,2,1,0:T(8,128)(2,1)}), bf16[32,2,64,128]{3,2,1,0:T(8,128)(2,1)S(1)}, u32[]{:S(2)}, u32[]{:S(2)}) async-start(bf16[32,2,64,128]{3,2,1,0:T(8,128)(2,1)} %round_both.1), calls=%async_computation | async-start | bytes 2097152 | tf_op jit(solution)/shard_map/all_to_all | solution.py:324
  22.6 37.0 %copy-start.1 = (s32[256,6]{0,1:T(8,128)S(1)}, s32[256,6]{0,1:T(8,128)}, u32[]{:S(2)}) copy-start(s32[256,6]{0,1:T(8,128)} %param.11) | copy-start | bytes 18436
  22.7 37.0 %copy-start.2 = (bf16[256,2048]{1,0:T(8,128)(2,1)S(1)}, bf16[256,2048]{1,0:T(8,128)(2,1)}, u32[]{:S(2)}) copy-start(bf16[256,2048]{1,0:T(8,128)(2,1)} %tokens_ref.1) | copy-start | bytes 3145732
  50.7 27.3 %copy-start.4 = (bf16[32,2,64,128]{3,2,1,0:T(8,128)(2,1)}, bf16[32,2,64,128]{3,2,1,0:T(8,128)(2,1)S(1)}, u32[]{:S(2)}) copy-start(bf16[32,2,64,128]{3,2,1,0:T(8,128)(2,1)S(1)} %all-to-all-done.refs_0_) | copy-start | bytes 3145732
  50.7 21.5 %all-to-all-start.1 = ((bf16[32,64,128]{2,1,0:T(8,128)(2,1)}), bf16[32,64,128]{2,1,0:T(8,128)(2,1)}, u32[]{:S(2)}, u32[]{:S(2)}) async-start(bf16[32,64,128]{2,1,0:T(8,128)(2,1)} %convert_element_type.24), calls=%async_computation.1 | async-start | bytes 1048576 | tf_op jit(solution)/shard_map/all_to_all | solution.py:324
  56.3 25.9 %collective-permute-start = (bf16[32,2,64,128]{3,2,1,0:T(8,128)(2,1)S(1)}, bf16[32,2,64,128]{3,2,1,0:T(8,128)(2,1)}, u32[]{:S(2)}, u32[]{:S(2)}) collective-permute-start(bf16[32,2,64,128]{3,2,1,0:T(8,128)(2,1)S(1)} %all-to-all-done.refs_0_), channel_id=1, source_target_pairs={{0,2},{2,4},{4,6},{6,0},{1,3},{3,5},{5,7},{7,1},{8,10},{10,12},{12... | collective-permute-start | bytes 3145736 | tf_op jit(solution)/shard_map/ppermute | solution.py:39
  57.9 25.4 %collective-permute-start.1 = (bf16[32,2,64,128]{3,2,1,0:T(8,128)(2,1)S(1)}, bf16[32,2,64,128]{3,2,1,0:T(8,128)(2,1)}, u32[]{:S(2)}, u32[]{:S(2)}) collective-permute-start(bf16[32,2,64,128]{3,2,1,0:T(8,128)(2,1)S(1)} %all-to-all-done.refs_0_), channel_id=1, source_target_pairs={{0,6},{2,0},{4,2},{6,4},{1,7},{3,1},{5,3},{7,5},{8,14},{10,8},{12,... | collective-permute-start | bytes 3145736 | tf_op jit(solution)/shard_map/ppermute | solution.py:39
  72.2 50.8 %all-to-all-start.2 = ((bf16[32,8,2560]{2,1,0:T(8,128)(2,1)}), bf16[32,8,2560]{2,1,0:T(8,128)(2,1)}, u32[]{:S(2)}, u32[]{:S(2)}) async-start(bf16[32,8,2560]{2,1,0:T(8,128)(2,1)} %bitcast.4), calls=%async_computation.2 | async-start | bytes 2621440 | tf_op jit(solution)/shard_map/all_to_all | solution.py:324
  77.9 84.4 %all-gather.2.cloned.1.call-start = ((), (), s32[]{:S(2)}) async-start(), calls=%async_computation.5 | async-start | bytes 1622016 | tf_op jit(solution)/shard_map/all_gather | solution.py:363
  78.0 18.0 %collective-permute-start.4 = (bf16[32,2,64,128]{3,2,1,0:T(8,128)(2,1)S(1)}, bf16[32,2,64,128]{3,2,1,0:T(8,128)(2,1)}, u32[]{:S(2)}, u32[]{:S(2)}) collective-permute-start(bf16[32,2,64,128]{3,2,1,0:T(8,128)(2,1)S(1)} %all-to-all-done.refs_0_), channel_id=1, source_target_pairs={{0,1},{1,0},{2,3},{3,2},{4,5},{5,4},{6,7},{7,6},{8,9},{9,8},{10,11... | collective-permute-start | bytes 3145736 | tf_op jit(solution)/shard_map/ppermute | solution.py:39
  78.1 16.3 %collective-permute-start.9 = (bf16[32,64,128]{2,1,0:T(8,128)(2,1)}, bf16[32,64,128]{2,1,0:T(8,128)(2,1)S(1)}, u32[]{:S(2)}, u32[]{:S(2)}) collective-permute-start(bf16[32,64,128]{2,1,0:T(8,128)(2,1)} %all-to-all-done.1.refs_10_), channel_id=1, source_target_pairs={{0,2},{2,4},{4,6},{6,0},{1,3},{3,5},{5,7},{7,1},{8,10},{10,12},{12... | collective-permute-start | bytes 1572872 | tf_op jit(solution)/shard_map/ppermute | solution.py:39
  80.4 16.1 %collective-permute-start.10 = (bf16[32,64,128]{2,1,0:T(8,128)(2,1)}, bf16[32,64,128]{2,1,0:T(8,128)(2,1)S(1)}, u32[]{:S(2)}, u32[]{:S(2)}) collective-permute-start(bf16[32,64,128]{2,1,0:T(8,128)(2,1)} %all-to-all-done.1.refs_10_), channel_id=1, source_target_pairs={{0,6},{2,0},{4,2},{6,4},{1,7},{3,1},{5,3},{7,5},{8,14},{10,8},{12,... | collective-permute-start | bytes 1572872 | tf_op jit(solution)/shard_map/ppermute | solution.py:39
  82.3 14.3 %collective-permute-start.13 = (bf16[32,64,128]{2,1,0:T(8,128)(2,1)}, bf16[32,64,128]{2,1,0:T(8,128)(2,1)S(1)}, u32[]{:S(2)}, u32[]{:S(2)}) collective-permute-start(bf16[32,64,128]{2,1,0:T(8,128)(2,1)} %all-to-all-done.1.refs_10_), channel_id=1, source_target_pairs={{0,1},{1,0},{2,3},{3,2},{4,5},{5,4},{6,7},{7,6},{8,9},{9,8},{10,11... | collective-permute-start | bytes 1572872 | tf_op jit(solution)/shard_map/ppermute | solution.py:39
  83.4 22.3 %collective-permute-start.2 = (bf16[16,2,64,128]{3,2,1,0:T(8,128)(2,1)S(1)}, bf16[16,2,64,128]{3,2,1,0:T(8,128)(2,1)S(1)}, u32[]{:S(2)}, u32[]{:S(2)}) collective-permute-start(bf16[16,2,64,128]{3,2,1,0:T(8,128)(2,1)S(1)} %slice.16), channel_id=1, source_target_pairs={{0,2},{2,4},{4,6},{6,0},{1,3},{3,5},{5,7},{7,1},{8,10},{10,12},{12... | collective-permute-start | bytes 1572872 | tf_op jit(solution)/shard_map/ppermute | solution.py:39
  94.4 28.6 %copy-start.5 = (bf16[32,64,128]{2,1,0:T(8,128)(2,1)}, bf16[32,64,128]{2,1,0:T(8,128)(2,1)S(1)}, u32[]{:S(2)}) copy-start(bf16[32,64,128]{2,1,0:T(8,128)(2,1)S(1)} %collective-permute-done.9.refs_11_) | copy-start | bytes 1572868
  94.4 12.9 %collective-permute-start.3 = (bf16[16,2,64,128]{3,2,1,0:T(8,128)(2,1)S(1)}, bf16[16,2,64,128]{3,2,1,0:T(8,128)(2,1)S(1)}, u32[]{:S(2)}, u32[]{:S(2)}) collective-permute-start(bf16[16,2,64,128]{3,2,1,0:T(8,128)(2,1)S(1)} %slice.17), channel_id=1, source_target_pairs={{0,6},{2,0},{4,2},{6,4},{1,7},{3,1},{5,3},{7,5},{8,14},{10,8},{12,... | collective-permute-start | bytes 1572872 | tf_op jit(solution)/shard_map/ppermute | solution.py:39
  96.0 14.7 %collective-permute-start.11 = (bf16[16,64,128]{2,1,0:T(8,128)(2,1)S(1)}, bf16[16,64,128]{2,1,0:T(8,128)(2,1)S(1)}, u32[]{:S(2)}, u32[]{:S(2)}) collective-permute-start(bf16[16,64,128]{2,1,0:T(8,128)(2,1)S(1)} %slice.18), channel_id=1, source_target_pairs={{0,2},{2,4},{4,6},{6,0},{1,3},{3,5},{5,7},{7,1},{8,10},{10,12},{12... | collective-permute-start | bytes 786440 | tf_op jit(solution)/shard_map/ppermute | solution.py:39
  96.5 25.5 %copy-start.6 = (bf16[32,64,128]{2,1,0:T(8,128)(2,1)}, bf16[32,64,128]{2,1,0:T(8,128)(2,1)S(1)}, u32[]{:S(2)}) copy-start(bf16[32,64,128]{2,1,0:T(8,128)(2,1)S(1)} %collective-permute-done.10.refs_12_) | copy-start | bytes 1572868
  96.5 22.0 %collective-permute-start.14 = (bf16[32,64,128]{2,1,0:T(8,128)(2,1)S(1)}, bf16[32,64,128]{2,1,0:T(8,128)(2,1)S(1)}, u32[]{:S(2)}, u32[]{:S(2)}) collective-permute-start(bf16[32,64,128]{2,1,0:T(8,128)(2,1)S(1)} %collective-permute-done.9.refs_11_), channel_id=1, source_target_pairs={{0,1},{1,0},{2,3},{3,2},{4,5},{5,4},{6,7},{7,6},{8,9},{9,8},{10,11... | collective-permute-start | bytes 1572872 | tf_op jit(solution)/shard_map/ppermute | solution.py:39
  96.6 25.5 %copy-start.12 = (bf16[32,64,128]{2,1,0:T(8,128)(2,1)}, bf16[32,64,128]{2,1,0:T(8,128)(2,1)S(1)}, u32[]{:S(2)}) copy-start(bf16[32,64,128]{2,1,0:T(8,128)(2,1)S(1)} %collective-permute-done.13.refs_15_) | copy-start | bytes 1572868
  96.6 22.5 %collective-permute-start.15 = (bf16[32,64,128]{2,1,0:T(8,128)(2,1)S(1)}, bf16[32,64,128]{2,1,0:T(8,128)(2,1)S(1)}, u32[]{:S(2)}, u32[]{:S(2)}) collective-permute-start(bf16[32,64,128]{2,1,0:T(8,128)(2,1)S(1)} %collective-permute-done.10.refs_12_), channel_id=1, source_target_pairs={{0,1},{1,0},{2,3},{3,2},{4,5},{5,4},{6,7},{7,6},{8,9},{9,8},{10,11... | collective-permute-start | bytes 1572872 | tf_op jit(solution)/shard_map/ppermute | solution.py:39
  105.6 16.4 %collective-permute-start.5 = (bf16[32,2,64,128]{3,2,1,0:T(8,128)(2,1)}, bf16[32,2,64,128]{3,2,1,0:T(8,128)(2,1)}, u32[]{:S(2)}, u32[]{:S(2)}) collective-permute-start(bf16[32,2,64,128]{3,2,1,0:T(8,128)(2,1)} %collective-permute-done.refs_1_), channel_id=1, source_target_pairs={{0,1},{1,0},{2,3},{3,2},{4,5},{5,4},{6,7},{7,6},{8,9},{9,8},{10,11... | collective-permute-start | bytes 3145736 | tf_op jit(solution)/shard_map/ppermute | solution.py:39
  107.3 14.7 %copy-start.13 = (bf16[16,2,64,128]{3,2,1,0:T(8,128)(2,1)}, bf16[16,2,64,128]{3,2,1,0:T(8,128)(2,1)S(1)}, u32[]{:S(2)}) copy-start(bf16[16,2,64,128]{3,2,1,0:T(8,128)(2,1)S(1)} %collective-permute-done.3.refs_4_) | copy-start | bytes 1572868
  107.3 15.6 %collective-permute-start.6 = (bf16[32,2,64,128]{3,2,1,0:T(8,128)(2,1)}, bf16[32,2,64,128]{3,2,1,0:T(8,128)(2,1)}, u32[]{:S(2)}, u32[]{:S(2)}) collective-permute-start(bf16[32,2,64,128]{3,2,1,0:T(8,128)(2,1)} %collective-permute-done.1.refs_2_), channel_id=1, source_target_pairs={{0,1},{1,0},{2,3},{3,2},{4,5},{5,4},{6,7},{7,6},{8,9},{9,8},{10,11... | collective-permute-start | bytes 3145736 | tf_op jit(solution)/shard_map/ppermute | solution.py:39
  110.7 7.9 %collective-permute-start.12 = (bf16[16,64,128]{2,1,0:T(8,128)(2,1)S(1)}, bf16[16,64,128]{2,1,0:T(8,128)(2,1)S(1)}, u32[]{:S(2)}, u32[]{:S(2)}) collective-permute-start(bf16[16,64,128]{2,1,0:T(8,128)(2,1)S(1)} %slice.19), channel_id=1, source_target_pairs={{0,6},{2,0},{4,2},{6,4},{1,7},{3,1},{5,3},{7,5},{8,14},{10,8},{12,... | collective-permute-start | bytes 786440 | tf_op jit(solution)/shard_map/ppermute | solution.py:39
  118.6 1.5 collective-permute-start.16
  118.6 3.4 %collective-permute-start.7 = (bf16[16,2,64,128]{3,2,1,0:T(8,128)(2,1)S(1)}, bf16[16,2,64,128]{3,2,1,0:T(8,128)(2,1)S(1)}, u32[]{:S(2)}, u32[]{:S(2)}) collective-permute-start(bf16[16,2,64,128]{3,2,1,0:T(8,128)(2,1)S(1)} %collective-permute-done.2.refs_3_), channel_id=1, source_target_pairs={{0,1},{1,0},{2,3},{3,2},{4,5},{5,4},{6,7},{7,6},{8,9},{9,8},{10,11... | collective-permute-start | bytes 1572872 | tf_op jit(solution)/shard_map/ppermute | solution.py:39
  119.1 2.9 %collective-permute-start.8 = (bf16[16,2,64,128]{3,2,1,0:T(8,128)(2,1)S(1)}, bf16[16,2,64,128]{3,2,1,0:T(8,128)(2,1)S(1)}, u32[]{:S(2)}, u32[]{:S(2)}) collective-permute-start(bf16[16,2,64,128]{3,2,1,0:T(8,128)(2,1)S(1)} %collective-permute-done.3.refs_4_), channel_id=1, source_target_pairs={{0,1},{1,0},{2,3},{3,2},{4,5},{5,4},{6,7},{7,6},{8,9},{9,8},{10,11... | collective-permute-start | bytes 1572872 | tf_op jit(solution)/shard_map/ppermute | solution.py:39
  120.1 1.9 collective-permute-start.17
  133.5 50.3 %all-to-all-start.3 = ((bf16[128,8,640]{2,1,0:T(8,128)(2,1)}), bf16[128,8,640]{2,1,0:T(8,128)(2,1)S(1)}, u32[]{:S(2)}, u32[]{:S(2)}) async-start(bf16[128,8,640]{2,1,0:T(8,128)(2,1)} %bitcast.16), calls=%async_computation.3 | async-start | bytes 2621440 | tf_op jit(solution)/shard_map/all_to_all | solution.py:324
  146.7 53.3 %reduce-scatter.2.cloned.1.call-start = ((), (), s32[]{:S(2)}) async-start(), calls=%async_computation.6 | async-start | bytes 1179648 | tf_op jit(solution)/shard_map/reduce_scatter | solution.py:387
  185.0 15.0 %collective-permute-start.18 = (bf16[256,256]{1,0:T(8,128)(2,1)S(1)}, bf16[256,256]{1,0:T(8,128)(2,1)S(1)}, u32[]{:S(2)}, u32[]{:S(2)}) collective-permute-start(bf16[256,256]{1,0:T(8,128)(2,1)S(1)} %get-tuple-element.38), channel_id=1, source_target_pairs={{0,1},{1,0},{2,3},{3,2},{4,5},{5,4},{6,7},{7,6},{8,9},{9,8},{10,11... | collective-permute-start | bytes 393224 | tf_op jit(solution)/shard_map/ppermute | solution.py:39
  (11 other events, 54.4 us)
Sparse Core Ops, SparseCore 0:
  81.9 80.3 all-gather.1
  166.6 33.2 reduce-scatter.1

commit v4 on v2

--- a/solution.py
+++ b/solution.py
@@ -170,18 +170,14 @@
     keep(2)
     out_row = iota((TOK, 64), 0)
     in_row = iota((TOK, 64), 1)
-    picks = [
-        flag(jnp.logical_and(in_row // 2 == out_row // 8, out_row % 8 == 2 * j + in_row % 2))
-        for j in range(4)
-    ]
-    for x in range(NX):
-        result = dot_t(hidden_ref[...], wide(2, range(8), slice(x * 8, (x + 1) * 8)))
+    packed = jnp.zeros((TOK, 512), F32)
+    for j in range(4):
+        result = dot_t(hidden_ref[...], wide(2, range(8), slice(j * 8, (j + 1) * 8)))
         result = result.astype(BF)
-        packed = jnp.zeros((TOK, 128), F32)
-        for j in range(4):
-            packed = packed + dot(picks[j], result[TOK:, j * 128 : (j + 1) * 128])
-        out_ref[:, x, :, 0:512] = result[:TOK].reshape(EXPERTS, 8, 512)
-        out_ref[:, x, :, 512:640] = packed.astype(BF).reshape(EXPERTS, 8, 128)
+        pick = jnp.logical_and(in_row // 2 == out_row // 8, out_row % 8 == 2 * j + in_row % 2)
+        packed = packed + dot(flag(pick), result[TOK:])
+        out_ref[:, j * 512 : (j + 1) * 512] = result[:TOK]
+    out_ref[:, D:] = packed.astype(BF)
     for copy in kept:
         copy.wait()
 
@@ -190,7 +186,7 @@
     sample = jax.ShapeDtypeStruct((EXPERTS, 64, 128), BF)
     return pl.pallas_call(
         ffn_kernel,
-        out_shape=(jax.ShapeDtypeStruct((EXPERTS, NX, 8, 640), BF), sample, sample, sample),
+        out_shape=(jax.ShapeDtypeStruct((TOK, D + 512), BF), sample, sample, sample),
         in_specs=[VMEM] + [HBM] * (2 * WAYS),
         out_specs=(VMEM, HBM, HBM, HBM),
         scratch_shapes=[
@@ -208,8 +204,7 @@
     )(block, *both, *single)
 
 
-def mixing_kernel(core_ref, routes_ref, weights_ref, first_ref, last_ref):
-    core = core_ref[0]
+def mixing_kernel(at_ref, routes_ref, weights_ref, first_ref, last_ref):
     expert = iota((TOK, EXPERTS), 1)
     member = jnp.zeros((TOK, EXPERTS), F32)
     weight = jnp.zeros((TOK, EXPERTS), F32)
@@ -220,21 +215,21 @@
     earlier = flag(iota((TOK, TOK), 1) < iota((TOK, TOK), 0))
     position = dot(earlier, member.astype(BF))
     slot = jnp.where(member > 0.0, position, -1.0).astype(BF)
-    spread = flag(iota((EXPERTS, LANES), 1) // (NX * 8) == iota((EXPERTS, LANES), 0))
+    spread = flag(iota((EXPERTS, LANES), 1) // 8 == iota((EXPERTS, LANES), 0))
     slots = dot(slot, spread)
     wide = dot(weight.astype(BF), spread)
     lane = iota((TOK, LANES), 1)
-    start = ((lane // 8) % NX * NC + core) * SHARE
+    start = at_ref[0] * SHARE
     first = slots == (start + lane % 8).astype(F32)
     last = slots == (start + 8 + lane % 2).astype(F32)
     first_ref[...] = jnp.where(first, wide, 0.0).astype(BF)
     last_ref[...] = jnp.where(last, wide, 0.0).astype(BF)
 
 
-LANES = EXPERTS * NX * 8
-
-
-def mixing(routes, route_weights, core):
+LANES = EXPERTS * 8
+
+
+def mixing(routes, route_weights, at):
     shape = jax.ShapeDtypeStruct((TOK, LANES), BF)
     return pl.pallas_call(
         mixing_kernel,
@@ -244,58 +239,67 @@
         compiler_params=pltpu.CompilerParams(vmem_limit_bytes=24 << 20),
         cost_estimate=pl.CostEstimate(flops=10**9, bytes_accessed=4 << 20, transcendentals=0),
         name="mixing",
-    )(core, routes, route_weights)
+    )(at, routes, route_weights)
 
 
 def combine_kernel(
-    core_ref, back_ref, first_hbm, last_hbm, own_ref, other_ref, first_ref, last_ref, sems
+    core_ref,
+    back_ref,
+    first_hbm,
+    last_hbm,
+    terms_hbm,
+    mine_ref,
+    other_ref,
+    first_ref,
+    last_ref,
+    terms_ref,
+    sems,
 ):
     core = core_ref[0]
     copies = [
         pltpu.make_async_copy(source, target, sems.at[i])
         for i, (source, target) in enumerate(
-            ((first_hbm, first_ref), (last_hbm, last_ref))
+            ((first_hbm, first_ref), (last_hbm, last_ref), (terms_hbm, terms_ref))
         )
     ]
     for copy in copies:
         copy.start()
     copies[0].wait()
-    total = dot(first_ref[...], back_ref[:, 0:512])
-    tail = back_ref[:, 512:640]
+    copies[1].wait()
     lane = iota((TOK, LANES), 1)
-    copies[1].wait()
     last = last_ref[...]
-    pieces = []
-    for j in range(4):
-        mine = lane % 8 // 2 == j
-        pieces.append(dot(jnp.where(mine, last, jnp.zeros_like(last)), tail))
-    total = total + jnp.concatenate(pieces, axis=1)
-    left, right = total[:, :256], total[:, 256:]
-    own_ref[...] = jnp.where(core == 0, left, right)
-    other_ref[...] = jnp.where(core == 0, right, left).astype(BF)
-
-
-def combine(back, mix, core):
+    tail = back_ref[:, D:]
+    for j in range(NX):
+        part = slice(j * 512, (j + 1) * 512)
+        pick = jnp.where(lane % 8 // 2 == j, last, jnp.zeros_like(last))
+        total = dot(first_ref[...], back_ref[:, part]) + dot(pick, tail)
+        if j == 0:
+            copies[2].wait()
+        total = total + terms_ref[:, part].astype(F32)
+        left, right = total[:, :256], total[:, 256:]
+        mine_ref[j] = jnp.where(core == 0, left, right)
+        other_ref[j] = jnp.where(core == 0, right, left).astype(BF)
+
+
+def combine(back, mix, terms, core):
     return pl.pallas_call(
         combine_kernel,
         out_shape=(
-            jax.ShapeDtypeStruct((TOK, 256), F32),
-            jax.ShapeDtypeStruct((TOK, 256), BF),
-        ),
-        in_specs=[SMEM, VMEM, HBM, HBM],
+            jax.ShapeDtypeStruct((NX, TOK, 256), F32),
+            jax.ShapeDtypeStruct((NX, TOK, 256), BF),
+        ),
+        in_specs=[SMEM, VMEM] + [HBM] * 3,
         out_specs=(VMEM, VMEM),
         scratch_shapes=[
             pltpu.VMEM((TOK, LANES), BF),
             pltpu.VMEM((TOK, LANES), BF),
-            pltpu.SemaphoreType.DMA((2,)),
+            pltpu.VMEM((TOK, D), BF),
+            pltpu.SemaphoreType.DMA((3,)),
         ],
         compiler_params=pltpu.CompilerParams(vmem_limit_bytes=24 << 20),
         cost_estimate=pl.CostEstimate(flops=10**9, bytes_accessed=4 << 20, transcendentals=0),
         name="combine",
-    )(core, back, *mix)
-
-
-Z_ORDER = (0, 4, 2, 6, 1, 5, 3, 7)
+    )(core, back, *mix, terms)
 
 
 def shared_kernel(at_ref, normed_ref, *refs):
@@ -303,24 +307,23 @@
     z, y = at_ref[0], at_ref[1]
     for dy in range(NY):
         for dz in range(NZ):
-            row = ((z + Z_ORDER[dz]) % NZ * NY + (y + dy) % NY) * 64
+            row = ((z + dz) % NZ * NY + (y + dy) % NY) * 64
             part = pl.ds(pl.multiple_of(row, 64), 64)
             for n in range(3):
                 common_refs[n][part, :] = block_refs[dy][dz, :, n * 128 : (n + 1) * 128]
-    normed = normed_ref[...]
     both = jnp.concatenate([common_refs[0][...], common_refs[1][...]], axis=1)
-    act = dot(normed, both)
+    act = dot(normed_ref[...], both)
     gate, up = act[:, 0:128], act[:, 128:256]
     hidden = (gate / (1.0 + jnp.exp(-gate)) * up).astype(BF)
-    for n in range(NX * NC):
-        terms_ref[n] = dot_t(hidden, common_refs[2][n * 256 : (n + 1) * 256, :]).astype(BF)
+    terms_ref[...] = dot_t(hidden, common_refs[2][...]).astype(BF)
 
 
 def shared_expert(normed, blocks, at):
     shape = jax.ShapeDtypeStruct((D, 128), BF)
+    terms = jax.ShapeDtypeStruct((TOK, D), BF)
     return pl.pallas_call(
         shared_kernel,
-        out_shape=(jax.ShapeDtypeStruct((NX * NC, TOK, 256), BF), shape, shape, shape),
+        out_shape=(terms, shape, shape, shape),
         in_specs=[SMEM] + [VMEM] * (1 + NY),
         out_specs=(VMEM,) * 4,
         compiler_params=pltpu.CompilerParams(vmem_limit_bytes=24 << 20),
@@ -329,6 +332,26 @@
         ),
         name="shared_expert",
     )(at, normed, *blocks)
+
+
+def pair_kernel(at_ref, mine_ref, swapped_ref, *out_refs):
+    for dx in range(NX):
+        x = (at_ref[0] + dx) % NX
+        total = mine_ref[x] + swapped_ref[x].astype(F32)
+        out_refs[dx][...] = total.astype(BF)
+
+
+def pair_sum(mine, swapped, at):
+    shape = jax.ShapeDtypeStruct((TOK, 256), BF)
+    return pl.pallas_call(
+        pair_kernel,
+        out_shape=(shape,) * NX,
+        in_specs=[SMEM, VMEM, VMEM],
+        out_specs=(VMEM,) * NX,
+        compiler_params=pltpu.CompilerParams(vmem_limit_bytes=8 << 20),
+        cost_estimate=pl.CostEstimate(flops=10**6, bytes_accessed=2 << 20, transcendentals=0),
+        name="pair_sum",
+    )(at, mine, swapped)
 
 
 def exchange(array, axes):
@@ -371,9 +394,8 @@
         ],
         axis=1,
     )
-    column = shared[None]
-    for k in (4, 2, 1):
-        column = jnp.concatenate([column, shift(column, "z", NZ, -k)])
+    column = [shared] + [shift(shared, "z", NZ, -k) for k in range(1, NZ)]
+    column = jnp.stack(column)
     blocks = [column] + [shift(column, "y", NY, -k) for k in range(1, NY)]
 
     both_in = round_both(norm_gain, expert_gate, expert_up)
@@ -397,17 +419,17 @@
     both_all += [shift(piece, "c", NC, 1) for piece in both_all]
     down_all += [shift(piece, "c", NC, 1) for piece in down_all]
 
-    shared_terms, common_gate, common_up, common_down = shared_expert(
+    terms, common_gate, common_up, common_down = shared_expert(
         normed, blocks, jnp.stack([z, y])
     )
-    shared_sum = lax.psum_scatter(shared_terms, TP, scatter_dimension=0, tiled=True)[0]
 
     results, sample_gate, sample_up, sample_down = ffn(block, both_all, down_all)
-    mix = mixing(routes, route_weights, core)
-    back = exchange(results.reshape(EXPERTS * NX, 8, 640), ("z", "y", "x"))
-    own, other = combine(back.reshape(EXPERTS * NX * 8, 640), mix, core)
-    other = shift(other, "c", NC, 1)
-    layer_output = (own + other.astype(F32) + shared_sum.astype(F32)).astype(BF)
+    mix = mixing(routes, route_weights, at)
+    back = exchange(results.reshape(EXPERTS, 8, D + 512), FS).reshape(TOK, D + 512)
+    mine, other = combine(back, mix, terms, core)
+    sums = pair_sum(mine, shift(other, "c", NC, 1), x.reshape(1))
+    sums = [sums[0]] + [shift(sums[k], "x", NX, k) for k in range(1, NX)]
+    layer_output = sum(part.astype(F32) for part in sums).astype(BF)
     return (
         layer_output,
         sample_gate.reshape(1, D, 128),

time: 257 us -> 224 us (0.87); the launches traced: 257 us -> 220 us
  waiting for transfers between devices: 152 us -> 117 us
  between operations: 14.4 us -> 1.07 us
  local copies, waits for them, and re-layouts: 5.64 us -> 13 us
  starting transfers between devices: 59.9 us -> 65.9 us
    reduce_scatter x1 -> x0, waiting for transfers between devices: 32.5 us -> none  [layer(): lax.psum_scatter(shared_terms, TP, scatter_dimension=0, tiled=True)[0]]
    ppermute x25 -> x32, starting transfers between devices: 24.6 us -> 33.1 us  [shift(): lax.ppermute(array, axis, [(i, (i + by) % size) for i in range(size)])]
    unnamed x42 -> x62, local copies, waits for them, and re-layouts: 3.45 us -> 10.8 us
    ppermute x25 -> x32, waiting for transfers between devices: 82.3 us -> 79.7 us  [shift(): lax.ppermute(array, axis, [(i, (i + by) % size) for i in range(size)])]
    pallas_call x3 -> x4, Pallas kernels: 14.7 us -> 14.7 us  [the longest x1 10.3 us: ffn(): pl.pallas_call(ffn_kernel, out_shape=(jax.ShapeDtypeStruct((TOK, D + 512)...]
  transfers between devices with their start and end apart: 30 -> 36, of which waited for: 15 -> 20; matrix products, arithmetic and copies ran while one was open for 1% -> 2% of each run, Pallas kernels for 7% -> 3%
where the time goes in v4:
time: 224 us; the launch traced here: 220 us
  waiting for transfers between devices  117 us (52%)
  starting transfers between devices  65.9 us (29%)
  Pallas kernels  21.4 us (10%)
  local copies, waits for them, and re-layouts  13 us (6%)
    ppermute x32, waiting for transfers between devices, shift(): lax.ppermute(array, axis, [(i, (i + by) % size) for i in range(size)])  79.7 us
    all_to_all x4, waiting for transfers between devices, exchange(): return lax.all_to_all(array, axes, split_axis=0, concat_axis=0, tiled=True)  37.5 us
    ppermute x32, starting transfers between devices, shift(): lax.ppermute(array, axis, [(i, (i + by) % size) for i in range(size)])  33.1 us
    all_to_all x4, starting transfers between devices, exchange(): return lax.all_to_all(array, axes, split_axis=0, concat_axis=0, tiled=True)  32.8 us
    unnamed x62, local copies, waits for them, and re-layouts  10.8 us
    pallas_call x1, Pallas kernels, ffn(): pl.pallas_call(ffn_kernel, out_shape=(jax.ShapeDtypeStruct((TOK, D + 512)...  10.3 us
  transfers between devices with their start and end apart: 36, of which 20 were waited for; matrix products, arithmetic and copies ran while one was open for 2% of the time, Pallas kernels for 3%

profile of v4, /device:TPU:16, one launch (start us, length us, event | category | flops | bytes accessed | tf_op | source)
XLA Modules:
  0.0 220.4 jit_solution(3760835685527359417)
XLA Ops:
  0.6 3.8 %round_both.1 = bf16[32,2,64,128]{3,2,1,0:T(8,128)(2,1)} custom-call(f32[1,64]{1,0:T(1,128)} %bitcast.33, f32[32,64,128]{2,1,0:T(8,128)} %gate_ref.1, f32[32,64,128]{2,1,0:T(8,128)} %up_ref.1), custom_call_target="tpu_custom_call" | custom-call | flops 10000000 | bytes 3145728 | tf_op jit(solution)/shard_map/round_both/pallas_call | solution.py:98
  4.4 11.7 %all-to-all-start = ((bf16[32,2,64,128]{3,2,1,0:T(8,128)(2,1)}), bf16[32,2,64,128]{3,2,1,0:T(8,128)(2,1)S(1)}, u32[]{:S(2)}, u32[]{:S(2)}) async-start(bf16[32,2,64,128]{3,2,1,0:T(8,128)(2,1)} %round_both.1), calls=%async_computation | async-start | bytes 2097152 | tf_op jit(solution)/shard_map/all_to_all | solution.py:358
  17.0 27.2 %all-to-all-done.refs_0_ = bf16[32,2,64,128]{3,2,1,0:T(8,128)(2,1)S(1)} async-done(((bf16[32,2,64,128]{3,2,1,0:T(8,128)(2,1)}), bf16[32,2,64,128]{3,2,1,0:T(8,128)(2,1)S(1)}, u32[]{:S(2)}, u32[]{:S(2)}) %all-to-all-start) | async-done | bytes 1048608 | tf_op jit(solution)/shard_map/all_to_all | solution.py:358
  44.2 5.6 %all-to-all-start.1 = ((bf16[32,64,128]{2,1,0:T(8,128)(2,1)}), bf16[32,64,128]{2,1,0:T(8,128)(2,1)}, u32[]{:S(2)}, u32[]{:S(2)}) async-start(bf16[32,64,128]{2,1,0:T(8,128)(2,1)} %convert_element_type.27), calls=%async_computation.1 | async-start | bytes 1048576 | tf_op jit(solution)/shard_map/all_to_all | solution.py:358
  51.4 1.7 collective-permute-start.1
  53.2 2.2 dispatch.1
  55.3 10.3 %all-to-all-done.1.refs_10_ = bf16[32,64,128]{2,1,0:T(8,128)(2,1)} async-done(((bf16[32,64,128]{2,1,0:T(8,128)(2,1)}), bf16[32,64,128]{2,1,0:T(8,128)(2,1)}, u32[]{:S(2)}, u32[]{:S(2)}) %all-to-all-start.1) | async-done | bytes 524320 | tf_op jit(solution)/shard_map/all_to_all | solution.py:358
  65.7 5.6 %all-to-all-start.2 = ((bf16[32,8,2560]{2,1,0:T(8,128)(2,1)}), bf16[32,8,2560]{2,1,0:T(8,128)(2,1)}, u32[]{:S(2)}, u32[]{:S(2)}) async-start(bf16[32,8,2560]{2,1,0:T(8,128)(2,1)} %bitcast.5), calls=%async_computation.2 | async-start | bytes 2621440 | tf_op jit(solution)/shard_map/all_to_all | solution.py:358
  73.0 1.7 collective-permute-start.10
  77.2 10.4 %collective-permute-done.9.refs_11_ = bf16[32,64,128]{2,1,0:T(8,128)(2,1)S(1)} collective-permute-done((bf16[32,64,128]{2,1,0:T(8,128)(2,1)}, bf16[32,64,128]{2,1,0:T(8,128)(2,1)S(1)}, u32[]{:S(2)}, u32[]{:S(2)}) %collective-permute-start.9) | collective-permute-done | bytes 524320 | tf_op jit(solution)/shard_map/ppermute | solution.py:39
  90.4 8.6 %collective-permute-done.2.refs_3_ = bf16[16,2,64,128]{3,2,1,0:T(8,128)(2,1)S(1)} collective-permute-done((bf16[16,2,64,128]{3,2,1,0:T(8,128)(2,1)S(1)}, bf16[16,2,64,128]{3,2,1,0:T(8,128)(2,1)S(1)}, u32[]{:S(2)}, u32[]{:S(2)}) %collective-permute-start.2) | collective-permute-done | bytes 524320 | tf_op jit(solution)/shard_map/ppermute | solution.py:39
  98.9 1.7 collective-permute-done.3.refs_4_
  100.7 3.3 %collective-permute-done.11.refs_13_ = bf16[16,64,128]{2,1,0:T(8,128)(2,1)S(1)} collective-permute-done((bf16[16,64,128]{2,1,0:T(8,128)(2,1)S(1)}, bf16[16,64,128]{2,1,0:T(8,128)(2,1)S(1)}, u32[]{:S(2)}, u32[]{:S(2)}) %collective-permute-start.11) | collective-permute-done | bytes 262176 | tf_op jit(solution)/shard_map/ppermute | solution.py:39
  105.5 6.3 %collective-permute-done.12.refs_14_ = bf16[16,64,128]{2,1,0:T(8,128)(2,1)S(1)} collective-permute-done((bf16[16,64,128]{2,1,0:T(8,128)(2,1)S(1)}, bf16[16,64,128]{2,1,0:T(8,128)(2,1)S(1)}, u32[]{:S(2)}, u32[]{:S(2)}) %collective-permute-start.12) | collective-permute-done | bytes 262176 | tf_op jit(solution)/shard_map/ppermute | solution.py:39
  113.5 1.7 collective-permute-done.17.refs_19_
  117.4 10.3 %ffn.1 = (bf16[256,2560]{1,0:T(8,128)(2,1)}, bf16[32,64,128]{2,1,0:T(8,128)(2,1)}, bf16[32,64,128]{2,1,0:T(8,128)(2,1)}, bf16[32,64,128]{2,1,0:T(8,128)(2,1)}) custom-call(bf16[256,2560]{1,0:T(8,128)(2,1)} %bitcast.6.block_ref, bf16[32,2,64,128]{3,2,1,0:T(8,128)(2,1)} %copy-done.11, bf16[32,2,64,128]{3,2,1,0:T(8,128)(2,1)} %collective-permute-done.refs_1_, ...), custom_call_target="tpu_custom_call" | custom-call | flops 4026531840 | bytes 16777216 | tf_op jit(solution)/shard_map/ffn/pallas_call | solution.py:187
  127.7 9.8 %all-to-all-start.3 = ((bf16[32,8,2560]{2,1,0:T(8,128)(2,1)}), bf16[32,8,2560]{2,1,0:T(8,128)(2,1)S(1)}, u32[]{:S(2)}, u32[]{:S(2)}) async-start(bf16[32,8,2560]{2,1,0:T(8,128)(2,1)} %bitcast.32), calls=%async_computation.3 | async-start | bytes 2621440 | tf_op jit(solution)/shard_map/all_to_all | solution.py:358
  137.7 2.8 %collective-permute-start.18 = (bf16[64,384]{1,0:T(8,128)(2,1)S(1)}, bf16[64,384]{1,0:T(8,128)(2,1)S(1)}, u32[]{:S(2)}, u32[]{:S(2)}) collective-permute-start(bf16[64,384]{1,0:T(8,128)(2,1)S(1)} %pad_maximum_fusion), channel_id=1, source_target_pairs={{0,224},{32,0},{64,32},{96,64},{128,96},{160,128},{192,160},{224,1... | collective-permute-start | bytes 147464 | tf_op jit(solution)/shard_map/ppermute | solution.py:39
  140.6 2.3 %collective-permute-start.19 = (bf16[64,384]{1,0:T(8,128)(2,1)S(1)}, bf16[64,384]{1,0:T(8,128)(2,1)S(1)}, u32[]{:S(2)}, u32[]{:S(2)}) collective-permute-start(bf16[64,384]{1,0:T(8,128)(2,1)S(1)} %pad_maximum_fusion), channel_id=1, source_target_pairs={{0,192},{32,224},{64,0},{96,32},{128,64},{160,96},{192,128},{224,1... | collective-permute-start | bytes 147464 | tf_op jit(solution)/shard_map/ppermute | solution.py:39
  144.3 3.6 %collective-permute-start.21 = (bf16[64,384]{1,0:T(8,128)(2,1)S(1)}, bf16[64,384]{1,0:T(8,128)(2,1)S(1)}, u32[]{:S(2)}, u32[]{:S(2)}) collective-permute-start(bf16[64,384]{1,0:T(8,128)(2,1)S(1)} %pad_maximum_fusion), channel_id=1, source_target_pairs={{0,128},{32,160},{64,192},{96,224},{128,0},{160,32},{192,64},{224,... | collective-permute-start | bytes 147464 | tf_op jit(solution)/shard_map/ppermute | solution.py:39
  148.1 23.3 %collective-permute-done.18 = bf16[64,384]{1,0:T(8,128)(2,1)S(1)} collective-permute-done((bf16[64,384]{1,0:T(8,128)(2,1)S(1)}, bf16[64,384]{1,0:T(8,128)(2,1)S(1)}, u32[]{:S(2)}, u32[]{:S(2)}) %collective-permute-start.18) | collective-permute-done | bytes 49184 | tf_op jit(solution)/shard_map/ppermute | solution.py:39
  172.2 2.0 collective-permute-done.19
  174.1 2.7 %collective-permute-start.24 = (bf16[64,384]{1,0:T(8,128)(2,1)S(1)}, bf16[64,384]{1,0:T(8,128)(2,1)S(1)}, u32[]{:S(2)}, u32[]{:S(2)}) collective-permute-start(bf16[64,384]{1,0:T(8,128)(2,1)S(1)} %pad_maximum_fusion), channel_id=1, source_target_pairs={{0,32},{32,64},{64,96},{96,128},{128,160},{160,192},{192,224},{224... | collective-permute-start | bytes 147464 | tf_op jit(solution)/shard_map/ppermute | solution.py:39
  180.0 2.7 %collective-permute-start.26 = (bf16[8,64,384]{2,1,0:T(8,128)(2,1)S(1)}, bf16[8,64,384]{2,1,0:T(8,128)(2,1)S(1)}, u32[]{:S(2)}, u32[]{:S(2)}) collective-permute-start(bf16[8,64,384]{2,1,0:T(8,128)(2,1)S(1)} %bitcast_dynamic-update-slice_fusion.refs_0_), channel_id=1, source_target_pairs={{0,16},{8,24},{16,0},{24,8},{1,17},{9,25},{17,1},{25,9},{2,18},{10... | collective-permute-start | bytes 1179656 | tf_op jit(solution)/shard_map/ppermute | solution.py:39
  188.5 2.4 %collective-permute-done.25.refs_1_ = bf16[8,64,384]{2,1,0:T(8,128)(2,1)S(1)} collective-permute-done((bf16[8,64,384]{2,1,0:T(8,128)(2,1)S(1)}, bf16[8,64,384]{2,1,0:T(8,128)(2,1)S(1)}, u32[]{:S(2)}, u32[]{:S(2)}) %collective-permute-start.25) | collective-permute-done | bytes 393248 | tf_op jit(solution)/shard_map/ppermute | solution.py:39
  191.0 2.0 collective-permute-done.26.refs_2_
  193.0 4.2 %collective-permute-done.27.refs_3_ = bf16[8,64,384]{2,1,0:T(8,128)(2,1)} collective-permute-done((bf16[8,64,384]{2,1,0:T(8,128)(2,1)S(1)}, bf16[8,64,384]{2,1,0:T(8,128)(2,1)}, u32[]{:S(2)}, u32[]{:S(2)}) %collective-permute-start.27) | collective-permute-done | bytes 393248 | tf_op jit(solution)/shard_map/ppermute | solution.py:39
  197.2 2.9 %shared_expert.1 = (bf16[256,2048]{1,0:T(8,128)(2,1)S(1)}, bf16[2048,128]{1,0:T(8,128)(2,1)}, bf16[2048,128]{1,0:T(8,128)(2,1)}, bf16[2048,128]{1,0:T(8,128)(2,1)}) custom-call(s32[2]{0:T(128)S(1)} %pad_add_fusion.at_ref, bf16[256,2048]{1,0:T(8,128)(2,1)S(1)} %get-tuple-element.41.normed_ref, ...), custom_call_target="tpu_custom_call" | custom-call | flops 402653184 | bytes 6291456 | tf_op jit(solution)/shard_map/shared_expert/pallas_call | solution.py:324
  205.6 1.9 collective-permute-done.28.swapped_ref
  207.6 2.8 %collective-permute-start.31 = (bf16[256,256]{1,0:T(8,128)(2,1)S(1)}, bf16[256,256]{1,0:T(8,128)(2,1)S(1)}, u32[]{:S(2)}, u32[]{:S(2)}) collective-permute-start(bf16[256,256]{1,0:T(8,128)(2,1)S(1)} %get-tuple-element.48), channel_id=1, source_target_pairs={{0,6},{2,0},{4,2},{6,4},{1,7},{3,1},{5,3},{7,5},{8,14},{10,8},{12,... | collective-permute-start | bytes 393224 | tf_op jit(solution)/shard_map/ppermute | solution.py:39
  211.4 4.9 %collective-permute-done.31 = bf16[256,256]{1,0:T(8,128)(2,1)S(1)} collective-permute-done((bf16[256,256]{1,0:T(8,128)(2,1)S(1)}, bf16[256,256]{1,0:T(8,128)(2,1)S(1)}, u32[]{:S(2)}, u32[]{:S(2)}) %collective-permute-start.31) | collective-permute-done | bytes 131104 | tf_op jit(solution)/shard_map/ppermute | solution.py:39
  216.3 2.0 collective-permute-done.30
  (121 shorter events, 34.5 us)
Async XLA Ops:
  4.4 39.8 %all-to-all-start = ((bf16[32,2,64,128]{3,2,1,0:T(8,128)(2,1)}), bf16[32,2,64,128]{3,2,1,0:T(8,128)(2,1)S(1)}, u32[]{:S(2)}, u32[]{:S(2)}) async-start(bf16[32,2,64,128]{3,2,1,0:T(8,128)(2,1)} %round_both.1), calls=%async_computation | async-start | bytes 2097152 | tf_op jit(solution)/shard_map/all_to_all | solution.py:358
  44.2 21.5 %all-to-all-start.1 = ((bf16[32,64,128]{2,1,0:T(8,128)(2,1)}), bf16[32,64,128]{2,1,0:T(8,128)(2,1)}, u32[]{:S(2)}, u32[]{:S(2)}) async-start(bf16[32,64,128]{2,1,0:T(8,128)(2,1)} %convert_element_type.27), calls=%async_computation.1 | async-start | bytes 1048576 | tf_op jit(solution)/shard_map/all_to_all | solution.py:358
  49.8 24.9 %collective-permute-start = (bf16[32,2,64,128]{3,2,1,0:T(8,128)(2,1)S(1)}, bf16[32,2,64,128]{3,2,1,0:T(8,128)(2,1)}, u32[]{:S(2)}, u32[]{:S(2)}) collective-permute-start(bf16[32,2,64,128]{3,2,1,0:T(8,128)(2,1)S(1)} %all-to-all-done.refs_0_), channel_id=1, source_target_pairs={{0,2},{2,4},{4,6},{6,0},{1,3},{3,5},{5,7},{7,1},{8,10},{10,12},{12... | collective-permute-start | bytes 3145736 | tf_op jit(solution)/shard_map/ppermute | solution.py:39
  51.4 24.4 %collective-permute-start.1 = (bf16[32,2,64,128]{3,2,1,0:T(8,128)(2,1)S(1)}, bf16[32,2,64,128]{3,2,1,0:T(8,128)(2,1)}, u32[]{:S(2)}, u32[]{:S(2)}) collective-permute-start(bf16[32,2,64,128]{3,2,1,0:T(8,128)(2,1)S(1)} %all-to-all-done.refs_0_), channel_id=1, source_target_pairs={{0,6},{2,0},{4,2},{6,4},{1,7},{3,1},{5,3},{7,5},{8,14},{10,8},{12,... | collective-permute-start | bytes 3145736 | tf_op jit(solution)/shard_map/ppermute | solution.py:39
  65.7 51.7 %all-to-all-start.2 = ((bf16[32,8,2560]{2,1,0:T(8,128)(2,1)}), bf16[32,8,2560]{2,1,0:T(8,128)(2,1)}, u32[]{:S(2)}, u32[]{:S(2)}) async-start(bf16[32,8,2560]{2,1,0:T(8,128)(2,1)} %bitcast.5), calls=%async_computation.2 | async-start | bytes 2621440 | tf_op jit(solution)/shard_map/all_to_all | solution.py:358
  71.3 18.0 %collective-permute-start.4 = (bf16[32,2,64,128]{3,2,1,0:T(8,128)(2,1)S(1)}, bf16[32,2,64,128]{3,2,1,0:T(8,128)(2,1)S(1)}, u32[]{:S(2)}, u32[]{:S(2)}) collective-permute-start(bf16[32,2,64,128]{3,2,1,0:T(8,128)(2,1)S(1)} %all-to-all-done.refs_0_), channel_id=1, source_target_pairs={{0,1},{1,0},{2,3},{3,2},{4,5},{5,4},{6,7},{7,6},{8,9},{9,8},{10,11... | collective-permute-start | bytes 3145736 | tf_op jit(solution)/shard_map/ppermute | solution.py:39
  71.4 16.3 %collective-permute-start.9 = (bf16[32,64,128]{2,1,0:T(8,128)(2,1)}, bf16[32,64,128]{2,1,0:T(8,128)(2,1)S(1)}, u32[]{:S(2)}, u32[]{:S(2)}) collective-permute-start(bf16[32,64,128]{2,1,0:T(8,128)(2,1)} %all-to-all-done.1.refs_10_), channel_id=1, source_target_pairs={{0,2},{2,4},{4,6},{6,0},{1,3},{3,5},{5,7},{7,1},{8,10},{10,12},{12... | collective-permute-start | bytes 1572872 | tf_op jit(solution)/shard_map/ppermute | solution.py:39
  73.0 16.9 %collective-permute-start.10 = (bf16[32,64,128]{2,1,0:T(8,128)(2,1)}, bf16[32,64,128]{2,1,0:T(8,128)(2,1)S(1)}, u32[]{:S(2)}, u32[]{:S(2)}) collective-permute-start(bf16[32,64,128]{2,1,0:T(8,128)(2,1)} %all-to-all-done.1.refs_10_), channel_id=1, source_target_pairs={{0,6},{2,0},{4,2},{6,4},{1,7},{3,1},{5,3},{7,5},{8,14},{10,8},{12,... | collective-permute-start | bytes 1572872 | tf_op jit(solution)/shard_map/ppermute | solution.py:39
  74.7 15.1 %collective-permute-start.13 = (bf16[32,64,128]{2,1,0:T(8,128)(2,1)}, bf16[32,64,128]{2,1,0:T(8,128)(2,1)S(1)}, u32[]{:S(2)}, u32[]{:S(2)}) collective-permute-start(bf16[32,64,128]{2,1,0:T(8,128)(2,1)} %all-to-all-done.1.refs_10_), channel_id=1, source_target_pairs={{0,1},{1,0},{2,3},{3,2},{4,5},{5,4},{6,7},{7,6},{8,9},{9,8},{10,11... | collective-permute-start | bytes 1572872 | tf_op jit(solution)/shard_map/ppermute | solution.py:39
  75.8 23.1 %collective-permute-start.2 = (bf16[16,2,64,128]{3,2,1,0:T(8,128)(2,1)S(1)}, bf16[16,2,64,128]{3,2,1,0:T(8,128)(2,1)S(1)}, u32[]{:S(2)}, u32[]{:S(2)}) collective-permute-start(bf16[16,2,64,128]{3,2,1,0:T(8,128)(2,1)S(1)} %slice.16), channel_id=1, source_target_pairs={{0,2},{2,4},{4,6},{6,0},{1,3},{3,5},{5,7},{7,1},{8,10},{10,12},{12... | collective-permute-start | bytes 1572872 | tf_op jit(solution)/shard_map/ppermute | solution.py:39
  87.7 12.9 %collective-permute-start.3 = (bf16[16,2,64,128]{3,2,1,0:T(8,128)(2,1)S(1)}, bf16[16,2,64,128]{3,2,1,0:T(8,128)(2,1)S(1)}, u32[]{:S(2)}, u32[]{:S(2)}) collective-permute-start(bf16[16,2,64,128]{3,2,1,0:T(8,128)(2,1)S(1)} %slice.17), channel_id=1, source_target_pairs={{0,6},{2,0},{4,2},{6,4},{1,7},{3,1},{5,3},{7,5},{8,14},{10,8},{12,... | collective-permute-start | bytes 1572872 | tf_op jit(solution)/shard_map/ppermute | solution.py:39
  89.3 14.7 %collective-permute-start.11 = (bf16[16,64,128]{2,1,0:T(8,128)(2,1)S(1)}, bf16[16,64,128]{2,1,0:T(8,128)(2,1)S(1)}, u32[]{:S(2)}, u32[]{:S(2)}) collective-permute-start(bf16[16,64,128]{2,1,0:T(8,128)(2,1)S(1)} %slice.18), channel_id=1, source_target_pairs={{0,2},{2,4},{4,6},{6,0},{1,3},{3,5},{5,7},{7,1},{8,10},{10,12},{12... | collective-permute-start | bytes 786440 | tf_op jit(solution)/shard_map/ppermute | solution.py:39
  89.8 22.0 %collective-permute-start.14 = (bf16[32,64,128]{2,1,0:T(8,128)(2,1)S(1)}, bf16[32,64,128]{2,1,0:T(8,128)(2,1)S(1)}, u32[]{:S(2)}, u32[]{:S(2)}) collective-permute-start(bf16[32,64,128]{2,1,0:T(8,128)(2,1)S(1)} %collective-permute-done.9.refs_11_), channel_id=1, source_target_pairs={{0,1},{1,0},{2,3},{3,2},{4,5},{5,4},{6,7},{7,6},{8,9},{9,8},{10,11... | collective-permute-start | bytes 1572872 | tf_op jit(solution)/shard_map/ppermute | solution.py:39
  89.9 22.5 %collective-permute-start.15 = (bf16[32,64,128]{2,1,0:T(8,128)(2,1)S(1)}, bf16[32,64,128]{2,1,0:T(8,128)(2,1)S(1)}, u32[]{:S(2)}, u32[]{:S(2)}) collective-permute-start(bf16[32,64,128]{2,1,0:T(8,128)(2,1)S(1)} %collective-permute-done.10.refs_12_), channel_id=1, source_target_pairs={{0,1},{1,0},{2,3},{3,2},{4,5},{5,4},{6,7},{7,6},{8,9},{9,8},{10,11... | collective-permute-start | bytes 1572872 | tf_op jit(solution)/shard_map/ppermute | solution.py:39
  98.9 16.4 %collective-permute-start.5 = (bf16[32,2,64,128]{3,2,1,0:T(8,128)(2,1)}, bf16[32,2,64,128]{3,2,1,0:T(8,128)(2,1)S(1)}, u32[]{:S(2)}, u32[]{:S(2)}) collective-permute-start(bf16[32,2,64,128]{3,2,1,0:T(8,128)(2,1)} %collective-permute-done.refs_1_), channel_id=1, source_target_pairs={{0,1},{1,0},{2,3},{3,2},{4,5},{5,4},{6,7},{7,6},{8,9},{9,8},{10,11... | collective-permute-start | bytes 3145736 | tf_op jit(solution)/shard_map/ppermute | solution.py:39
  100.6 16.7 %collective-permute-start.6 = (bf16[32,2,64,128]{3,2,1,0:T(8,128)(2,1)}, bf16[32,2,64,128]{3,2,1,0:T(8,128)(2,1)}, u32[]{:S(2)}, u32[]{:S(2)}) collective-permute-start(bf16[32,2,64,128]{3,2,1,0:T(8,128)(2,1)} %collective-permute-done.1.refs_2_), channel_id=1, source_target_pairs={{0,1},{1,0},{2,3},{3,2},{4,5},{5,4},{6,7},{7,6},{8,9},{9,8},{10,11... | collective-permute-start | bytes 3145736 | tf_op jit(solution)/shard_map/ppermute | solution.py:39
  104.0 7.9 %collective-permute-start.12 = (bf16[16,64,128]{2,1,0:T(8,128)(2,1)S(1)}, bf16[16,64,128]{2,1,0:T(8,128)(2,1)S(1)}, u32[]{:S(2)}, u32[]{:S(2)}) collective-permute-start(bf16[16,64,128]{2,1,0:T(8,128)(2,1)S(1)} %slice.19), channel_id=1, source_target_pairs={{0,6},{2,0},{4,2},{6,4},{1,7},{3,1},{5,3},{7,5},{8,14},{10,8},{12,... | collective-permute-start | bytes 786440 | tf_op jit(solution)/shard_map/ppermute | solution.py:39
  111.9 3.4 %collective-permute-start.7 = (bf16[16,2,64,128]{3,2,1,0:T(8,128)(2,1)S(1)}, bf16[16,2,64,128]{3,2,1,0:T(8,128)(2,1)S(1)}, u32[]{:S(2)}, u32[]{:S(2)}) collective-permute-start(bf16[16,2,64,128]{3,2,1,0:T(8,128)(2,1)S(1)} %collective-permute-done.2.refs_3_), channel_id=1, source_target_pairs={{0,1},{1,0},{2,3},{3,2},{4,5},{5,4},{6,7},{7,6},{8,9},{9,8},{10,11... | collective-permute-start | bytes 1572872 | tf_op jit(solution)/shard_map/ppermute | solution.py:39
  127.7 73.3 %all-to-all-start.3 = ((bf16[32,8,2560]{2,1,0:T(8,128)(2,1)}), bf16[32,8,2560]{2,1,0:T(8,128)(2,1)S(1)}, u32[]{:S(2)}, u32[]{:S(2)}) async-start(bf16[32,8,2560]{2,1,0:T(8,128)(2,1)} %bitcast.32), calls=%async_computation.3 | async-start | bytes 2621440 | tf_op jit(solution)/shard_map/all_to_all | solution.py:358
  137.7 33.8 %collective-permute-start.18 = (bf16[64,384]{1,0:T(8,128)(2,1)S(1)}, bf16[64,384]{1,0:T(8,128)(2,1)S(1)}, u32[]{:S(2)}, u32[]{:S(2)}) collective-permute-start(bf16[64,384]{1,0:T(8,128)(2,1)S(1)} %pad_maximum_fusion), channel_id=1, source_target_pairs={{0,224},{32,0},{64,32},{96,64},{128,96},{160,128},{192,160},{224,1... | collective-permute-start | bytes 147464 | tf_op jit(solution)/shard_map/ppermute | solution.py:39
  140.6 33.6 %collective-permute-start.19 = (bf16[64,384]{1,0:T(8,128)(2,1)S(1)}, bf16[64,384]{1,0:T(8,128)(2,1)S(1)}, u32[]{:S(2)}, u32[]{:S(2)}) collective-permute-start(bf16[64,384]{1,0:T(8,128)(2,1)S(1)} %pad_maximum_fusion), channel_id=1, source_target_pairs={{0,192},{32,224},{64,0},{96,32},{128,64},{160,96},{192,128},{224,1... | collective-permute-start | bytes 147464 | tf_op jit(solution)/shard_map/ppermute | solution.py:39
  142.9 33.9 %collective-permute-start.20 = (bf16[64,384]{1,0:T(8,128)(2,1)S(1)}, bf16[64,384]{1,0:T(8,128)(2,1)S(1)}, u32[]{:S(2)}, u32[]{:S(2)}) collective-permute-start(bf16[64,384]{1,0:T(8,128)(2,1)S(1)} %pad_maximum_fusion), channel_id=1, source_target_pairs={{0,160},{32,192},{64,224},{96,0},{128,32},{160,64},{192,96},{224,1... | collective-permute-start | bytes 147464 | tf_op jit(solution)/shard_map/ppermute | solution.py:39
  144.3 32.5 %collective-permute-start.21 = (bf16[64,384]{1,0:T(8,128)(2,1)S(1)}, bf16[64,384]{1,0:T(8,128)(2,1)S(1)}, u32[]{:S(2)}, u32[]{:S(2)}) collective-permute-start(bf16[64,384]{1,0:T(8,128)(2,1)S(1)} %pad_maximum_fusion), channel_id=1, source_target_pairs={{0,128},{32,160},{64,192},{96,224},{128,0},{160,32},{192,64},{224,... | collective-permute-start | bytes 147464 | tf_op jit(solution)/shard_map/ppermute | solution.py:39
  147.9 28.9 %collective-permute-start.22 = (bf16[64,384]{1,0:T(8,128)(2,1)S(1)}, bf16[64,384]{1,0:T(8,128)(2,1)S(1)}, u32[]{:S(2)}, u32[]{:S(2)}) collective-permute-start(bf16[64,384]{1,0:T(8,128)(2,1)S(1)} %pad_maximum_fusion), channel_id=1, source_target_pairs={{0,96},{32,128},{64,160},{96,192},{128,224},{160,0},{192,32},{224,... | collective-permute-start | bytes 147464 | tf_op jit(solution)/shard_map/ppermute | solution.py:39
  171.5 6.4 %collective-permute-start.23 = (bf16[64,384]{1,0:T(8,128)(2,1)S(1)}, bf16[64,384]{1,0:T(8,128)(2,1)S(1)}, u32[]{:S(2)}, u32[]{:S(2)}) collective-permute-start(bf16[64,384]{1,0:T(8,128)(2,1)S(1)} %pad_maximum_fusion), channel_id=1, source_target_pairs={{0,64},{32,96},{64,128},{96,160},{128,192},{160,224},{192,0},{224,... | collective-permute-start | bytes 147464 | tf_op jit(solution)/shard_map/ppermute | solution.py:39
  174.1 5.3 %collective-permute-start.24 = (bf16[64,384]{1,0:T(8,128)(2,1)S(1)}, bf16[64,384]{1,0:T(8,128)(2,1)S(1)}, u32[]{:S(2)}, u32[]{:S(2)}) collective-permute-start(bf16[64,384]{1,0:T(8,128)(2,1)S(1)} %pad_maximum_fusion), channel_id=1, source_target_pairs={{0,32},{32,64},{64,96},{96,128},{128,160},{160,192},{192,224},{224... | collective-permute-start | bytes 147464 | tf_op jit(solution)/shard_map/ppermute | solution.py:39
  179.4 11.5 %collective-permute-start.25 = (bf16[8,64,384]{2,1,0:T(8,128)(2,1)S(1)}, bf16[8,64,384]{2,1,0:T(8,128)(2,1)S(1)}, u32[]{:S(2)}, u32[]{:S(2)}) collective-permute-start(bf16[8,64,384]{2,1,0:T(8,128)(2,1)S(1)} %bitcast_dynamic-update-slice_fusion.refs_0_), channel_id=1, source_target_pairs={{0,24},{8,0},{16,8},{24,16},{1,25},{9,1},{17,9},{25,17},{2,26},{10... | collective-permute-start | bytes 1179656 | tf_op jit(solution)/shard_map/ppermute | solution.py:39
  180.0 13.0 %collective-permute-start.26 = (bf16[8,64,384]{2,1,0:T(8,128)(2,1)S(1)}, bf16[8,64,384]{2,1,0:T(8,128)(2,1)S(1)}, u32[]{:S(2)}, u32[]{:S(2)}) collective-permute-start(bf16[8,64,384]{2,1,0:T(8,128)(2,1)S(1)} %bitcast_dynamic-update-slice_fusion.refs_0_), channel_id=1, source_target_pairs={{0,16},{8,24},{16,0},{24,8},{1,17},{9,25},{17,1},{25,9},{2,18},{10... | collective-permute-start | bytes 1179656 | tf_op jit(solution)/shard_map/ppermute | solution.py:39
  182.7 14.4 %collective-permute-start.27 = (bf16[8,64,384]{2,1,0:T(8,128)(2,1)S(1)}, bf16[8,64,384]{2,1,0:T(8,128)(2,1)}, u32[]{:S(2)}, u32[]{:S(2)}) collective-permute-start(bf16[8,64,384]{2,1,0:T(8,128)(2,1)S(1)} %bitcast_dynamic-update-slice_fusion.refs_0_), channel_id=1, source_target_pairs={{0,8},{8,16},{16,24},{24,0},{1,9},{9,17},{17,25},{25,1},{2,10},{10... | collective-permute-start | bytes 1179656 | tf_op jit(solution)/shard_map/ppermute | solution.py:39
  207.6 8.7 %collective-permute-start.31 = (bf16[256,256]{1,0:T(8,128)(2,1)S(1)}, bf16[256,256]{1,0:T(8,128)(2,1)S(1)}, u32[]{:S(2)}, u32[]{:S(2)}) collective-permute-start(bf16[256,256]{1,0:T(8,128)(2,1)S(1)} %get-tuple-element.48), channel_id=1, source_target_pairs={{0,6},{2,0},{4,2},{6,4},{1,7},{3,1},{5,3},{7,5},{8,14},{10,8},{12,... | collective-permute-start | bytes 393224 | tf_op jit(solution)/shard_map/ppermute | solution.py:39
  210.4 7.9 %collective-permute-start.30 = (bf16[256,256]{1,0:T(8,128)(2,1)S(1)}, bf16[256,256]{1,0:T(8,128)(2,1)S(1)}, u32[]{:S(2)}, u32[]{:S(2)}) collective-permute-start(bf16[256,256]{1,0:T(8,128)(2,1)S(1)} %get-tuple-element.47), channel_id=1, source_target_pairs={{0,4},{2,6},{4,0},{6,2},{1,5},{3,7},{5,1},{7,3},{8,12},{10,14},{12... | collective-permute-start | bytes 393224 | tf_op jit(solution)/shard_map/ppermute | solution.py:39
  210.4 9.3 %collective-permute-start.29 = (bf16[256,256]{1,0:T(8,128)(2,1)S(1)}, bf16[256,256]{1,0:T(8,128)(2,1)S(1)}, u32[]{:S(2)}, u32[]{:S(2)}) collective-permute-start(bf16[256,256]{1,0:T(8,128)(2,1)S(1)} %get-tuple-element.46), channel_id=1, source_target_pairs={{0,2},{2,4},{4,6},{6,0},{1,3},{3,5},{5,7},{7,1},{8,10},{10,12},{12... | collective-permute-start | bytes 393224 | tf_op jit(solution)/shard_map/ppermute | solution.py:39
  (31 other events, 354.6 us)

commit v5 on v2

--- a/solution.py
+++ b/solution.py
@@ -289,46 +289,67 @@
             pltpu.VMEM((TOK, LANES), BF),
             pltpu.SemaphoreType.DMA((2,)),
         ],
-        compiler_params=pltpu.CompilerParams(vmem_limit_bytes=24 << 20),
+        compiler_params=pltpu.CompilerParams(vmem_limit_bytes=52 << 20),
         cost_estimate=pl.CostEstimate(flops=10**9, bytes_accessed=4 << 20, transcendentals=0),
         name="combine",
     )(core, back, *mix)
 
 
-Z_ORDER = (0, 4, 2, 6, 1, 5, 3, 7)
-
-
 def shared_kernel(at_ref, normed_ref, *refs):
-    block_refs, terms_ref, common_refs = refs[:NY], refs[NY], refs[NY + 1 :]
-    z, y = at_ref[0], at_ref[1]
+    block_refs, mine_ref, other_ref = refs[:NY], refs[NY], refs[NY + 1]
+    common_refs = refs[NY + 2 :]
+    z, y, core = at_ref[0], at_ref[1], at_ref[2]
     for dy in range(NY):
         for dz in range(NZ):
-            row = ((z + Z_ORDER[dz]) % NZ * NY + (y + dy) % NY) * 64
+            row = ((z + dz) % NZ * NY + (y + dy) % NY) * 64
             part = pl.ds(pl.multiple_of(row, 64), 64)
             for n in range(3):
                 common_refs[n][part, :] = block_refs[dy][dz, :, n * 128 : (n + 1) * 128]
-    normed = normed_ref[...]
     both = jnp.concatenate([common_refs[0][...], common_refs[1][...]], axis=1)
-    act = dot(normed, both)
+    act = dot(normed_ref[...], both)
     gate, up = act[:, 0:128], act[:, 128:256]
     hidden = (gate / (1.0 + jnp.exp(-gate)) * up).astype(BF)
-    for n in range(NX * NC):
-        terms_ref[n] = dot_t(hidden, common_refs[2][n * 256 : (n + 1) * 256, :]).astype(BF)
+    for x in range(NX):
+        term = dot_t(hidden, common_refs[2][x * 512 : (x + 1) * 512, :])
+        left, right = term[:, :256], term[:, 256:]
+        mine_ref[x] = jnp.where(core == 0, left, right).astype(BF)
+        other_ref[x] = jnp.where(core == 0, right, left).astype(BF)
 
 
 def shared_expert(normed, blocks, at):
     shape = jax.ShapeDtypeStruct((D, 128), BF)
+    terms = jax.ShapeDtypeStruct((NX, TOK, 256), BF)
     return pl.pallas_call(
         shared_kernel,
-        out_shape=(jax.ShapeDtypeStruct((NX * NC, TOK, 256), BF), shape, shape, shape),
+        out_shape=(terms, terms, shape, shape, shape),
         in_specs=[SMEM] + [VMEM] * (1 + NY),
-        out_specs=(VMEM,) * 4,
+        out_specs=(VMEM,) * 5,
         compiler_params=pltpu.CompilerParams(vmem_limit_bytes=24 << 20),
         cost_estimate=pl.CostEstimate(
             flops=6 * TOK * D * 128, bytes_accessed=6 << 20, transcendentals=TOK * 128
         ),
         name="shared_expert",
     )(at, normed, *blocks)
+
+
+def pair_kernel(at_ref, mine_ref, swapped_ref, *out_refs):
+    for dx in range(NX):
+        x = (at_ref[0] + dx) % NX
+        total = mine_ref[x].astype(F32) + swapped_ref[x].astype(F32)
+        out_refs[dx][...] = total.astype(BF)
+
+
+def pair_sum(mine, swapped, at):
+    shape = jax.ShapeDtypeStruct((TOK, 256), BF)
+    return pl.pallas_call(
+        pair_kernel,
+        out_shape=(shape,) * NX,
+        in_specs=[SMEM, VMEM, VMEM],
+        out_specs=(VMEM,) * NX,
+        compiler_params=pltpu.CompilerParams(vmem_limit_bytes=8 << 20),
+        cost_estimate=pl.CostEstimate(flops=10**6, bytes_accessed=2 << 20, transcendentals=0),
+        name="pair_sum",
+    )(at, mine, swapped)
 
 
 def exchange(array, axes):
@@ -371,9 +392,8 @@
         ],
         axis=1,
     )
-    column = shared[None]
-    for k in (4, 2, 1):
-        column = jnp.concatenate([column, shift(column, "z", NZ, -k)])
+    column = [shared] + [shift(shared, "z", NZ, -k) for k in range(1, NZ)]
+    column = jnp.stack(column)
     blocks = [column] + [shift(column, "y", NY, -k) for k in range(1, NY)]
 
     both_in = round_both(norm_gain, expert_gate, expert_up)
@@ -397,17 +417,20 @@
     both_all += [shift(piece, "c", NC, 1) for piece in both_all]
     down_all += [shift(piece, "c", NC, 1) for piece in down_all]
 
-    shared_terms, common_gate, common_up, common_down = shared_expert(
-        normed, blocks, jnp.stack([z, y])
+    mine, other, common_gate, common_up, common_down = shared_expert(
+        normed, blocks, jnp.stack([z, y, c])
     )
-    shared_sum = lax.psum_scatter(shared_terms, TP, scatter_dimension=0, tiled=True)[0]
+    swapped = shift(other, "c", NC, 1)
+    sums = pair_sum(mine, swapped, x.reshape(1))
+    sums = [sums[0]] + [shift(sums[k], "x", NX, k) for k in range(1, NX)]
 
     results, sample_gate, sample_up, sample_down = ffn(block, both_all, down_all)
     mix = mixing(routes, route_weights, core)
     back = exchange(results.reshape(EXPERTS * NX, 8, 640), ("z", "y", "x"))
     own, other = combine(back.reshape(EXPERTS * NX * 8, 640), mix, core)
     other = shift(other, "c", NC, 1)
-    layer_output = (own + other.astype(F32) + shared_sum.astype(F32)).astype(BF)
+    shared_sum = sum(part.astype(F32) for part in sums)
+    layer_output = (own + other.astype(F32) + shared_sum).astype(BF)
     return (
         layer_output,
         sample_gate.reshape(1, D, 128),

time: 257 us -> 222 us (0.86); the launches traced: 257 us -> 218 us
  waiting for transfers between devices: 152 us -> 116 us
  between operations: 14.4 us -> 1.04 us
  starting transfers between devices: 59.9 us -> 72 us
    reduce_scatter x1 -> x0, waiting for transfers between devices: 32.5 us -> none  [layer(): lax.psum_scatter(shared_terms, TP, scatter_dimension=0, tiled=True)[0]]
    ppermute x25 -> x33, starting transfers between devices: 24.6 us -> 36 us  [shift(): lax.ppermute(array, axis, [(i, (i + by) % size) for i in range(size)])]
    ppermute x25 -> x33, waiting for transfers between devices: 82.3 us -> 78.5 us  [shift(): lax.ppermute(array, axis, [(i, (i + by) % size) for i in range(size)])]
  transfers between devices with their start and end apart: 30 -> 37, of which waited for: 15 -> 15; matrix products, arithmetic and copies ran while one was open for 1% -> 2% of each run, Pallas kernels for 7% -> 9%
where the time goes in v5:
time: 222 us; the launch traced here: 218 us
  waiting for transfers between devices  116 us (52%)
  starting transfers between devices  72 us (32%)
  Pallas kernels  22.9 us (10%)
  local copies, waits for them, and re-layouts  4.46 us (2%)
    ppermute x33, waiting for transfers between devices, shift(): lax.ppermute(array, axis, [(i, (i + by) % size) for i in range(size)])  78.5 us
    all_to_all x4, waiting for transfers between devices, exchange(): return lax.all_to_all(array, axes, split_axis=0, concat_axis=0, tiled=True)  37.5 us
    all_to_all x4, starting transfers between devices, exchange(): return lax.all_to_all(array, axes, split_axis=0, concat_axis=0, tiled=True)  36 us
    ppermute x33, starting transfers between devices, shift(): lax.ppermute(array, axis, [(i, (i + by) % size) for i in range(size)])  36 us
    pallas_call x1, Pallas kernels, ffn(): pl.pallas_call(ffn_kernel, out_shape=(jax.ShapeDtypeStruct((EXPERTS, NX,...  10.5 us
  transfers between devices with their start and end apart: 37, of which 15 were waited for; matrix products, arithmetic and copies ran while one was open for 2% of the time, Pallas kernels for 9%

profile of v5, /device:TPU:16, one launch (start us, length us, event | category | flops | bytes accessed | tf_op | source)
XLA Modules:
  0.0 218.2 jit_solution(3407240422998992601)
XLA Ops:
  0.6 3.8 %round_both.1 = bf16[32,2,64,128]{3,2,1,0:T(8,128)(2,1)} custom-call(f32[1,64]{1,0:T(1,128)} %bitcast.32, f32[32,64,128]{2,1,0:T(8,128)} %gate_ref.1, f32[32,64,128]{2,1,0:T(8,128)} %up_ref.1), custom_call_target="tpu_custom_call" | custom-call | flops 10000000 | bytes 3145728 | tf_op jit(solution)/shard_map/round_both/pallas_call | solution.py:98
  4.4 11.7 %all-to-all-start = ((bf16[32,2,64,128]{3,2,1,0:T(8,128)(2,1)}), bf16[32,2,64,128]{3,2,1,0:T(8,128)(2,1)S(1)}, u32[]{:S(2)}, u32[]{:S(2)}) async-start(bf16[32,2,64,128]{3,2,1,0:T(8,128)(2,1)} %round_both.1), calls=%async_computation | async-start | bytes 2097152 | tf_op jit(solution)/shard_map/all_to_all | solution.py:356
  17.0 27.2 %all-to-all-done.refs_0_ = bf16[32,2,64,128]{3,2,1,0:T(8,128)(2,1)S(1)} async-done(((bf16[32,2,64,128]{3,2,1,0:T(8,128)(2,1)}), bf16[32,2,64,128]{3,2,1,0:T(8,128)(2,1)S(1)}, u32[]{:S(2)}, u32[]{:S(2)}) %all-to-all-start) | async-done | bytes 1048608 | tf_op jit(solution)/shard_map/all_to_all | solution.py:356
  44.2 5.6 %all-to-all-start.1 = ((bf16[32,64,128]{2,1,0:T(8,128)(2,1)}), bf16[32,64,128]{2,1,0:T(8,128)(2,1)}, u32[]{:S(2)}, u32[]{:S(2)}) async-start(bf16[32,64,128]{2,1,0:T(8,128)(2,1)} %convert_element_type.30), calls=%async_computation.1 | async-start | bytes 1048576 | tf_op jit(solution)/shard_map/all_to_all | solution.py:356
  51.4 1.7 collective-permute-start.1
  53.1 2.2 %dispatch.1 = (bf16[256,2560]{1,0:T(8,128)(2,1)}, bf16[256,2048]{1,0:T(8,128)(2,1)S(1)}) custom-call(s32[1]{0:T(128)} %bitcast.1.at_ref, bf16[256,2048]{1,0:T(8,128)(2,1)S(1)} %copy-done.1, s32[6,256]{1,0:T(8,128)S(1)} %bitcast.30), custom_call_target="tpu_custom_call" | custom-call | flops 1000000000 | bytes 4194304 | tf_op jit(solution)/shard_map/dispatch/pallas_call | solution.py:75
  55.3 10.3 %all-to-all-done.1.refs_10_ = bf16[32,64,128]{2,1,0:T(8,128)(2,1)} async-done(((bf16[32,64,128]{2,1,0:T(8,128)(2,1)}), bf16[32,64,128]{2,1,0:T(8,128)(2,1)}, u32[]{:S(2)}, u32[]{:S(2)}) %all-to-all-start.1) | async-done | bytes 524320 | tf_op jit(solution)/shard_map/all_to_all | solution.py:356
  65.6 5.6 %all-to-all-start.2 = ((bf16[32,8,2560]{2,1,0:T(8,128)(2,1)}), bf16[32,8,2560]{2,1,0:T(8,128)(2,1)}, u32[]{:S(2)}, u32[]{:S(2)}) async-start(bf16[32,8,2560]{2,1,0:T(8,128)(2,1)} %bitcast.4), calls=%async_computation.2 | async-start | bytes 2621440 | tf_op jit(solution)/shard_map/all_to_all | solution.py:356
  72.9 1.7 collective-permute-start.10
  77.3 10.4 %collective-permute-done.9.refs_11_ = bf16[32,64,128]{2,1,0:T(8,128)(2,1)S(1)} collective-permute-done((bf16[32,64,128]{2,1,0:T(8,128)(2,1)}, bf16[32,64,128]{2,1,0:T(8,128)(2,1)S(1)}, u32[]{:S(2)}, u32[]{:S(2)}) %collective-permute-start.9) | collective-permute-done | bytes 524320 | tf_op jit(solution)/shard_map/ppermute | solution.py:39
  90.3 8.6 %collective-permute-done.2.refs_3_ = bf16[16,2,64,128]{3,2,1,0:T(8,128)(2,1)S(1)} collective-permute-done((bf16[16,2,64,128]{3,2,1,0:T(8,128)(2,1)S(1)}, bf16[16,2,64,128]{3,2,1,0:T(8,128)(2,1)S(1)}, u32[]{:S(2)}, u32[]{:S(2)}) %collective-permute-start.2) | collective-permute-done | bytes 524320 | tf_op jit(solution)/shard_map/ppermute | solution.py:39
  98.9 1.7 collective-permute-done.3.refs_4_
  100.6 3.3 %collective-permute-done.11.refs_13_ = bf16[16,64,128]{2,1,0:T(8,128)(2,1)S(1)} collective-permute-done((bf16[16,64,128]{2,1,0:T(8,128)(2,1)S(1)}, bf16[16,64,128]{2,1,0:T(8,128)(2,1)S(1)}, u32[]{:S(2)}, u32[]{:S(2)}) %collective-permute-start.11) | collective-permute-done | bytes 262176 | tf_op jit(solution)/shard_map/ppermute | solution.py:39
  105.5 6.3 %collective-permute-done.12.refs_14_ = bf16[16,64,128]{2,1,0:T(8,128)(2,1)S(1)} collective-permute-done((bf16[16,64,128]{2,1,0:T(8,128)(2,1)S(1)}, bf16[16,64,128]{2,1,0:T(8,128)(2,1)S(1)}, u32[]{:S(2)}, u32[]{:S(2)}) %collective-permute-start.12) | collective-permute-done | bytes 262176 | tf_op jit(solution)/shard_map/ppermute | solution.py:39
  113.9 1.6 collective-permute-done.17.refs_19_
  115.5 2.7 %collective-permute-start.19 = (bf16[64,384]{1,0:T(8,128)(2,1)S(1)}, bf16[64,384]{1,0:T(8,128)(2,1)S(1)}, u32[]{:S(2)}, u32[]{:S(2)}) collective-permute-start(bf16[64,384]{1,0:T(8,128)(2,1)S(1)} %pad_maximum_fusion), channel_id=1, source_target_pairs={{0,224},{32,0},{64,32},{96,64},{128,96},{160,128},{192,160},{224,1... | collective-permute-start | bytes 147464 | tf_op jit(solution)/shard_map/ppermute | solution.py:39
  118.2 2.4 %collective-permute-start.20 = (bf16[64,384]{1,0:T(8,128)(2,1)S(1)}, bf16[64,384]{1,0:T(8,128)(2,1)S(1)}, u32[]{:S(2)}, u32[]{:S(2)}) collective-permute-start(bf16[64,384]{1,0:T(8,128)(2,1)S(1)} %pad_maximum_fusion), channel_id=1, source_target_pairs={{0,192},{32,224},{64,0},{96,32},{128,64},{160,96},{192,128},{224,1... | collective-permute-start | bytes 147464 | tf_op jit(solution)/shard_map/ppermute | solution.py:39
  122.0 3.7 %collective-permute-start.22 = (bf16[64,384]{1,0:T(8,128)(2,1)S(1)}, bf16[64,384]{1,0:T(8,128)(2,1)S(1)}, u32[]{:S(2)}, u32[]{:S(2)}) collective-permute-start(bf16[64,384]{1,0:T(8,128)(2,1)S(1)} %pad_maximum_fusion), channel_id=1, source_target_pairs={{0,128},{32,160},{64,192},{96,224},{128,0},{160,32},{192,64},{224,... | collective-permute-start | bytes 147464 | tf_op jit(solution)/shard_map/ppermute | solution.py:39
  126.9 10.5 %ffn.1 = (bf16[32,4,8,640]{3,2,1,0:T(8,128)(2,1)}, bf16[32,64,128]{2,1,0:T(8,128)(2,1)}, bf16[32,64,128]{2,1,0:T(8,128)(2,1)}, bf16[32,64,128]{2,1,0:T(8,128)(2,1)}) custom-call(bf16[256,2560]{1,0:T(8,128)(2,1)} %bitcast.5.block_ref, bf16[32,2,64,128]{3,2,1,0:T(8,128)(2,1)} %copy-done.3, bf16[32,2,64,128]{3,2,1,0:T(8,128)(2,1)} %collective-permute-done.refs_1_, ...), custom_call_target="tpu_custom_call" | custom-call | flops 4026531840 | bytes 16777216 | tf_op jit(solution)/shard_map/ffn/pallas_call | solution.py:191
  137.5 13.1 %all-to-all-start.3 = ((bf16[128,8,640]{2,1,0:T(8,128)(2,1)}), bf16[128,8,640]{2,1,0:T(8,128)(2,1)}, u32[]{:S(2)}, u32[]{:S(2)}) async-start(bf16[128,8,640]{2,1,0:T(8,128)(2,1)} %bitcast.31), calls=%async_computation.3 | async-start | bytes 2621440 | tf_op jit(solution)/shard_map/all_to_all | solution.py:356
  150.6 2.6 %collective-permute-start.24 = (bf16[64,384]{1,0:T(8,128)(2,1)S(1)}, bf16[64,384]{1,0:T(8,128)(2,1)S(1)}, u32[]{:S(2)}, u32[]{:S(2)}) collective-permute-start(bf16[64,384]{1,0:T(8,128)(2,1)S(1)} %pad_maximum_fusion), channel_id=1, source_target_pairs={{0,64},{32,96},{64,128},{96,160},{128,192},{160,224},{192,0},{224,... | collective-permute-start | bytes 147464 | tf_op jit(solution)/shard_map/ppermute | solution.py:39
  153.2 1.6 collective-permute-start.25
  154.9 27.6 %collective-permute-done.24 = bf16[64,384]{1,0:T(8,128)(2,1)S(1)} collective-permute-done((bf16[64,384]{1,0:T(8,128)(2,1)S(1)}, bf16[64,384]{1,0:T(8,128)(2,1)S(1)}, u32[]{:S(2)}, u32[]{:S(2)}) %collective-permute-start.24) | collective-permute-done | bytes 49184 | tf_op jit(solution)/shard_map/ppermute | solution.py:39
  183.9 2.6 %collective-permute-start.27 = (bf16[8,64,384]{2,1,0:T(8,128)(2,1)S(1)}, bf16[8,64,384]{2,1,0:T(8,128)(2,1)S(1)}, u32[]{:S(2)}, u32[]{:S(2)}) collective-permute-start(bf16[8,64,384]{2,1,0:T(8,128)(2,1)S(1)} %bitcast_dynamic-update-slice_fusion.refs_0_), channel_id=1, source_target_pairs={{0,16},{8,24},{16,0},{24,8},{1,17},{9,25},{17,1},{25,9},{2,18},{10... | collective-permute-start | bytes 1179656 | tf_op jit(solution)/shard_map/ppermute | solution.py:39
  186.5 8.6 %collective-permute-done.26.refs_1_ = bf16[8,64,384]{2,1,0:T(8,128)(2,1)S(1)} collective-permute-done((bf16[8,64,384]{2,1,0:T(8,128)(2,1)S(1)}, bf16[8,64,384]{2,1,0:T(8,128)(2,1)S(1)}, u32[]{:S(2)}, u32[]{:S(2)}) %collective-permute-start.26) | collective-permute-done | bytes 393248 | tf_op jit(solution)/shard_map/ppermute | solution.py:39
  195.2 2.2 %collective-permute-done.27.refs_2_ = bf16[8,64,384]{2,1,0:T(8,128)(2,1)S(1)} collective-permute-done((bf16[8,64,384]{2,1,0:T(8,128)(2,1)S(1)}, bf16[8,64,384]{2,1,0:T(8,128)(2,1)S(1)}, u32[]{:S(2)}, u32[]{:S(2)}) %collective-permute-start.27) | collective-permute-done | bytes 393248 | tf_op jit(solution)/shard_map/ppermute | solution.py:39
  197.4 4.6 %collective-permute-done.28.refs_3_ = bf16[8,64,384]{2,1,0:T(8,128)(2,1)S(1)} collective-permute-done((bf16[8,64,384]{2,1,0:T(8,128)(2,1)S(1)}, bf16[8,64,384]{2,1,0:T(8,128)(2,1)S(1)}, u32[]{:S(2)}, u32[]{:S(2)}) %collective-permute-start.28) | collective-permute-done | bytes 393248 | tf_op jit(solution)/shard_map/ppermute | solution.py:39
  202.0 2.9 %shared_expert.1 = (bf16[4,256,256]{2,1,0:T(8,128)(2,1)S(1)}, bf16[4,256,256]{2,1,0:T(8,128)(2,1)}, bf16[2048,128]{1,0:T(8,128)(2,1)}, bf16[2048,128]{1,0:T(8,128)(2,1)}, bf16[2048,128]{1,0:T(8,128)(2,1)}) custom-call(s32[3]{0:T(128)S(1)} %pad_add_fusion.at_ref, bf16[256,2048]{1,0:T(8,128)(2,1)S(1)} %get-tuple-element.44.normed_ref, ...), custom_call_target="tpu_custom_call" | custom-call | flops 402653184 | bytes 6291456 | tf_op jit(solution)/shard_map/shared_expert/pallas_call | solution.py:322
  207.1 1.6 collective-permute-start.30
  208.7 2.5 %collective-permute-start.31 = (bf16[256,256]{1,0:T(8,128)(2,1)S(1)}, bf16[256,256]{1,0:T(8,128)(2,1)S(1)}, u32[]{:S(2)}, u32[]{:S(2)}) collective-permute-start(bf16[256,256]{1,0:T(8,128)(2,1)S(1)} %get-tuple-element.49), channel_id=1, source_target_pairs={{0,4},{2,6},{4,0},{6,2},{1,5},{3,7},{5,1},{7,3},{8,12},{10,14},{12... | collective-permute-start | bytes 393224 | tf_op jit(solution)/shard_map/ppermute | solution.py:39
  212.7 2.5 %combine.1 = (f32[256,256]{1,0:T(8,128)S(1)}, bf16[256,256]{1,0:T(8,128)(2,1)S(1)}) custom-call(s32[1]{0:T(128)} %bitcast.core_ref, bf16[1024,640]{1,0:T(8,128)(2,1)} %bitcast.7.back_ref, bf16[256,1024]{1,0:T(8,128)(2,1)S(1)} %get-tuple-element.40.first_hbm, bf16[256,1024]{1,0:T(8,128)(2,1)S(1)} %get-tuple-element.41.last_hbm), custom_call_target="tpu_custom_call" | custom-call | flops 1000000000 | bytes 4194304 | tf_op jit(solution)/shard_map/combine/pallas_call | solution.py:279
  215.3 2.1 collective-permute-done.31
  (109 shorter events, 21.7 us)
Async XLA Ops:
  4.4 39.8 %all-to-all-start = ((bf16[32,2,64,128]{3,2,1,0:T(8,128)(2,1)}), bf16[32,2,64,128]{3,2,1,0:T(8,128)(2,1)S(1)}, u32[]{:S(2)}, u32[]{:S(2)}) async-start(bf16[32,2,64,128]{3,2,1,0:T(8,128)(2,1)} %round_both.1), calls=%async_computation | async-start | bytes 2097152 | tf_op jit(solution)/shard_map/all_to_all | solution.py:356
  44.2 21.5 %all-to-all-start.1 = ((bf16[32,64,128]{2,1,0:T(8,128)(2,1)}), bf16[32,64,128]{2,1,0:T(8,128)(2,1)}, u32[]{:S(2)}, u32[]{:S(2)}) async-start(bf16[32,64,128]{2,1,0:T(8,128)(2,1)} %convert_element_type.30), calls=%async_computation.1 | async-start | bytes 1048576 | tf_op jit(solution)/shard_map/all_to_all | solution.py:356
  49.8 24.9 %collective-permute-start = (bf16[32,2,64,128]{3,2,1,0:T(8,128)(2,1)S(1)}, bf16[32,2,64,128]{3,2,1,0:T(8,128)(2,1)}, u32[]{:S(2)}, u32[]{:S(2)}) collective-permute-start(bf16[32,2,64,128]{3,2,1,0:T(8,128)(2,1)S(1)} %all-to-all-done.refs_0_), channel_id=1, source_target_pairs={{0,2},{2,4},{4,6},{6,0},{1,3},{3,5},{5,7},{7,1},{8,10},{10,12},{12... | collective-permute-start | bytes 3145736 | tf_op jit(solution)/shard_map/ppermute | solution.py:39
  51.4 24.4 %collective-permute-start.1 = (bf16[32,2,64,128]{3,2,1,0:T(8,128)(2,1)S(1)}, bf16[32,2,64,128]{3,2,1,0:T(8,128)(2,1)}, u32[]{:S(2)}, u32[]{:S(2)}) collective-permute-start(bf16[32,2,64,128]{3,2,1,0:T(8,128)(2,1)S(1)} %all-to-all-done.refs_0_), channel_id=1, source_target_pairs={{0,6},{2,0},{4,2},{6,4},{1,7},{3,1},{5,3},{7,5},{8,14},{10,8},{12,... | collective-permute-start | bytes 3145736 | tf_op jit(solution)/shard_map/ppermute | solution.py:39
  65.6 61.3 %all-to-all-start.2 = ((bf16[32,8,2560]{2,1,0:T(8,128)(2,1)}), bf16[32,8,2560]{2,1,0:T(8,128)(2,1)}, u32[]{:S(2)}, u32[]{:S(2)}) async-start(bf16[32,8,2560]{2,1,0:T(8,128)(2,1)} %bitcast.4), calls=%async_computation.2 | async-start | bytes 2621440 | tf_op jit(solution)/shard_map/all_to_all | solution.py:356
  71.3 18.0 %collective-permute-start.4 = (bf16[32,2,64,128]{3,2,1,0:T(8,128)(2,1)S(1)}, bf16[32,2,64,128]{3,2,1,0:T(8,128)(2,1)S(1)}, u32[]{:S(2)}, u32[]{:S(2)}) collective-permute-start(bf16[32,2,64,128]{3,2,1,0:T(8,128)(2,1)S(1)} %all-to-all-done.refs_0_), channel_id=1, source_target_pairs={{0,1},{1,0},{2,3},{3,2},{4,5},{5,4},{6,7},{7,6},{8,9},{9,8},{10,11... | collective-permute-start | bytes 3145736 | tf_op jit(solution)/shard_map/ppermute | solution.py:39
  71.4 16.3 %collective-permute-start.9 = (bf16[32,64,128]{2,1,0:T(8,128)(2,1)}, bf16[32,64,128]{2,1,0:T(8,128)(2,1)S(1)}, u32[]{:S(2)}, u32[]{:S(2)}) collective-permute-start(bf16[32,64,128]{2,1,0:T(8,128)(2,1)} %all-to-all-done.1.refs_10_), channel_id=1, source_target_pairs={{0,2},{2,4},{4,6},{6,0},{1,3},{3,5},{5,7},{7,1},{8,10},{10,12},{12... | collective-permute-start | bytes 1572872 | tf_op jit(solution)/shard_map/ppermute | solution.py:39
  72.9 16.9 %collective-permute-start.10 = (bf16[32,64,128]{2,1,0:T(8,128)(2,1)}, bf16[32,64,128]{2,1,0:T(8,128)(2,1)S(1)}, u32[]{:S(2)}, u32[]{:S(2)}) collective-permute-start(bf16[32,64,128]{2,1,0:T(8,128)(2,1)} %all-to-all-done.1.refs_10_), channel_id=1, source_target_pairs={{0,6},{2,0},{4,2},{6,4},{1,7},{3,1},{5,3},{7,5},{8,14},{10,8},{12,... | collective-permute-start | bytes 1572872 | tf_op jit(solution)/shard_map/ppermute | solution.py:39
  74.7 15.1 %collective-permute-start.13 = (bf16[32,64,128]{2,1,0:T(8,128)(2,1)}, bf16[32,64,128]{2,1,0:T(8,128)(2,1)S(1)}, u32[]{:S(2)}, u32[]{:S(2)}) collective-permute-start(bf16[32,64,128]{2,1,0:T(8,128)(2,1)} %all-to-all-done.1.refs_10_), channel_id=1, source_target_pairs={{0,1},{1,0},{2,3},{3,2},{4,5},{5,4},{6,7},{7,6},{8,9},{9,8},{10,11... | collective-permute-start | bytes 1572872 | tf_op jit(solution)/shard_map/ppermute | solution.py:39
  75.8 23.1 %collective-permute-start.2 = (bf16[16,2,64,128]{3,2,1,0:T(8,128)(2,1)S(1)}, bf16[16,2,64,128]{3,2,1,0:T(8,128)(2,1)S(1)}, u32[]{:S(2)}, u32[]{:S(2)}) collective-permute-start(bf16[16,2,64,128]{3,2,1,0:T(8,128)(2,1)S(1)} %slice.16), channel_id=1, source_target_pairs={{0,2},{2,4},{4,6},{6,0},{1,3},{3,5},{5,7},{7,1},{8,10},{10,12},{12... | collective-permute-start | bytes 1572872 | tf_op jit(solution)/shard_map/ppermute | solution.py:39
  87.7 12.9 %collective-permute-start.3 = (bf16[16,2,64,128]{3,2,1,0:T(8,128)(2,1)S(1)}, bf16[16,2,64,128]{3,2,1,0:T(8,128)(2,1)S(1)}, u32[]{:S(2)}, u32[]{:S(2)}) collective-permute-start(bf16[16,2,64,128]{3,2,1,0:T(8,128)(2,1)S(1)} %slice.17), channel_id=1, source_target_pairs={{0,6},{2,0},{4,2},{6,4},{1,7},{3,1},{5,3},{7,5},{8,14},{10,8},{12,... | collective-permute-start | bytes 1572872 | tf_op jit(solution)/shard_map/ppermute | solution.py:39
  89.3 14.7 %collective-permute-start.11 = (bf16[16,64,128]{2,1,0:T(8,128)(2,1)S(1)}, bf16[16,64,128]{2,1,0:T(8,128)(2,1)S(1)}, u32[]{:S(2)}, u32[]{:S(2)}) collective-permute-start(bf16[16,64,128]{2,1,0:T(8,128)(2,1)S(1)} %slice.18), channel_id=1, source_target_pairs={{0,2},{2,4},{4,6},{6,0},{1,3},{3,5},{5,7},{7,1},{8,10},{10,12},{12... | collective-permute-start | bytes 786440 | tf_op jit(solution)/shard_map/ppermute | solution.py:39
  89.8 22.0 %collective-permute-start.14 = (bf16[32,64,128]{2,1,0:T(8,128)(2,1)S(1)}, bf16[32,64,128]{2,1,0:T(8,128)(2,1)S(1)}, u32[]{:S(2)}, u32[]{:S(2)}) collective-permute-start(bf16[32,64,128]{2,1,0:T(8,128)(2,1)S(1)} %collective-permute-done.9.refs_11_), channel_id=1, source_target_pairs={{0,1},{1,0},{2,3},{3,2},{4,5},{5,4},{6,7},{7,6},{8,9},{9,8},{10,11... | collective-permute-start | bytes 1572872 | tf_op jit(solution)/shard_map/ppermute | solution.py:39
  89.8 22.5 %collective-permute-start.15 = (bf16[32,64,128]{2,1,0:T(8,128)(2,1)S(1)}, bf16[32,64,128]{2,1,0:T(8,128)(2,1)S(1)}, u32[]{:S(2)}, u32[]{:S(2)}) collective-permute-start(bf16[32,64,128]{2,1,0:T(8,128)(2,1)S(1)} %collective-permute-done.10.refs_12_), channel_id=1, source_target_pairs={{0,1},{1,0},{2,3},{3,2},{4,5},{5,4},{6,7},{7,6},{8,9},{9,8},{10,11... | collective-permute-start | bytes 1572872 | tf_op jit(solution)/shard_map/ppermute | solution.py:39
  98.9 23.1 %collective-permute-start.5 = (bf16[32,2,64,128]{3,2,1,0:T(8,128)(2,1)}, bf16[32,2,64,128]{3,2,1,0:T(8,128)(2,1)S(1)}, u32[]{:S(2)}, u32[]{:S(2)}) collective-permute-start(bf16[32,2,64,128]{3,2,1,0:T(8,128)(2,1)} %collective-permute-done.refs_1_), channel_id=1, source_target_pairs={{0,1},{1,0},{2,3},{3,2},{4,5},{5,4},{6,7},{7,6},{8,9},{9,8},{10,11... | collective-permute-start | bytes 3145736 | tf_op jit(solution)/shard_map/ppermute | solution.py:39
  100.6 25.1 %collective-permute-start.6 = (bf16[32,2,64,128]{3,2,1,0:T(8,128)(2,1)}, bf16[32,2,64,128]{3,2,1,0:T(8,128)(2,1)S(1)}, u32[]{:S(2)}, u32[]{:S(2)}) collective-permute-start(bf16[32,2,64,128]{3,2,1,0:T(8,128)(2,1)} %collective-permute-done.1.refs_2_), channel_id=1, source_target_pairs={{0,1},{1,0},{2,3},{3,2},{4,5},{5,4},{6,7},{7,6},{8,9},{9,8},{10,11... | collective-permute-start | bytes 3145736 | tf_op jit(solution)/shard_map/ppermute | solution.py:39
  104.0 7.9 %collective-permute-start.12 = (bf16[16,64,128]{2,1,0:T(8,128)(2,1)S(1)}, bf16[16,64,128]{2,1,0:T(8,128)(2,1)S(1)}, u32[]{:S(2)}, u32[]{:S(2)}) collective-permute-start(bf16[16,64,128]{2,1,0:T(8,128)(2,1)S(1)} %slice.19), channel_id=1, source_target_pairs={{0,6},{2,0},{4,2},{6,4},{1,7},{3,1},{5,3},{7,5},{8,14},{10,8},{12,... | collective-permute-start | bytes 786440 | tf_op jit(solution)/shard_map/ppermute | solution.py:39
  113.2 7.4 %collective-permute-start.8 = (bf16[16,2,64,128]{3,2,1,0:T(8,128)(2,1)S(1)}, bf16[16,2,64,128]{3,2,1,0:T(8,128)(2,1)S(1)}, u32[]{:S(2)}, u32[]{:S(2)}) collective-permute-start(bf16[16,2,64,128]{3,2,1,0:T(8,128)(2,1)S(1)} %collective-permute-done.3.refs_4_), channel_id=1, source_target_pairs={{0,1},{1,0},{2,3},{3,2},{4,5},{5,4},{6,7},{7,6},{8,9},{9,8},{10,11... | collective-permute-start | bytes 1572872 | tf_op jit(solution)/shard_map/ppermute | solution.py:39
  115.5 35.1 %collective-permute-start.19 = (bf16[64,384]{1,0:T(8,128)(2,1)S(1)}, bf16[64,384]{1,0:T(8,128)(2,1)S(1)}, u32[]{:S(2)}, u32[]{:S(2)}) collective-permute-start(bf16[64,384]{1,0:T(8,128)(2,1)S(1)} %pad_maximum_fusion), channel_id=1, source_target_pairs={{0,224},{32,0},{64,32},{96,64},{128,96},{160,128},{192,160},{224,1... | collective-permute-start | bytes 147464 | tf_op jit(solution)/shard_map/ppermute | solution.py:39
  118.2 35.0 %collective-permute-start.20 = (bf16[64,384]{1,0:T(8,128)(2,1)S(1)}, bf16[64,384]{1,0:T(8,128)(2,1)S(1)}, u32[]{:S(2)}, u32[]{:S(2)}) collective-permute-start(bf16[64,384]{1,0:T(8,128)(2,1)S(1)} %pad_maximum_fusion), channel_id=1, source_target_pairs={{0,192},{32,224},{64,0},{96,32},{128,64},{160,96},{192,128},{224,1... | collective-permute-start | bytes 147464 | tf_op jit(solution)/shard_map/ppermute | solution.py:39
  120.5 34.3 %collective-permute-start.21 = (bf16[64,384]{1,0:T(8,128)(2,1)S(1)}, bf16[64,384]{1,0:T(8,128)(2,1)S(1)}, u32[]{:S(2)}, u32[]{:S(2)}) collective-permute-start(bf16[64,384]{1,0:T(8,128)(2,1)S(1)} %pad_maximum_fusion), channel_id=1, source_target_pairs={{0,160},{32,192},{64,224},{96,0},{128,32},{160,64},{192,96},{224,1... | collective-permute-start | bytes 147464 | tf_op jit(solution)/shard_map/ppermute | solution.py:39
  122.0 32.9 %collective-permute-start.22 = (bf16[64,384]{1,0:T(8,128)(2,1)S(1)}, bf16[64,384]{1,0:T(8,128)(2,1)S(1)}, u32[]{:S(2)}, u32[]{:S(2)}) collective-permute-start(bf16[64,384]{1,0:T(8,128)(2,1)S(1)} %pad_maximum_fusion), channel_id=1, source_target_pairs={{0,128},{32,160},{64,192},{96,224},{128,0},{160,32},{192,64},{224,... | collective-permute-start | bytes 147464 | tf_op jit(solution)/shard_map/ppermute | solution.py:39
  126.8 28.1 %collective-permute-start.23 = (bf16[64,384]{1,0:T(8,128)(2,1)S(1)}, bf16[64,384]{1,0:T(8,128)(2,1)S(1)}, u32[]{:S(2)}, u32[]{:S(2)}) collective-permute-start(bf16[64,384]{1,0:T(8,128)(2,1)S(1)} %pad_maximum_fusion), channel_id=1, source_target_pairs={{0,96},{32,128},{64,160},{96,192},{128,224},{160,0},{192,32},{224,... | collective-permute-start | bytes 147464 | tf_op jit(solution)/shard_map/ppermute | solution.py:39
  137.5 75.2 %all-to-all-start.3 = ((bf16[128,8,640]{2,1,0:T(8,128)(2,1)}), bf16[128,8,640]{2,1,0:T(8,128)(2,1)}, u32[]{:S(2)}, u32[]{:S(2)}) async-start(bf16[128,8,640]{2,1,0:T(8,128)(2,1)} %bitcast.31), calls=%async_computation.3 | async-start | bytes 2621440 | tf_op jit(solution)/shard_map/all_to_all | solution.py:356
  150.6 32.0 %collective-permute-start.24 = (bf16[64,384]{1,0:T(8,128)(2,1)S(1)}, bf16[64,384]{1,0:T(8,128)(2,1)S(1)}, u32[]{:S(2)}, u32[]{:S(2)}) collective-permute-start(bf16[64,384]{1,0:T(8,128)(2,1)S(1)} %pad_maximum_fusion), channel_id=1, source_target_pairs={{0,64},{32,96},{64,128},{96,160},{128,192},{160,224},{192,0},{224,... | collective-permute-start | bytes 147464 | tf_op jit(solution)/shard_map/ppermute | solution.py:39
  153.2 29.9 %collective-permute-start.25 = (bf16[64,384]{1,0:T(8,128)(2,1)S(1)}, bf16[64,384]{1,0:T(8,128)(2,1)S(1)}, u32[]{:S(2)}, u32[]{:S(2)}) collective-permute-start(bf16[64,384]{1,0:T(8,128)(2,1)S(1)} %pad_maximum_fusion), channel_id=1, source_target_pairs={{0,32},{32,64},{64,96},{96,128},{128,160},{160,192},{192,224},{224... | collective-permute-start | bytes 147464 | tf_op jit(solution)/shard_map/ppermute | solution.py:39
  183.1 12.1 %collective-permute-start.26 = (bf16[8,64,384]{2,1,0:T(8,128)(2,1)S(1)}, bf16[8,64,384]{2,1,0:T(8,128)(2,1)S(1)}, u32[]{:S(2)}, u32[]{:S(2)}) collective-permute-start(bf16[8,64,384]{2,1,0:T(8,128)(2,1)S(1)} %bitcast_dynamic-update-slice_fusion.refs_0_), channel_id=1, source_target_pairs={{0,24},{8,0},{16,8},{24,16},{1,25},{9,1},{17,9},{25,17},{2,26},{10... | collective-permute-start | bytes 1179656 | tf_op jit(solution)/shard_map/ppermute | solution.py:39
  183.9 13.5 %collective-permute-start.27 = (bf16[8,64,384]{2,1,0:T(8,128)(2,1)S(1)}, bf16[8,64,384]{2,1,0:T(8,128)(2,1)S(1)}, u32[]{:S(2)}, u32[]{:S(2)}) collective-permute-start(bf16[8,64,384]{2,1,0:T(8,128)(2,1)S(1)} %bitcast_dynamic-update-slice_fusion.refs_0_), channel_id=1, source_target_pairs={{0,16},{8,24},{16,0},{24,8},{1,17},{9,25},{17,1},{25,9},{2,18},{10... | collective-permute-start | bytes 1179656 | tf_op jit(solution)/shard_map/ppermute | solution.py:39
  186.4 15.6 %collective-permute-start.28 = (bf16[8,64,384]{2,1,0:T(8,128)(2,1)S(1)}, bf16[8,64,384]{2,1,0:T(8,128)(2,1)S(1)}, u32[]{:S(2)}, u32[]{:S(2)}) collective-permute-start(bf16[8,64,384]{2,1,0:T(8,128)(2,1)S(1)} %bitcast_dynamic-update-slice_fusion.refs_0_), channel_id=1, source_target_pairs={{0,8},{8,16},{16,24},{24,0},{1,9},{9,17},{17,25},{25,1},{2,10},{10... | collective-permute-start | bytes 1179656 | tf_op jit(solution)/shard_map/ppermute | solution.py:39
  207.1 8.2 %collective-permute-start.30 = (bf16[256,256]{1,0:T(8,128)(2,1)S(1)}, bf16[256,256]{1,0:T(8,128)(2,1)S(1)}, u32[]{:S(2)}, u32[]{:S(2)}) collective-permute-start(bf16[256,256]{1,0:T(8,128)(2,1)S(1)} %get-tuple-element.48), channel_id=1, source_target_pairs={{0,2},{2,4},{4,6},{6,0},{1,3},{3,5},{5,7},{7,1},{8,10},{10,12},{12... | collective-permute-start | bytes 393224 | tf_op jit(solution)/shard_map/ppermute | solution.py:39
  208.7 8.8 %collective-permute-start.31 = (bf16[256,256]{1,0:T(8,128)(2,1)S(1)}, bf16[256,256]{1,0:T(8,128)(2,1)S(1)}, u32[]{:S(2)}, u32[]{:S(2)}) collective-permute-start(bf16[256,256]{1,0:T(8,128)(2,1)S(1)} %get-tuple-element.49), channel_id=1, source_target_pairs={{0,4},{2,6},{4,0},{6,2},{1,5},{3,7},{5,1},{7,3},{8,12},{10,14},{12... | collective-permute-start | bytes 393224 | tf_op jit(solution)/shard_map/ppermute | solution.py:39
  211.2 6.3 %collective-permute-start.32 = (bf16[256,256]{1,0:T(8,128)(2,1)S(1)}, bf16[256,256]{1,0:T(8,128)(2,1)S(1)}, u32[]{:S(2)}, u32[]{:S(2)}) collective-permute-start(bf16[256,256]{1,0:T(8,128)(2,1)S(1)} %get-tuple-element.50), channel_id=1, source_target_pairs={{0,6},{2,0},{4,2},{6,4},{1,7},{3,1},{5,3},{7,5},{8,14},{10,8},{12,... | collective-permute-start | bytes 393224 | tf_op jit(solution)/shard_map/ppermute | solution.py:39
  (25 other events, 473.7 us)
